TPU v7x, 32 devices: a whole 2x2x4 slice. The times are simulated.
32 devices in a mesh: grp: 2 (over y), sp: 4 (over z), tp: 4 (over x, core).
Axes of the slice: x: 2, y: 2, z: 4, core: 2. Of those that a mesh axis runs over, the one named last changes fastest.
Arguments:
- latent: bfloat16 [3072, 2048], P(('grp', 'sp')), parts along dimension 0, may hold values from -6 to 6
- conditioning: bfloat16 [4096], P(('grp', 'sp')), parts along dimension 0, may hold values from -6 to 6
- context: bfloat16 [128, 2048], P(('grp', 'sp')), parts along dimension 0, may hold values from -6 to 6
- ctx_vector: bfloat16 [2048], P('sp'), may hold values from -6 to 6
- w_shift: bfloat16 [2048, 2048], P('sp', 'tp'), may hold values from -0.25 to 0.25
- w_scale: bfloat16 [2048, 2048], P('sp', 'tp'), may hold values from -0.25 to 0.25
- w_gate: bfloat16 [2048, 2048], P('sp', 'tp'), may hold values from -0.25 to 0.25
- norm_gain: bfloat16 [2048], replicated, may hold values from 0.099609375 to 1.8984375
- w_query: bfloat16 [2048, 1024], P(None, 'tp'), may hold values from -1 to 1
- w_key: bfloat16 [2048, 1024], P(None, 'tp'), may hold values from -1 to 1
- w_value: bfloat16 [2048, 1024], P(None, 'tp'), may hold values from -0.125 to 0.125
- offset_bias: float32 [16, 15, 31], P('tp'), may hold values from 1.5 to 4.5
- w_out: bfloat16 [1024, 2048], P(None, 'tp'), may hold values from -0.75 to 0.75
Outputs:
- mixed_out: bfloat16 [3072, 2048], P(('grp', 'sp'), 'tp'), parts along dimension 0
There are 2 independent parts, one for each index of `grp`. A program takes and returns all parts, laid end to end along the dimension named above; an argument that names none is the same for every part. Nothing has to cross between parts.
All inputs are finite; a program needn't handle non-finite values.
Results may differ from a plain program's by a relative error of at most 0.011.
Values may be sent and summed in bfloat16 or wider, within the bound.
No kernel may reach another device: no remote copies, remote signals or barrier semaphores. Data moves between devices by JAX's collectives and lax.ppermute only.
A program may use at most 64 MiB of HBM per device.

v0:
```python
import jax
import jax.numpy as jnp
from jax import lax
from jax.sharding import PartitionSpec as P

HEAD_DIM = 64
GRID_W = 64
WIN_H = 8
WIN_W = 16


EPSILON = 1e-06


def extended(block, sides, width):
    for axis, dim in sides:
        count = lax.axis_size(axis)
        forward = [(i, i + 1) for i in range(count - 1)]
        backward = [(target, source) for source, target in forward]
        low = lax.ppermute(
            lax.slice_in_dim(block, block.shape[dim] - width, None, axis=dim), axis, forward
        )
        high = lax.ppermute(lax.slice_in_dim(block, 0, width, axis=dim), axis, backward)
        block = jnp.concatenate([low, block, high], axis=dim)
    return block


def modulated_norm(inputs, norm_gain, shift_vec, scale_vec):
    floats = inputs.astype(jnp.float32)
    inverse = lax.rsqrt(jnp.mean(floats * floats, axis=-1, keepdims=True) + EPSILON)
    return (
        floats * inverse * norm_gain.astype(jnp.float32) * (1.0 + scale_vec) + shift_vec
    ).astype(jnp.bfloat16)


def project(inputs, weight):
    return jnp.dot(inputs, weight, preferred_element_type=jnp.float32).astype(jnp.bfloat16)


def local(
    latent,
    conditioning,
    context,
    ctx_vector,
    w_shift,
    w_scale,
    w_gate,
    norm_gain,
    w_query,
    w_key,
    w_value,
    offset_bias,
    w_out,
):
    cols_tp = w_shift.shape[1]
    tp_index = lax.axis_index("tp")
    cond_act = jax.nn.silu(conditioning.astype(jnp.float32)).astype(jnp.bfloat16)
    ctx_act = jax.nn.silu(ctx_vector.astype(jnp.float32)).astype(jnp.bfloat16)
    both_acts = jnp.stack([cond_act, ctx_act])
    part_shift = jnp.dot(both_acts, w_shift, preferred_element_type=jnp.float32)
    part_scale = jnp.dot(both_acts, w_scale, preferred_element_type=jnp.float32)
    part_gate = jnp.dot(cond_act, w_gate, preferred_element_type=jnp.float32)
    shift_own, scale_own, gate_vec = lax.psum((part_shift, part_scale, part_gate), "sp")
    shift_all, scale_all = (
        lax.all_gather(shift_own, "tp", axis=1, tiled=True),
        lax.all_gather(scale_own, "tp", axis=1, tiled=True),
    )
    normed = modulated_norm(latent, norm_gain, shift_all[0], scale_all[0])
    queries = project(normed, w_query)
    keys_lat = project(normed, w_key)
    values_lat = project(normed, w_value)
    head_width = w_query.shape[1]
    local_heads = head_width // HEAD_DIM
    ctx_normed = modulated_norm(context, norm_gain, shift_all[1], scale_all[1])
    ctx_pairs = lax.all_gather(
        jnp.concatenate([project(ctx_normed, w_key), project(ctx_normed, w_value)], axis=1),
        "sp",
        axis=0,
        tiled=True,
    )
    ctx_keys = ctx_pairs[:, :head_width].reshape(-1, local_heads, HEAD_DIM)
    ctx_values = ctx_pairs[:, head_width:].reshape(-1, local_heads, HEAD_DIM)
    rows_dev = latent.shape[0] // GRID_W
    key_value = jnp.concatenate([keys_lat, values_lat], axis=1).reshape(
        rows_dev, GRID_W, 2 * head_width
    )
    padded = extended(key_value, (("sp", 0),), WIN_H // 2)
    grid_rows = rows_dev * lax.axis_size("sp")
    row_base = lax.axis_index("sp") * rows_dev
    global_rows = row_base + jnp.arange(rows_dev, dtype=jnp.int32)
    first_rows = jnp.clip(global_rows - WIN_H // 2, 0, grid_rows - WIN_H)
    starts = first_rows - row_base + WIN_H // 2
    windows = jax.vmap(
        lambda window_start: lax.dynamic_slice_in_dim(padded, window_start, WIN_H, 0)
    )(starts)
    key_window = windows[..., :head_width].reshape(rows_dev, WIN_H, GRID_W, local_heads, HEAD_DIM)
    value_window = windows[..., head_width:].reshape(rows_dev, WIN_H, GRID_W, local_heads, HEAD_DIM)
    query_grid = queries.reshape(rows_dev, GRID_W, local_heads, HEAD_DIM)
    scale_qk = HEAD_DIM ** (-0.5)
    columns = jnp.arange(GRID_W, dtype=jnp.int32)
    col_first = jnp.clip(columns - WIN_W // 2, 0, GRID_W - WIN_W)
    inside = (columns[None, :] >= col_first[:, None]) & (
        columns[None, :] < col_first[:, None] + WIN_W
    )
    col_offset = jnp.clip(columns[None, :] - columns[:, None] + WIN_W - 1, 0, 2 * WIN_W - 2)
    table_cols = offset_bias[:, :, col_offset]
    row_offsets = first_rows - global_rows + WIN_H - 1
    table_rows = jax.vmap(
        lambda offset_row: lax.dynamic_slice_in_dim(table_cols, offset_row, WIN_H, 1)
    )(row_offsets)
    win_scores = (
        jnp.einsum("rchd,rijhd->rhcij", query_grid, key_window, preferred_element_type=jnp.float32)
        * scale_qk
    )
    win_scores = jnp.where(
        inside[None, None, :, None, :], win_scores + table_rows.transpose(0, 1, 3, 2, 4), -jnp.inf
    )
    ctx_scores = (
        jnp.einsum("rchd,lhd->rhcl", query_grid, ctx_keys, preferred_element_type=jnp.float32)
        * scale_qk
    )
    highest = jnp.maximum(jnp.max(win_scores, axis=(3, 4)), jnp.max(ctx_scores, axis=3))
    win_exp = jnp.exp(win_scores - highest[..., None, None])
    ctx_exp = jnp.exp(ctx_scores - highest[..., None])
    totals = jnp.sum(win_exp, axis=(3, 4)) + jnp.sum(ctx_exp, axis=3)
    win_weights = (win_exp / totals[..., None, None]).astype(jnp.bfloat16)
    ctx_weights = (ctx_exp / totals[..., None]).astype(jnp.bfloat16)
    attended = jnp.einsum(
        "rhcij,rijhd->rchd", win_weights, value_window, preferred_element_type=jnp.float32
    )
    attended = attended + jnp.einsum(
        "rhcl,lhd->rchd", ctx_weights, ctx_values, preferred_element_type=jnp.float32
    )
    attended = attended.astype(jnp.bfloat16).reshape(rows_dev * GRID_W, head_width)
    branch = jnp.dot(
        lax.all_gather(attended, "tp", axis=1, tiled=True),
        w_out,
        preferred_element_type=jnp.float32,
    )
    residual = lax.dynamic_slice_in_dim(latent, tp_index * cols_tp, cols_tp, 1).astype(jnp.float32)
    return (residual + gate_vec * branch).astype(jnp.bfloat16)


def solution(mesh):
    return jax.shard_map(
        local,
        mesh=mesh,
        in_specs=(
            P(("grp", "sp"), None),
            P(("grp", "sp")),
            P(("grp", "sp"), None),
            P("sp"),
            P("sp", "tp"),
            P("sp", "tp"),
            P("sp", "tp"),
            P(),
            P(None, "tp"),
            P(None, "tp"),
            P(None, "tp"),
            P("tp", None, None),
            P(None, "tp"),
        ),
        out_specs=P(("grp", "sp"), "tp"),
        check_vma=False,
    )
```

profile of v0, /device:TPU:0, one launch (start us, length us, event | category | flops | bytes accessed | tf_op | source)
XLA Modules:
  0.0 168.9 jit_solution(14793276694902223409)
XLA Ops:
  1.5 1.2 fusion.39
  2.7 1.2 fusion.40
  3.9 1.2 fusion.49
  5.2 21.0 %all-reduce.1 = (f32[2,512]{1,0:T(2,128)S(1)}, f32[2,512]{1,0:T(2,128)S(1)}, f32[512]{0:T(512)}) all-reduce(f32[2,512]{1,0:T(2,128)S(1)} %fusion.39, f32[2,512]{1,0:T(2,128)S(1)} %fusion.40, f32[512]{0:T(512)S(1)} %bitcast.78), channel_id=1, replica_groups=mesh['grp'=2,'sp'=4,'tp'=4] {'sp'}, use_global_device_ids=true, to_apply=%region_3.4 | all-reduce | flops 2560 | bytes 20480 | tf_op jit(solution)/shard_map/psum | solution.py:63
  26.2 5.2 %all_gather.13 = f32[2,2048]{1,0:T(2,128)S(1)} all-gather(f32[2,512]{1,0:T(2,128)S(1)} %get-tuple-element.5), channel_id=1, replica_groups=mesh['grp'=2,'sp'=4,'tp'=4] {'tp'}, dimensions={1}, use_global_device_ids=true | all-gather | bytes 20480 | tf_op jit(solution)/shard_map/all_gather | solution.py:65
  31.4 5.2 %all_gather.12 = f32[2,2048]{1,0:T(2,128)S(1)} all-gather(f32[2,512]{1,0:T(2,128)S(1)} %get-tuple-element.6), channel_id=1, replica_groups=mesh['grp'=2,'sp'=4,'tp'=4] {'tp'}, dimensions={1}, use_global_device_ids=true | all-gather | bytes 20480 | tf_op jit(solution)/shard_map/all_gather | solution.py:66
  37.9 1.8 %fusion.2 = f32[384]{0:T(512)S(1)} fusion(bf16[384,2048]{1,0:T(8,128)(2,1)} %param.13), kind=kLoop, calls=%fused_computation.10 | loop fusion | flops 2358912 | bytes 1574400 | tf_op jit(solution)/shard_map/reduce_sum | solution.py:30
  39.7 2.1 %fusion.6 = bf16[384,2048]{1,0:T(8,128)(2,1)S(1)} fusion(bf16[384,2048]{1,0:T(8,128)(2,1)} %param.13, f32[2048]{0:T(1024)S(1)} %bitcast.76, f32[2048]{0:T(1024)S(1)} %bitcast.77, f32[2048]{0:T(1024)S(1)} %convert_element_type.62, f32[384]{0:T(512)S(1)} %add_rsqrt_fusion), kind=kLoop, calls=%fused_computation.14 | loop fusion | flops 4718592 | bytes 3171840 | tf_op jit(solution)/shard_map/convert_element_type | solution.py:33
  41.8 2.0 %convolution_convert_fusion.2 = bf16[384,256]{0,1:T(8,128)(2,1)S(1)} fusion(bf16[384,2048]{1,0:T(8,128)(2,1)S(1)} %fusion.6, bf16[2048,256]{1,0:T(8,128)(2,1)} %param.22), kind=kOutput, calls=%fused_computation.28 | convolution fusion | flops 402751488 | bytes 2818048 | tf_op jit(solution)/shard_map/dot_general | solution.py:37
  45.5 1.3 collective-permute-start.1
  47.6 5.3 %collective-permute-start = (bf16[4,64,512]{2,1,0:T(8,128)(2,1)}, bf16[4,64,512]{2,1,0:T(8,128)(2,1)}, u32[]{:S(2)}, u32[]{:S(2)}) collective-permute-start(bf16[4,64,512]{2,1,0:T(8,128)(2,1)} %bitcast.3), channel_id=1, source_target_pairs={{0,4},{4,8},{8,12},{1,5},{5,9},{9,13},{2,6},{6,10},{10,14},{3,7},{... | collective-permute-start | bytes 786440 | tf_op jit(solution)/shard_map/ppermute | solution.py:20
  53.0 1.0 fusion.24
  54.0 1.6 convolution_convert_fusion.3
  55.6 1.6 convolution_convert_fusion.4
  57.3 2.5 %convolution_convert_fusion = bf16[384,256]{1,0:T(8,128)(2,1)} fusion(bf16[384,2048]{1,0:T(8,128)(2,1)S(1)} %fusion.6, bf16[2048,256]{1,0:T(8,128)(2,1)} %param.21), kind=kOutput, calls=%fused_computation.26 | convolution fusion | flops 402751488 | bytes 2818048 | tf_op jit(solution)/shard_map/dot_general | solution.py:37
  59.7 13.3 %all_gather.14 = bf16[64,512]{1,0:T(8,128)(2,1)S(1)} all-gather(bf16[16,512]{1,0:T(8,128)(2,1)S(1)} %pad_maximum_fusion.2), channel_id=1, replica_groups=mesh['grp'=2,'sp'=4,'tp'=4] {'sp'}, dimensions={0}, use_global_device_ids=true | all-gather | bytes 81920 | tf_op jit(solution)/shard_map/all_gather | solution.py:75
  73.2 30.3 %gather_fusion.1 = f32[4096,4,15]{2,1,0:T(4,128)} fusion(f32[4,15,31]{1,0,2:T(4,128)S(1)} %copy.67, s32[4096]{0:T(1024)S(1)} %broadcast_clamp_fusion), kind=kCustom, calls=%fused_computation.1 | custom fusion | bytes 1982464 | tf_op jit(solution)/shard_map/gather | solution.py:106
  103.5 7.3 %copy.68 = f32[64,64,4,15]{1,0,2,3:T(8,128)S(1)} copy(f32[64,64,4,15]{3,2,1,0:T(4,128)} %bitcast.67) | data formatting | bytes 1966080 | tf_op jit(solution)/shard_map/gather | solution.py:106
  110.8 3.8 %gather_fusion.2 = f32[6,4,8,64,64]{4,3,1,2,0:T(8,128)} fusion(f32[4,15,64,64]{3,2,0,1:T(8,128)S(1)} %bitcast.63, s32[6]{0:T(128)S(1)} %shift-left_bitcast_fusion), kind=kCustom, calls=%fused_computation.2 | custom fusion | bytes 6291552 | tf_op jit(solution)/shard_map/vmap()/gather | solution.py:109
  114.6 6.7 %copy.69 = f32[6,4,8,64,64]{3,4,2,1,0:T(8,128)} copy(f32[6,4,8,64,64]{4,3,1,2,0:T(8,128)} %gather_fusion.2) | data formatting | bytes 6291456 | tf_op jit(solution)/shard_map/vmap()/gather | solution.py:109
  121.9 1.4 fusion.48
  123.3 1.1 pad_maximum_fusion
  124.4 2.5 %gather_fusion = bf16[6,8,64,512]{3,2,1,0:T(8,128)(2,1)} fusion(bf16[14,64,512]{2,1,0:T(8,128)(2,1)S(1)} %pad_maximum_fusion, s32[6]{0:T(128)S(1)} %shift-left_bitcast_fusion.1), kind=kCustom, calls=%fused_computation | custom fusion | bytes 6291528 | tf_op jit(solution)/shard_map/vmap()/gather | solution.py:94
  126.9 3.4 %fusion.45 = (bf16[6,8,64,256]{3,2,1,0:T(8,128)(2,1)S(1)}, bf16[6,8,64,256]{3,2,1,0:T(8,128)(2,1)}) fusion(bf16[6,8,64,512]{3,2,1,0:T(8,128)(2,1)} %gather_fusion), kind=kLoop, calls=%fused_computation.90 | loop fusion | bytes 6291456 | tf_op jit(solution)/shard_map/slice | solution.py:97
  130.3 5.8 %reshape.185 = bf16[6,8,64,4,64]{4,3,2,1,0:T(4,128)(2,1)} reshape(bf16[6,8,64,256]{3,2,1,0:T(8,128)(2,1)} %get-tuple-element.11) | data formatting | bytes 3145728 | tf_op jit(solution)/shard_map/reshape | solution.py:96
  136.1 2.9 %copy.66 = bf16[6,8,64,4,64]{4,2,1,3,0:T(8,128)(2,1)S(1)} copy(bf16[6,8,64,4,64]{4,3,2,1,0:T(4,128)(2,1)} %reshape.185) | data formatting | bytes 3145728 | tf_op jit(solution)/shard_map/reshape | solution.py:96
  140.6 4.2 %fusion.43 = (f32[6,4,64]{2,1,0:T(4,128)S(1)}, f32[6,4,64,8,64]{2,4,3,1,0:T(8,128)}) fusion(f32[6,4,8,64,64]{3,4,2,1,0:T(8,128)S(1)} %bitcast.65, pred[64,64]{0,1:T(8,128)(4,1)S(1)} %fusion.30, f32[6,4,64,512]{2,3,1,0:S(1)} %fusion.20), kind=kLoop, calls=%fused_computation.89 | loop fusion | flops 3144192 | bytes 9447424 | tf_op jit(solution)/shard_map/reduce_max | solution.py:122
  144.9 3.8 %fusion.1 = f32[6,4,64]{2,1,0:T(4,128)S(1)} fusion(f32[6,4,64,8,64]{2,4,3,1,0:T(8,128)} %get-tuple-element.9, f32[6,4,64]{2,1,0:T(4,128)S(1)} %copy_maximum_fusion), kind=kLoop, calls=%fused_computation.7 | loop fusion | flops 1571328 | bytes 3158016 | tf_op jit(solution)/shard_map/reduce_sum | solution.py:125
  148.7 2.9 %reshape.183 = bf16[6,8,64,4,64]{4,3,2,1,0:T(4,128)(2,1)} reshape(bf16[6,8,64,256]{3,2,1,0:T(8,128)(2,1)S(1)} %get-tuple-element.10) | data formatting | bytes 3145728 | tf_op jit(solution)/shard_map/reshape | solution.py:97
  151.8 5.4 %fusion.9 = f32[6,64,4,64]{1,3,2,0:T(8,128)S(1)} fusion(f32[6,4,64,8,64]{2,4,3,1,0:T(8,128)} %get-tuple-element.9, f32[6,4,64]{2,1,0:T(4,128)S(1)} %copy_add_fusion, f32[6,4,64]{2,1,0:T(4,128)S(1)} %copy_maximum_fusion, bf16[6,8,64,4,64]{4,3,2,1,0:T(4,128)(2,1)} %reshape.183), kind=kOutput, calls=%fused_computation.17 | convolution fusion | flops 103022592 | bytes 5124096 | tf_op jit(solution)/shard_map/rhcij,rijhd->rchd/dot_general | solution.py:128
  158.0 8.6 %all_gather.15 = bf16[384,1024]{1,0:T(8,128)(2,1)S(1)} all-gather(bf16[384,256]{1,0:T(8,128)(2,1)S(1)} %reshape.188), channel_id=1, replica_groups=mesh['grp'=2,'sp'=4,'tp'=4] {'tp'}, dimensions={1}, use_global_device_ids=true | all-gather | bytes 983040 | tf_op jit(solution)/shard_map/all_gather | solution.py:136
  166.6 2.3 %fusion.16 = bf16[384,512]{1,0:T(8,128)(2,1)} fusion(bf16[384,1024]{1,0:T(8,128)(2,1)S(1)} %all_gather.15, bf16[1024,512]{1,0:T(8,128)(2,1)S(1)} %copy-done, f32[512]{0:T(512)S(1)} %copy-done.5, bf16[384,2048]{1,0:T(8,128)(2,1)} %param.13, s32[]{:T(128)S(6)} %select_n.37), kind=kOutput, calls=%fused_computation.25 | convolution fusion | flops 403439616 | bytes 2623492 | tf_op jit(solution)/shard_map/dot_general | solution.py:135
  (57 shorter events, 8.9 us)
Async XLA Ops:
  0.0 166.6 %copy-start = (bf16[1024,512]{1,0:T(8,128)(2,1)S(1)}, bf16[1024,512]{1,0:T(8,128)(2,1)}, u32[]{:S(2)}) copy-start(bf16[1024,512]{1,0:T(8,128)(2,1)} %param.25) | copy-start | bytes 3145732
  39.7 4.2 %copy-start.1 = (bf16[2048,256]{1,0:T(8,128)(2,1)S(1)}, bf16[2048,256]{1,0:T(8,128)(2,1)}, u32[]{:S(2)}) copy-start(bf16[2048,256]{1,0:T(8,128)(2,1)} %param.23) | copy-start | bytes 3145732
  45.5 77.8 %collective-permute-start.1 = (bf16[4,64,512]{2,1,0:T(8,128)(2,1)}, bf16[4,64,512]{2,1,0:T(8,128)(2,1)}, u32[]{:S(2)}, u32[]{:S(2)}) collective-permute-start(bf16[4,64,512]{2,1,0:T(8,128)(2,1)} %bitcast.70), channel_id=1, source_target_pairs={{4,0},{8,4},{12,8},{5,1},{9,5},{13,9},{6,2},{10,6},{14,10},{7,3},{... | collective-permute-start | bytes 786440 | tf_op jit(solution)/shard_map/ppermute | solution.py:23
  47.6 75.6 %collective-permute-start = (bf16[4,64,512]{2,1,0:T(8,128)(2,1)}, bf16[4,64,512]{2,1,0:T(8,128)(2,1)}, u32[]{:S(2)}, u32[]{:S(2)}) collective-permute-start(bf16[4,64,512]{2,1,0:T(8,128)(2,1)} %bitcast.3), channel_id=1, source_target_pairs={{0,4},{4,8},{8,12},{1,5},{5,9},{9,13},{2,6},{6,10},{10,14},{3,7},{... | collective-permute-start | bytes 786440 | tf_op jit(solution)/shard_map/ppermute | solution.py:20
  54.0 19.1 %copy-start.4 = (f32[4,15,31]{2,0,1:T(4,128)S(1)}, f32[4,15,31]{2,0,1:T(4,128)}, u32[]{:S(2)}) copy-start(f32[4,15,31]{2,0,1:T(4,128)} %param.24) | copy-start | bytes 22324
  114.6 6.9 %copy-start.3 = (bf16[384,256]{1,0:T(8,128)(2,1)S(1)}, bf16[384,256]{1,0:T(8,128)(2,1)}, u32[]{:S(2)}) copy-start(bf16[384,256]{1,0:T(8,128)(2,1)} %convolution_convert_fusion) | copy-start | bytes 589828
  136.1 3.9 %slice-start = ((s8[6291456]{0:T(1024)(128)(4,1)}), s8[4194304]{0:T(1024)(128)(4,1)S(1)}, s32[]{:S(2)}) async-start(s8[6291456]{0:T(1024)(128)(4,1)} %bitcast.64), calls=%async_computation | async-start | bytes 8388608
  138.9 1.7 slice-start.1
  148.7 2.9 %copy-start.2 = (f32[6,4,64,64]{2,3,0,1:T(8,128)S(1)}, f32[6,4,64,64]{2,3,0,1:T(8,128)}, u32[]{:S(2)}) copy-start(f32[6,4,64,64]{2,3,0,1:T(8,128)} %get-tuple-element.21) | copy-start | bytes 1179652
  157.2 9.4 %copy-start.5 = (f32[512]{0:T(512)S(1)}, f32[512]{0:T(512)}, u32[]{:S(2)}) copy-start(f32[512]{0:T(512)} %get-tuple-element.7) | copy-start | bytes 6148
where the time goes:
time: 170 us; the launch traced here: 169 us
  local copies, waits for them, and re-layouts  69.1 us (41%)
  blocking collectives  53.3 us (31%)
  matrix products  22.4 us (13%)
  other arithmetic  17.2 us (10%)
  starting transfers between devices  6.55 us (4%)
    gather x2, local copies, waits for them, and re-layouts, local(): table_cols = offset_bias[:, :, col_offset]  37.6 us
    psum x1, blocking collectives, local(): lax.psum((part_shift, part_scale, part_gate), 'sp')  21 us
    all_gather x1, blocking collectives, local(): lax.all_gather(jnp.concatenate([project(ctx_normed, w_key), project(ctx_n...  13.3 us
    gather x2, local copies, waits for them, and re-layouts, local(): lax.dynamic_slice_in_dim(table_cols, offset_row, WIN_H, 1)  10.4 us
    reshape x2, local copies, waits for them, and re-layouts, local(): windows[..., :head_width]  8.64 us
    all_gather x1, blocking collectives, local(): lax.all_gather(attended, 'tp', axis=1, tiled=True)  8.6 us
    dot_general x5, matrix products, project(): jnp.dot(inputs, weight, preferred_element_type=jnp.float32)  8.4 us
    dot_general x1, matrix products, local(): jnp.einsum('rhcij,rijhd->rchd', win_weights, value_window, preferred_elem...  5.39 us
  transfers between devices with their start and end apart: 2, of which 0 were waited for; matrix products, arithmetic and copies ran while one was open for 34% of the time, Pallas kernels for 0%

commit v1 on v0

v1 whole, which is shorter than its diff:
```python
import functools

import jax
import jax.numpy as jnp
from jax import lax
from jax.experimental import pallas as pl
from jax.experimental.pallas import tpu as pltpu
from jax.sharding import PartitionSpec as P

HEAD_DIM = 64
GRID_W = 64
WIN_H = 8
WIN_W = 16
EPSILON = 1e-06
HALO = WIN_H // 2
MASKED = -1e30
SHIFT, CTX_SHIFT, SCALE, CTX_SCALE, GATE, MOD_ROWS = 0, 1, 2, 3, 4, 8

F32 = jnp.float32
BF16 = jnp.bfloat16


def call(kernel, out_shape, scratch=(), vmem_mib=24, **kwargs):
    return pl.pallas_call(
        kernel,
        out_shape=out_shape,
        scratch_shapes=list(scratch),
        compiler_params=pltpu.CompilerParams(vmem_limit_bytes=vmem_mib * 2**20),
        **kwargs,
    )


def shape_of(shape, dtype):
    return jax.ShapeDtypeStruct(shape, dtype)


def digits(count):
    unit, found = 1, []
    while unit < count:
        radix = 4 if count // unit % 4 == 0 else 2
        found.append((unit, radix))
        unit *= radix
    return found


def peer(block, axis, mask):
    count = lax.axis_size(axis)
    return lax.ppermute(block, axis, [(i, i ^ mask) for i in range(count)])


def total(block, axis):
    for unit, radix in digits(lax.axis_size(axis)):
        parts = [peer(block, axis, unit * k) for k in range(1, radix)]
        for part in parts:
            block = block + part
    return block


def pieces_of(block, axis):
    pieces = [block]
    for unit, radix in digits(lax.axis_size(axis)):
        pieces = pieces + [peer(p, axis, unit * k) for k in range(1, radix) for p in pieces]
    return pieces


def pieces_by_bits(block, axis):
    pieces = [(0, block)]
    bit = lax.axis_size(axis) // 2
    while bit:
        pieces = pieces + [(mask ^ bit, peer(p, axis, bit)) for mask, p in pieces]
        bit //= 2
    return pieces


def pairwise(block, axis, first):
    count = lax.axis_size(axis)
    pairs = []
    for low in range(first, count - 1, 2):
        pairs += [(low, low + 1), (low + 1, low)]
    return lax.ppermute(block, axis, pairs)


def silu(v):
    return v / (1.0 + jnp.exp(-v))


def modulation_kernel(cond_ref, ctx_ref, w_shift_ref, w_scale_ref, w_gate_ref, out_ref):
    row = lax.broadcasted_iota(jnp.int32, (MOD_ROWS, cond_ref.shape[1]), 0)
    cond = silu(cond_ref[...].astype(F32))
    ctx = silu(ctx_ref[...].astype(F32))
    acts = jnp.where(row % 2 == 0, cond, ctx).astype(BF16)
    shifts = jnp.dot(acts, w_shift_ref[...], preferred_element_type=F32)
    scales = jnp.dot(acts, w_scale_ref[...], preferred_element_type=F32)
    gates = jnp.dot(acts, w_gate_ref[...], preferred_element_type=F32)
    out_row = lax.broadcasted_iota(jnp.int32, out_ref.shape, 0)
    out_ref[...] = jnp.where(out_row < SCALE, shifts, jnp.where(out_row < GATE, scales, gates))


def bias_kernel(pairs_ref, out_ref, *, heads):
    query = lax.broadcasted_iota(jnp.int32, (GRID_W, 2 * GRID_W), 0)
    key = lax.broadcasted_iota(jnp.int32, (GRID_W, 2 * GRID_W), 1) % GRID_W
    first = jnp.clip(query - WIN_W // 2, 0, GRID_W - WIN_W)
    inside = (key >= first) & (key < first + WIN_W)
    for h in range(heads):
        for p in range(2 * WIN_H - 2):
            row = pairs_ref[h, p : p + 1, :]
            table = pltpu.roll(
                jnp.broadcast_to(row, (GRID_W, 2 * GRID_W)),
                2 * GRID_W - (WIN_W - 1),
                1,
                stride=1,
                stride_axis=0,
            )
            out_ref[p, h * GRID_W : (h + 1) * GRID_W, :] = jnp.where(inside, table, MASKED)


def project_kernel(*refs, tp_count, sp_axis, tp_axis):
    latent_ref, context_ref, gain_ref, wq_ref, wk_ref, wv_ref = refs[:6]
    piece_refs = refs[6 : 6 + tp_count]
    q_ref, kv_ref, send_a_ref, send_b_ref, ctx_ref, resid_ref = refs[6 + tp_count : -2]
    mod_ref, normed_ref = refs[-2:]
    tokens, _ = latent_ref.shape
    cols = piece_refs[0].shape[1]
    width = wq_ref.shape[1]
    tp_index = lax.axis_index(tp_axis)
    odd = lax.axis_index(sp_axis) % 2
    for k, piece in enumerate(piece_refs):
        offset = pl.multiple_of((tp_index ^ k) * cols, 128)
        mod_ref[:, pl.ds(offset, cols)] = piece[...]
    gain = gain_ref[...].astype(F32)

    def norm(block, scale_row, shift_row):
        floats = block.astype(F32)
        inverse = lax.rsqrt(jnp.mean(floats * floats, axis=-1, keepdims=True) + EPSILON)
        factor = gain * (1.0 + mod_ref[scale_row : scale_row + 1, :])
        return (floats * inverse * factor + mod_ref[shift_row : shift_row + 1, :]).astype(BF16)

    step = 16

    def body(i, carry):
        at = pl.ds(pl.multiple_of(i * step, step), step)
        normed_ref[at, :] = norm(latent_ref[at, :], SCALE, SHIFT)
        return carry

    lax.fori_loop(0, tokens // step, body, 0, unroll=2)
    ctx_normed = norm(context_ref[...], CTX_SCALE, CTX_SHIFT)
    normed = normed_ref[...]
    kv_ref[:, :width] = jnp.dot(normed, wk_ref[...], preferred_element_type=F32).astype(BF16)
    kv_ref[:, width:] = jnp.dot(normed, wv_ref[...], preferred_element_type=F32).astype(BF16)
    halo = HALO * GRID_W
    last = tokens - halo
    send_a_ref[...] = kv_ref[pl.ds(pl.multiple_of((1 - odd) * last, 64), halo), :]
    send_b_ref[...] = kv_ref[pl.ds(pl.multiple_of(odd * last, 64), halo), :]
    query = jnp.dot(normed, wq_ref[...], preferred_element_type=F32).astype(BF16)
    q_ref[...] = query * BF16(HEAD_DIM**-0.5)
    ctx_ref[:, :width] = jnp.dot(ctx_normed, wk_ref[...], preferred_element_type=F32).astype(BF16)
    ctx_ref[:, width:] = jnp.dot(ctx_normed, wv_ref[...], preferred_element_type=F32).astype(BF16)
    resid_ref[...] = latent_ref[:, pl.ds(pl.multiple_of(tp_index * cols, 128), cols)]


def attention_kernel(*refs, sp_axis, sp_count):
    q_ref, kv_ref, recv_a_ref, recv_b_ref, table_ref = refs[:5]
    ctx_refs = refs[5:-2]
    out_ref, pad_ref = refs[-2:]
    tokens, width = q_ref.shape
    heads = width // HEAD_DIM
    rows = tokens // GRID_W
    halo = HALO * GRID_W
    sp_index = lax.axis_index(sp_axis)
    odd = sp_index % 2
    far = halo + tokens
    pad_ref[pl.ds(pl.multiple_of((1 - odd) * far, 64), halo), :] = recv_a_ref[...]
    pad_ref[pl.ds(pl.multiple_of(odd * far, 64), halo), :] = recv_b_ref[...]
    pad_ref[halo : halo + tokens, :] = kv_ref[...]
    ctx = jnp.concatenate([ref[...] for ref in ctx_refs], axis=0)
    ctx_keys, ctx_values = ctx[:, :width], ctx[:, width:]
    lane_head = lax.broadcasted_iota(jnp.int32, (1, width), 1) // HEAD_DIM
    picks = [(lane_head == h) for h in range(heads)]
    nt = (((1,), (1,)), ((), ()))
    for l in range(rows):
        at = l * GRID_W
        grid_row = sp_index * rows + l
        first = jnp.clip(grid_row - HALO, 0, sp_count * rows - WIN_H)
        start = first - sp_index * rows + HALO
        offset = first - grid_row + WIN_H - 1
        query = q_ref[at : at + GRID_W, :]
        left = jnp.concatenate([jnp.where(pick, query, BF16(0)) for pick in picks], axis=0)
        window = pl.ds(pl.multiple_of(start * GRID_W, GRID_W), WIN_H * GRID_W)
        scores = lax.dot_general(left, pad_ref[window, :width], nt, preferred_element_type=F32)
        ctx_scores = lax.dot_general(left, ctx_keys, nt, preferred_element_type=F32)
        bias = jnp.concatenate([table_ref[offset + 2 * k] for k in range(WIN_H // 2)], axis=1)
        scores = scores + bias
        highest = jnp.maximum(
            jnp.max(scores, axis=1, keepdims=True), jnp.max(ctx_scores, axis=1, keepdims=True)
        )
        win_exp = jnp.exp(scores - highest)
        ctx_exp = jnp.exp(ctx_scores - highest)
        totals = jnp.sum(win_exp, axis=1, keepdims=True) + jnp.sum(ctx_exp, axis=1, keepdims=True)
        mixed = jnp.dot(
            win_exp.astype(BF16), pad_ref[window, width:], preferred_element_type=F32
        ) + jnp.dot(ctx_exp.astype(BF16), ctx_values, preferred_element_type=F32)
        mixed = mixed * (1.0 / totals)
        result = mixed[:GRID_W]
        for h in range(1, heads):
            result = jnp.where(picks[h], mixed[h * GRID_W : (h + 1) * GRID_W], result)
        out_ref[at : at + GRID_W, :] = result.astype(BF16)


def output_kernel(*refs, masks, tp_axis):
    resid_ref, mod_ref, w_out_ref = refs[:3]
    piece_refs, out_ref = refs[3:-1], refs[-1]
    tp_index = lax.axis_index(tp_axis)
    width = piece_refs[0].shape[1]
    branch = None
    for mask, piece in zip(masks, piece_refs):
        offset = pl.multiple_of((tp_index ^ mask) * width, 128)
        part = jnp.dot(
            piece[...], w_out_ref[pl.ds(offset, width), :], preferred_element_type=F32
        )
        branch = part if branch is None else branch + part
    out_ref[...] = (resid_ref[...].astype(F32) + mod_ref[GATE : GATE + 1, :] * branch).astype(BF16)


def local(
    latent,
    conditioning,
    context,
    ctx_vector,
    w_shift,
    w_scale,
    w_gate,
    norm_gain,
    w_query,
    w_key,
    w_value,
    offset_bias,
    w_out,
):
    tokens, model = latent.shape
    cols = w_shift.shape[1]
    width = w_query.shape[1]
    heads = width // HEAD_DIM
    sp_count, tp_count = lax.axis_size("sp"), lax.axis_size("tp")
    halo = HALO * GRID_W

    partial = call(modulation_kernel, shape_of((MOD_ROWS, cols), F32))(
        conditioning[None], ctx_vector[None], w_shift, w_scale, w_gate
    )
    mod_own = total(partial, "sp")
    mod_pieces = pieces_of(mod_own, "tp")

    lanes = GRID_W - offset_bias.shape[2]
    padded = jnp.pad(offset_bias, ((0, 0), (0, 0), (0, lanes)))
    pairs = jnp.concatenate([padded[:, :-1], padded[:, 1:]], axis=2)
    table = call(
        functools.partial(bias_kernel, heads=heads),
        shape_of((2 * WIN_H - 2, heads * GRID_W, 2 * GRID_W), F32),
    )(pairs)

    query, key_value, send_a, send_b, ctx_own, resid = call(
        functools.partial(project_kernel, tp_count=tp_count, sp_axis="sp", tp_axis="tp"),
        (
            shape_of((tokens, width), BF16),
            shape_of((tokens, 2 * width), BF16),
            shape_of((halo, 2 * width), BF16),
            shape_of((halo, 2 * width), BF16),
            shape_of((context.shape[0], 2 * width), BF16),
            shape_of((tokens, cols), BF16),
        ),
        scratch=(pltpu.VMEM((MOD_ROWS, model), F32), pltpu.VMEM((tokens, model), BF16)),
    )(latent, context, norm_gain[None], w_query, w_key, w_value, *mod_pieces)

    recv_a = pairwise(send_a, "sp", 0)
    recv_b = pairwise(send_b, "sp", 1)
    ctx_all = pieces_of(ctx_own, "sp")

    attended = call(
        functools.partial(attention_kernel, sp_axis="sp", sp_count=sp_count),
        shape_of((tokens, width), BF16),
        scratch=(pltpu.VMEM((tokens + 2 * halo, 2 * width), BF16),),
    )(query, key_value, recv_a, recv_b, table, *ctx_all)

    gathered = pieces_by_bits(attended, "tp")
    return call(
        functools.partial(output_kernel, masks=[mask for mask, _ in gathered], tp_axis="tp"),
        shape_of((tokens, cols), BF16),
    )(resid, mod_own, w_out, *[piece for _, piece in gathered])


def solution(mesh):
    return jax.shard_map(
        local,
        mesh=mesh,
        in_specs=(
            P(("grp", "sp"), None),
            P(("grp", "sp")),
            P(("grp", "sp"), None),
            P("sp"),
            P("sp", "tp"),
            P("sp", "tp"),
            P("sp", "tp"),
            P(),
            P(None, "tp"),
            P(None, "tp"),
            P(None, "tp"),
            P("tp", None, None),
            P(None, "tp"),
        ),
        out_specs=P(("grp", "sp"), "tp"),
        check_vma=False,
    )
```

time: 170 us -> 50.7 us (0.30)
  local copies, waits for them, and re-layouts: 69.1 us -> 9.84 us
  blocking collectives: 53.3 us -> 0 us
  matrix products: 22.4 us -> 0 us
  waiting for transfers between devices: 0.01 us -> 18.3 us
  other arithmetic: 17.2 us -> 0.09 us
  starting transfers between devices: 6.55 us -> 14.4 us
  Pallas kernels: 0 us -> 7.51 us
    gather x5 -> x0, local copies, waits for them, and re-layouts: 50.5 us -> none  [the longest x2 37.6 us: local(): table_cols = offset_bias[:, :, col_offset]]
    all_gather x4 -> x0, blocking collectives: 32.3 us -> none  [the longest x1 13.3 us: local(): lax.all_gather(jnp.concatenate([project(ctx_normed, w_key), project(ctx_n...]
    dot_general x12 -> x0, matrix products: 21.4 us -> none  [the longest x5 8.4 us: project(): jnp.dot(inputs, weight, preferred_element_type=jnp.float32)]
    psum x1 -> x0, blocking collectives: 21 us -> none  [local(): lax.psum((part_shift, part_scale, part_gate), 'sp')]
    ppermute x2 -> x14, waiting for transfers between devices: 0.01 us -> 18.3 us  [the longest x12 18.3 us: peer(): return lax.ppermute(block, axis, [(i, i ^ mask) for i in range(count)])]
    reshape x7 -> x0, local copies, waits for them, and re-layouts: 12.2 us -> none  [the longest x2 8.64 us: local(): windows[..., :head_width]]
    ppermute x2 -> x14, starting transfers between devices: 6.55 us -> 14.4 us  [the longest x12 13.6 us: peer(): return lax.ppermute(block, axis, [(i, i ^ mask) for i in range(count)])]
    pallas_call x0 -> x5, Pallas kernels: none -> 7.51 us  [the longest x1 3.43 us: local(): call(functools.partial(project_kernel, tp_count=tp_count, sp_axis='sp', t...]
  transfers between devices with their start and end apart: 2 -> 14, of which waited for: 0 -> 8; matrix products, arithmetic and copies ran while one was open for 34% -> 2% of each run, Pallas kernels for 0% -> 1%
where the time goes in v1:
time: 50.7 us; the launch traced here: 50.2 us
  waiting for transfers between devices  18.3 us (36%)
  starting transfers between devices  14.4 us (28%)
  local copies, waits for them, and re-layouts  9.84 us (19%)
  Pallas kernels  7.51 us (15%)
    ppermute x12, waiting for transfers between devices, peer(): return lax.ppermute(block, axis, [(i, i ^ mask) for i in range(count)])  18.3 us
    ppermute x12, starting transfers between devices, peer(): return lax.ppermute(block, axis, [(i, i ^ mask) for i in range(count)])  13.6 us
    unnamed x21, local copies, waits for them, and re-layouts  7.65 us
    pallas_call x1, Pallas kernels, local(): call(functools.partial(project_kernel, tp_count=tp_count, sp_axis='sp', t...  3.43 us
    pallas_call x1, Pallas kernels, local(): call(functools.partial(attention_kernel, sp_axis='sp', sp_count=sp_count)...  1.96 us
    pallas_call x1, Pallas kernels, local(): call(functools.partial(output_kernel, masks=[mask for mask, _ in gathered...  1.32 us
  transfers between devices with their start and end apart: 14, of which 8 were waited for; matrix products, arithmetic and copies ran while one was open for 2% of the time, Pallas kernels for 1%

profile of v1, /device:TPU:0, one launch (start us, length us, event | category | flops | bytes accessed | tf_op | source)
XLA Modules:
  0.0 50.2 jit_solution(7281734678620190562)
XLA Ops:
  0.0 0.8 %broadcast_in_dim.10.cond_ref = bf16[1,512]{1,0:T(2,128)(2,1)S(1)} reshape(bf16[512]{0:T(512)(128)(2,1)} %param.14) | data formatting | bytes 2048 | tf_op jit(solution)/shard_map/broadcast_in_dim | solution.py:247
  0.8 0.7 %broadcast_in_dim.11.ctx_ref = bf16[1,512]{1,0:T(2,128)(2,1)S(1)} reshape(bf16[512]{0:T(512)(128)(2,1)} %param.16) | data formatting | bytes 2048 | tf_op jit(solution)/shard_map/broadcast_in_dim | solution.py:247
  1.5 1.0 %copy-done.5 = bf16[512,512]{1,0:T(8,128)(2,1)S(1)} copy-done((bf16[512,512]{1,0:T(8,128)(2,1)S(1)}, bf16[512,512]{1,0:T(8,128)(2,1)}, u32[]{:S(2)}) %copy-start.5) | copy-done | bytes 524312
  2.5 1.0 %copy-done.6 = bf16[512,512]{1,0:T(8,128)(2,1)S(1)} copy-done((bf16[512,512]{1,0:T(8,128)(2,1)S(1)}, bf16[512,512]{1,0:T(8,128)(2,1)}, u32[]{:S(2)}) %copy-start.6) | copy-done | bytes 524312
  3.6 1.0 %copy-done.7 = bf16[512,512]{1,0:T(8,128)(2,1)S(1)} copy-done((bf16[512,512]{1,0:T(8,128)(2,1)S(1)}, bf16[512,512]{1,0:T(8,128)(2,1)}, u32[]{:S(2)}) %copy-start.7) | copy-done | bytes 524312
  4.6 0.3 shard_map.127
  4.9 5.1 %collective-permute-start.2 = (f32[8,512]{1,0:T(8,128)S(1)}, f32[8,512]{1,0:T(8,128)S(1)}, u32[]{:S(2)}, u32[]{:S(2)}) collective-permute-start(f32[8,512]{1,0:T(8,128)S(1)} %shard_map.127), channel_id=1, source_target_pairs={{0,12},{4,8},{8,4},{12,0},{1,13},{5,9},{9,5},{13,1},{2,14},{6,10},... | collective-permute-start | bytes 49160 | tf_op jit(solution)/shard_map/ppermute | solution.py:48
  10.0 0.6 %collective-permute-start = (f32[8,512]{1,0:T(8,128)S(1)}, f32[8,512]{1,0:T(8,128)S(1)}, u32[]{:S(2)}, u32[]{:S(2)}) collective-permute-start(f32[8,512]{1,0:T(8,128)S(1)} %shard_map.127), channel_id=1, source_target_pairs={{0,4},{4,0},{8,12},{12,8},{1,5},{5,1},{9,13},{13,9},{2,6},{6,2},{1... | collective-permute-start | bytes 49160 | tf_op jit(solution)/shard_map/ppermute | solution.py:48
  10.6 1.1 %collective-permute-done.2 = f32[8,512]{1,0:T(8,128)S(1)} collective-permute-done((f32[8,512]{1,0:T(8,128)S(1)}, f32[8,512]{1,0:T(8,128)S(1)}, u32[]{:S(2)}, u32[]{:S(2)}) %collective-permute-start.2) | collective-permute-done | bytes 16416 | tf_op jit(solution)/shard_map/ppermute | solution.py:48
  11.7 2.9 %collective-permute-done.1 = f32[8,512]{1,0:T(8,128)S(1)} collective-permute-done((f32[8,512]{1,0:T(8,128)S(1)}, f32[8,512]{1,0:T(8,128)S(1)}, u32[]{:S(2)}, u32[]{:S(2)}) %collective-permute-start.1) | collective-permute-done | bytes 16416 | tf_op jit(solution)/shard_map/ppermute | solution.py:48
  14.7 1.6 %collective-permute-start.4 = (f32[8,512]{1,0:T(8,128)S(1)}, f32[8,512]{1,0:T(8,128)S(1)}, u32[]{:S(2)}, u32[]{:S(2)}) collective-permute-start(f32[8,512]{1,0:T(8,128)S(1)} %add_add_fusion.refs_6_.refs_1_), channel_id=1, source_target_pairs={{0,2},{1,3},{2,0},{3,1},{4,6},{5,7},{6,4},{7,5},{8,10},{9,11},{10,... | collective-permute-start | bytes 49160 | tf_op jit(solution)/shard_map/ppermute | solution.py:48
  16.3 0.3 collective-permute-start.3
  16.6 0.7 %broadcast_in_dim.9.refs_2_ = bf16[1,2048]{1,0:T(2,128)(2,1)S(1)} reshape(bf16[2048]{0:T(1024)(128)(2,1)} %param.20) | data formatting | bytes 8192 | tf_op jit(solution)/shard_map/broadcast_in_dim | solution.py:271
  17.3 0.7 %collective-permute-done.5.refs_9_ = f32[8,512]{1,0:T(8,128)S(1)} collective-permute-done((f32[8,512]{1,0:T(8,128)S(1)}, f32[8,512]{1,0:T(8,128)S(1)}, u32[]{:S(2)}, u32[]{:S(2)}) %collective-permute-start.5) | collective-permute-done | bytes 16416 | tf_op jit(solution)/shard_map/ppermute | solution.py:48
  18.0 0.5 %collective-permute-done.4.refs_8_ = f32[8,512]{1,0:T(8,128)S(1)} collective-permute-done((f32[8,512]{1,0:T(8,128)S(1)}, f32[8,512]{1,0:T(8,128)S(1)}, u32[]{:S(2)}, u32[]{:S(2)}) %collective-permute-start.4) | collective-permute-done | bytes 16416 | tf_op jit(solution)/shard_map/ppermute | solution.py:48
  18.6 1.2 %copy-done.1 = bf16[2048,256]{1,0:T(8,128)(2,1)S(1)} copy-done((bf16[2048,256]{1,0:T(8,128)(2,1)S(1)}, bf16[2048,256]{1,0:T(8,128)(2,1)}, u32[]{:S(2)}) %copy-start.1) | copy-done | bytes 1048600
  19.8 1.2 %copy-done.2 = bf16[2048,256]{1,0:T(8,128)(2,1)S(1)} copy-done((bf16[2048,256]{1,0:T(8,128)(2,1)S(1)}, bf16[2048,256]{1,0:T(8,128)(2,1)}, u32[]{:S(2)}) %copy-start.2) | copy-done | bytes 1048600
  21.0 1.2 %copy-done.3 = bf16[2048,256]{1,0:T(8,128)(2,1)S(1)} copy-done((bf16[2048,256]{1,0:T(8,128)(2,1)S(1)}, bf16[2048,256]{1,0:T(8,128)(2,1)}, u32[]{:S(2)}) %copy-start.3) | copy-done | bytes 1048600
  22.2 0.8 %copy-done.8 = bf16[16,2048]{1,0:T(8,128)(2,1)S(1)} copy-done((bf16[16,2048]{1,0:T(8,128)(2,1)S(1)}, bf16[16,2048]{1,0:T(8,128)(2,1)}, u32[]{:S(2)}) %copy-start.8) | copy-done | bytes 65560
  23.1 3.4 %shard_map.128 = (bf16[384,256]{1,0:T(8,128)(2,1)S(1)}, bf16[384,512]{1,0:T(8,128)(2,1)S(1)}, bf16[256,512]{1,0:T(8,128)(2,1)S(1)}, bf16[256,512]{1,0:T(8,128)(2...) custom-call(bf16[384,2048]{1,0:T(8,128)(2,1)S(1)} %copy-done, bf16[16,2048]{1,0:T(8,128)(2,1)S(1)} %copy-done.8, ...), custom_call_target="tpu_custom_call" | custom-call | tf_op jit(solution)/shard_map/pallas_call | solution.py:260
  26.6 0.7 %collective-permute-start.7 = (bf16[256,512]{1,0:T(8,128)(2,1)S(1)}, bf16[256,512]{1,0:T(8,128)(2,1)S(1)}, u32[]{:S(2)}, u32[]{:S(2)}) collective-permute-start(bf16[256,512]{1,0:T(8,128)(2,1)S(1)} %get-tuple-element.15), channel_id=1, source_target_pairs={{4,8},{8,4},{5,9},{9,5},{6,10},{10,6},{7,11},{11,7},{20,24},{24,20... | collective-permute-start | bytes 786440 | tf_op jit(solution)/shard_map/ppermute | solution.py:80
  27.3 3.4 %collective-permute-start.10 = (bf16[16,512]{1,0:T(8,128)(2,1)S(1)}, bf16[16,512]{1,0:T(8,128)(2,1)S(1)}, u32[]{:S(2)}, u32[]{:S(2)}) collective-permute-start(bf16[16,512]{1,0:T(8,128)(2,1)S(1)} %get-tuple-element.16.refs_5_), channel_id=1, source_target_pairs={{0,12},{4,8},{8,4},{12,0},{1,13},{5,9},{9,5},{13,1},{2,14},{6,10},... | collective-permute-start | bytes 49160 | tf_op jit(solution)/shard_map/ppermute | solution.py:48
  30.8 1.8 %collective-permute-start.9 = (bf16[16,512]{1,0:T(8,128)(2,1)S(1)}, bf16[16,512]{1,0:T(8,128)(2,1)S(1)}, u32[]{:S(2)}, u32[]{:S(2)}) collective-permute-start(bf16[16,512]{1,0:T(8,128)(2,1)S(1)} %get-tuple-element.16.refs_5_), channel_id=1, source_target_pairs={{0,8},{4,12},{8,0},{12,4},{1,9},{5,13},{9,1},{13,5},{2,10},{6,14},... | collective-permute-start | bytes 49160 | tf_op jit(solution)/shard_map/ppermute | solution.py:48
  32.6 0.1 pad_maximum_fusion.pairs_ref
  32.7 0.5 %shard_map.129.refs_4_ = f32[14,256,128]{2,1,0:T(8,128)S(1)} custom-call(f32[4,14,128]{2,1,0:T(8,128)S(1)} %pad_maximum_fusion.pairs_ref), custom_call_target="tpu_custom_call" | custom-call | tf_op jit(solution)/shard_map/pallas_call | solution.py:255
  33.3 4.1 %collective-permute-done.10.refs_8_ = bf16[16,512]{1,0:T(8,128)(2,1)S(1)} collective-permute-done((bf16[16,512]{1,0:T(8,128)(2,1)S(1)}, bf16[16,512]{1,0:T(8,128)(2,1)S(1)}, u32[]{:S(2)}, u32[]{:S(2)}) %collective-permute-start.10) | collective-permute-done | bytes 16416 | tf_op jit(solution)/shard_map/ppermute | solution.py:48
  37.4 2.3 %collective-permute-done.9.refs_7_ = bf16[16,512]{1,0:T(8,128)(2,1)S(1)} collective-permute-done((bf16[16,512]{1,0:T(8,128)(2,1)S(1)}, bf16[16,512]{1,0:T(8,128)(2,1)S(1)}, u32[]{:S(2)}, u32[]{:S(2)}) %collective-permute-start.9) | collective-permute-done | bytes 16416 | tf_op jit(solution)/shard_map/ppermute | solution.py:48
  39.6 2.0 %shard_map.130.refs_3_ = bf16[384,256]{1,0:T(8,128)(2,1)S(1)} custom-call(bf16[384,256]{1,0:T(8,128)(2,1)S(1)} %get-tuple-element.12.refs_0_, bf16[384,512]{1,0:T(8,128)(2,1)S(1)} %get-tuple-element.13.refs_1_, bf16[256,512]{1,0:T(8,128)(2,1)S(1)} %collective-permute-done.6.refs_2_, bf16[256,512]{1,0:T(8,128)(2,1)S(1)} %collective-permute-done.7.refs_3_, ...), custom_call_target="tpu_custom_call" | custom-call | tf_op jit(solution)/shard_map/pallas_call | solution.py:277
  41.6 0.6 %collective-permute-start.11 = (bf16[384,256]{1,0:T(8,128)(2,1)S(1)}, bf16[384,256]{1,0:T(8,128)(2,1)S(1)}, u32[]{:S(2)}, u32[]{:S(2)}) collective-permute-start(bf16[384,256]{1,0:T(8,128)(2,1)S(1)} %shard_map.130.refs_3_), channel_id=1, source_target_pairs={{0,2},{1,3},{2,0},{3,1},{4,6},{5,7},{6,4},{7,5},{8,10},{9,11},{10,... | collective-permute-start | bytes 589832 | tf_op jit(solution)/shard_map/ppermute | solution.py:48
  42.2 5.2 %collective-permute-done.11.refs_4_ = bf16[384,256]{1,0:T(8,128)(2,1)S(1)} collective-permute-done((bf16[384,256]{1,0:T(8,128)(2,1)S(1)}, bf16[384,256]{1,0:T(8,128)(2,1)S(1)}, u32[]{:S(2)}, u32[]{:S(2)}) %collective-permute-start.11) | collective-permute-done | bytes 196640 | tf_op jit(solution)/shard_map/ppermute | solution.py:48
  47.4 1.4 %collective-permute-done.13.refs_6_ = bf16[384,256]{1,0:T(8,128)(2,1)S(1)} collective-permute-done((bf16[384,256]{1,0:T(8,128)(2,1)S(1)}, bf16[384,256]{1,0:T(8,128)(2,1)S(1)}, u32[]{:S(2)}, u32[]{:S(2)}) %collective-permute-start.13) | collective-permute-done | bytes 196640 | tf_op jit(solution)/shard_map/ppermute | solution.py:48
  48.9 1.3 %shard_map.131 = bf16[384,512]{1,0:T(8,128)(2,1)} custom-call(bf16[384,512]{1,0:T(8,128)(2,1)S(1)} %get-tuple-element.11.refs_0_, f32[8,512]{1,0:T(8,128)S(1)} %add_add_fusion.refs_6_.refs_1_, bf16[1024,512]{1,0:T(8,128)(2,1)S(1)} %copy-done.4, bf16[384,256]{1,0:T(8,128)(2,1)S(1)} %shard_map.130.refs_3_, ...), custom_call_target="tpu_custom_call" | custom-call | tf_op jit(solution)/shard_map/pallas_call | solution.py:284
  (28 shorter events, 0.3 us)
Async XLA Ops:
  0.0 18.6 %copy-start = (bf16[384,2048]{1,0:T(8,128)(2,1)S(1)}, bf16[384,2048]{1,0:T(8,128)(2,1)}, u32[]{:S(2)}) copy-start(bf16[384,2048]{1,0:T(8,128)(2,1)} %refs_0_.1) | copy-start | bytes 4718596
  1.5 1.0 %copy-start.5 = (bf16[512,512]{1,0:T(8,128)(2,1)S(1)}, bf16[512,512]{1,0:T(8,128)(2,1)}, u32[]{:S(2)}) copy-start(bf16[512,512]{1,0:T(8,128)(2,1)} %w_shift_ref.1) | copy-start | bytes 1572868
  2.5 1.0 %copy-start.6 = (bf16[512,512]{1,0:T(8,128)(2,1)S(1)}, bf16[512,512]{1,0:T(8,128)(2,1)}, u32[]{:S(2)}) copy-start(bf16[512,512]{1,0:T(8,128)(2,1)} %w_scale_ref.1) | copy-start | bytes 1572868
  3.6 1.0 %copy-start.7 = (bf16[512,512]{1,0:T(8,128)(2,1)S(1)}, bf16[512,512]{1,0:T(8,128)(2,1)}, u32[]{:S(2)}) copy-start(bf16[512,512]{1,0:T(8,128)(2,1)} %w_gate_ref.1) | copy-start | bytes 1572868
  4.9 6.8 %collective-permute-start.2 = (f32[8,512]{1,0:T(8,128)S(1)}, f32[8,512]{1,0:T(8,128)S(1)}, u32[]{:S(2)}, u32[]{:S(2)}) collective-permute-start(f32[8,512]{1,0:T(8,128)S(1)} %shard_map.127), channel_id=1, source_target_pairs={{0,12},{4,8},{8,4},{12,0},{1,13},{5,9},{9,5},{13,1},{2,14},{6,10},... | collective-permute-start | bytes 49160 | tf_op jit(solution)/shard_map/ppermute | solution.py:48
  10.0 4.6 %collective-permute-start.1 = (f32[8,512]{1,0:T(8,128)S(1)}, f32[8,512]{1,0:T(8,128)S(1)}, u32[]{:S(2)}, u32[]{:S(2)}) collective-permute-start(f32[8,512]{1,0:T(8,128)S(1)} %shard_map.127), channel_id=1, source_target_pairs={{0,8},{4,12},{8,0},{12,4},{1,9},{5,13},{9,1},{13,5},{2,10},{6,14},... | collective-permute-start | bytes 49160 | tf_op jit(solution)/shard_map/ppermute | solution.py:48
  10.0 4.6 %collective-permute-start = (f32[8,512]{1,0:T(8,128)S(1)}, f32[8,512]{1,0:T(8,128)S(1)}, u32[]{:S(2)}, u32[]{:S(2)}) collective-permute-start(f32[8,512]{1,0:T(8,128)S(1)} %shard_map.127), channel_id=1, source_target_pairs={{0,4},{4,0},{8,12},{12,8},{1,5},{5,1},{9,13},{13,9},{2,6},{6,2},{1... | collective-permute-start | bytes 49160 | tf_op jit(solution)/shard_map/ppermute | solution.py:48
  14.7 3.4 %collective-permute-start.5 = (f32[8,512]{1,0:T(8,128)S(1)}, f32[8,512]{1,0:T(8,128)S(1)}, u32[]{:S(2)}, u32[]{:S(2)}) collective-permute-start(f32[8,512]{1,0:T(8,128)S(1)} %add_add_fusion.refs_6_.refs_1_), channel_id=1, source_target_pairs={{0,3},{1,2},{2,1},{3,0},{4,7},{5,6},{6,5},{7,4},{8,11},{9,10},{10,... | collective-permute-start | bytes 49160 | tf_op jit(solution)/shard_map/ppermute | solution.py:48
  14.7 3.8 %collective-permute-start.4 = (f32[8,512]{1,0:T(8,128)S(1)}, f32[8,512]{1,0:T(8,128)S(1)}, u32[]{:S(2)}, u32[]{:S(2)}) collective-permute-start(f32[8,512]{1,0:T(8,128)S(1)} %add_add_fusion.refs_6_.refs_1_), channel_id=1, source_target_pairs={{0,2},{1,3},{2,0},{3,1},{4,6},{5,7},{6,4},{7,5},{8,10},{9,11},{10,... | collective-permute-start | bytes 49160 | tf_op jit(solution)/shard_map/ppermute | solution.py:48
  16.3 2.3 %collective-permute-start.3 = (f32[8,512]{1,0:T(8,128)S(1)}, f32[8,512]{1,0:T(8,128)S(1)}, u32[]{:S(2)}, u32[]{:S(2)}) collective-permute-start(f32[8,512]{1,0:T(8,128)S(1)} %add_add_fusion.refs_6_.refs_1_), channel_id=1, source_target_pairs={{0,1},{1,0},{2,3},{3,2},{4,5},{5,4},{6,7},{7,6},{8,9},{9,8},{10,11... | collective-permute-start | bytes 49160 | tf_op jit(solution)/shard_map/ppermute | solution.py:48
  18.6 1.2 %copy-start.1 = (bf16[2048,256]{1,0:T(8,128)(2,1)S(1)}, bf16[2048,256]{1,0:T(8,128)(2,1)}, u32[]{:S(2)}) copy-start(bf16[2048,256]{1,0:T(8,128)(2,1)} %refs_3_.1) | copy-start | bytes 3145732
  19.8 1.2 %copy-start.2 = (bf16[2048,256]{1,0:T(8,128)(2,1)S(1)}, bf16[2048,256]{1,0:T(8,128)(2,1)}, u32[]{:S(2)}) copy-start(bf16[2048,256]{1,0:T(8,128)(2,1)} %refs_4_.1) | copy-start | bytes 3145732
  21.0 1.2 %copy-start.3 = (bf16[2048,256]{1,0:T(8,128)(2,1)S(1)}, bf16[2048,256]{1,0:T(8,128)(2,1)}, u32[]{:S(2)}) copy-start(bf16[2048,256]{1,0:T(8,128)(2,1)} %refs_5_.1) | copy-start | bytes 3145732
  22.2 0.8 %copy-start.8 = (bf16[16,2048]{1,0:T(8,128)(2,1)S(1)}, bf16[16,2048]{1,0:T(8,128)(2,1)}, u32[]{:S(2)}) copy-start(bf16[16,2048]{1,0:T(8,128)(2,1)} %refs_1_.1) | copy-start | bytes 196612
  23.1 4.2 %copy-start.9 = (f32[4,15,31]{2,0,1:T(4,128)S(1)}, f32[4,15,31]{2,0,1:T(4,128)}, u32[]{:S(2)}) copy-start(f32[4,15,31]{2,0,1:T(4,128)} %param.24) | copy-start | bytes 22324
  26.5 13.1 %collective-permute-start.6 = (bf16[256,512]{1,0:T(8,128)(2,1)S(1)}, bf16[256,512]{1,0:T(8,128)(2,1)S(1)}, u32[]{:S(2)}, u32[]{:S(2)}) collective-permute-start(bf16[256,512]{1,0:T(8,128)(2,1)S(1)} %get-tuple-element.14), channel_id=1, source_target_pairs={{0,4},{4,0},{8,12},{12,8},{1,5},{5,1},{9,13},{13,9},{2,6},{6,2},{1... | collective-permute-start | bytes 786440 | tf_op jit(solution)/shard_map/ppermute | solution.py:80
  26.6 13.1 %collective-permute-start.7 = (bf16[256,512]{1,0:T(8,128)(2,1)S(1)}, bf16[256,512]{1,0:T(8,128)(2,1)S(1)}, u32[]{:S(2)}, u32[]{:S(2)}) collective-permute-start(bf16[256,512]{1,0:T(8,128)(2,1)S(1)} %get-tuple-element.15), channel_id=1, source_target_pairs={{4,8},{8,4},{5,9},{9,5},{6,10},{10,6},{7,11},{11,7},{20,24},{24,20... | collective-permute-start | bytes 786440 | tf_op jit(solution)/shard_map/ppermute | solution.py:80
  27.3 10.0 %collective-permute-start.10 = (bf16[16,512]{1,0:T(8,128)(2,1)S(1)}, bf16[16,512]{1,0:T(8,128)(2,1)S(1)}, u32[]{:S(2)}, u32[]{:S(2)}) collective-permute-start(bf16[16,512]{1,0:T(8,128)(2,1)S(1)} %get-tuple-element.16.refs_5_), channel_id=1, source_target_pairs={{0,12},{4,8},{8,4},{12,0},{1,13},{5,9},{9,5},{13,1},{2,14},{6,10},... | collective-permute-start | bytes 49160 | tf_op jit(solution)/shard_map/ppermute | solution.py:48
  30.8 8.9 %collective-permute-start.9 = (bf16[16,512]{1,0:T(8,128)(2,1)S(1)}, bf16[16,512]{1,0:T(8,128)(2,1)S(1)}, u32[]{:S(2)}, u32[]{:S(2)}) collective-permute-start(bf16[16,512]{1,0:T(8,128)(2,1)S(1)} %get-tuple-element.16.refs_5_), channel_id=1, source_target_pairs={{0,8},{4,12},{8,0},{12,4},{1,9},{5,13},{9,1},{13,5},{2,10},{6,14},... | collective-permute-start | bytes 49160 | tf_op jit(solution)/shard_map/ppermute | solution.py:48
  32.6 7.0 %collective-permute-start.8 = (bf16[16,512]{1,0:T(8,128)(2,1)S(1)}, bf16[16,512]{1,0:T(8,128)(2,1)S(1)}, u32[]{:S(2)}, u32[]{:S(2)}) collective-permute-start(bf16[16,512]{1,0:T(8,128)(2,1)S(1)} %get-tuple-element.16.refs_5_), channel_id=1, source_target_pairs={{0,4},{4,0},{8,12},{12,8},{1,5},{5,1},{9,13},{13,9},{2,6},{6,2},{1... | collective-permute-start | bytes 49160 | tf_op jit(solution)/shard_map/ppermute | solution.py:48
  33.3 15.6 %copy-start.4 = (bf16[1024,512]{1,0:T(8,128)(2,1)S(1)}, bf16[1024,512]{1,0:T(8,128)(2,1)}, u32[]{:S(2)}) copy-start(bf16[1024,512]{1,0:T(8,128)(2,1)} %refs_2_.1) | copy-start | bytes 3145732
  41.6 5.8 %collective-permute-start.11 = (bf16[384,256]{1,0:T(8,128)(2,1)S(1)}, bf16[384,256]{1,0:T(8,128)(2,1)S(1)}, u32[]{:S(2)}, u32[]{:S(2)}) collective-permute-start(bf16[384,256]{1,0:T(8,128)(2,1)S(1)} %shard_map.130.refs_3_), channel_id=1, source_target_pairs={{0,2},{1,3},{2,0},{3,1},{4,6},{5,7},{6,4},{7,5},{8,10},{9,11},{10,... | collective-permute-start | bytes 589832 | tf_op jit(solution)/shard_map/ppermute | solution.py:48
  42.2 5.2 %collective-permute-start.12 = (bf16[384,256]{1,0:T(8,128)(2,1)S(1)}, bf16[384,256]{1,0:T(8,128)(2,1)S(1)}, u32[]{:S(2)}, u32[]{:S(2)}) collective-permute-start(bf16[384,256]{1,0:T(8,128)(2,1)S(1)} %shard_map.130.refs_3_), channel_id=1, source_target_pairs={{0,1},{1,0},{2,3},{3,2},{4,5},{5,4},{6,7},{7,6},{8,9},{9,8},{10,11... | collective-permute-start | bytes 589832 | tf_op jit(solution)/shard_map/ppermute | solution.py:48
  47.4 1.4 %collective-permute-start.13 = (bf16[384,256]{1,0:T(8,128)(2,1)S(1)}, bf16[384,256]{1,0:T(8,128)(2,1)S(1)}, u32[]{:S(2)}, u32[]{:S(2)}) collective-permute-start(bf16[384,256]{1,0:T(8,128)(2,1)S(1)} %collective-permute-done.11.refs_4_), channel_id=1, source_target_pairs={{0,1},{1,0},{2,3},{3,2},{4,5},{5,4},{6,7},{7,6},{8,9},{9,8},{10,11... | collective-permute-start | bytes 589832 | tf_op jit(solution)/shard_map/ppermute | solution.py:48

commit v2 on v1

--- a/solution.py
+++ b/solution.py
@@ -16,6 +16,8 @@
 MASKED = -1e30
 SHIFT, CTX_SHIFT, SCALE, CTX_SCALE, GATE, MOD_ROWS = 0, 1, 2, 3, 4, 8
 
+ANY = pl.BlockSpec(memory_space=pl.ANY)
+VMEM = pl.BlockSpec(memory_space=pltpu.VMEM)
 F32 = jnp.float32
 BF16 = jnp.bfloat16
 
@@ -84,13 +86,32 @@
     return v / (1.0 + jnp.exp(-v))
 
 
-def modulation_kernel(cond_ref, ctx_ref, w_shift_ref, w_scale_ref, w_gate_ref, out_ref):
-    row = lax.broadcasted_iota(jnp.int32, (MOD_ROWS, cond_ref.shape[1]), 0)
-    cond = silu(cond_ref[...].astype(F32))
-    ctx = silu(ctx_ref[...].astype(F32))
+def fetch(pairs, sems):
+    copies = [
+        pltpu.make_async_copy(source, target, sems.at[i]) for i, (source, target) in enumerate(pairs)
+    ]
+    for copy in copies:
+        copy.start()
+    return copies
+
+
+def modulation_kernel(
+    cond_hbm, ctx_hbm, w_shift_hbm, w_scale_hbm, w_gate_hbm, out_ref, *scratch
+):
+    cond_ref, ctx_ref, w_shift_ref, w_scale_ref, w_gate_ref, sems = scratch
+    sources = (cond_hbm, ctx_hbm, w_shift_hbm, w_scale_hbm, w_gate_hbm)
+    copies = fetch(list(zip(sources, scratch[:-1])), sems)
+    copies[0].wait()
+    copies[1].wait()
+    cond = silu(cond_ref[...].astype(F32)).reshape(1, -1)
+    ctx = silu(ctx_ref[...].astype(F32)).reshape(1, -1)
+    row = lax.broadcasted_iota(jnp.int32, (MOD_ROWS, cond.shape[1]), 0)
     acts = jnp.where(row % 2 == 0, cond, ctx).astype(BF16)
+    copies[2].wait()
     shifts = jnp.dot(acts, w_shift_ref[...], preferred_element_type=F32)
+    copies[3].wait()
     scales = jnp.dot(acts, w_scale_ref[...], preferred_element_type=F32)
+    copies[4].wait()
     gates = jnp.dot(acts, w_gate_ref[...], preferred_element_type=F32)
     out_row = lax.broadcasted_iota(jnp.int32, out_ref.shape, 0)
     out_ref[...] = jnp.where(out_row < SCALE, shifts, jnp.where(out_row < GATE, scales, gates))
@@ -115,10 +136,13 @@
 
 
 def project_kernel(*refs, tp_count, sp_axis, tp_axis):
-    latent_ref, context_ref, gain_ref, wq_ref, wk_ref, wv_ref = refs[:6]
+    latent_ref, gain_ref = refs[:2]
+    sources = refs[2:6]
     piece_refs = refs[6 : 6 + tp_count]
-    q_ref, kv_ref, send_a_ref, send_b_ref, ctx_ref, resid_ref = refs[6 + tp_count : -2]
-    mod_ref, normed_ref = refs[-2:]
+    q_ref, kv_ref, send_a_ref, send_b_ref, ctx_ref, resid_ref = refs[6 + tp_count : -7]
+    mod_ref, normed_ref = refs[-7:-5]
+    context_ref, wk_ref, wv_ref, wq_ref, sems = refs[-5:]
+    copies = fetch(list(zip(sources, refs[-5:-1])), sems)
     tokens, _ = latent_ref.shape
     cols = piece_refs[0].shape[1]
     width = wq_ref.shape[1]
@@ -143,14 +167,18 @@
         return carry
 
     lax.fori_loop(0, tokens // step, body, 0, unroll=2)
+    copies[0].wait()
     ctx_normed = norm(context_ref[...], CTX_SCALE, CTX_SHIFT)
     normed = normed_ref[...]
+    copies[1].wait()
     kv_ref[:, :width] = jnp.dot(normed, wk_ref[...], preferred_element_type=F32).astype(BF16)
+    copies[2].wait()
     kv_ref[:, width:] = jnp.dot(normed, wv_ref[...], preferred_element_type=F32).astype(BF16)
     halo = HALO * GRID_W
     last = tokens - halo
     send_a_ref[...] = kv_ref[pl.ds(pl.multiple_of((1 - odd) * last, 64), halo), :]
     send_b_ref[...] = kv_ref[pl.ds(pl.multiple_of(odd * last, 64), halo), :]
+    copies[3].wait()
     query = jnp.dot(normed, wq_ref[...], preferred_element_type=F32).astype(BF16)
     q_ref[...] = query * BF16(HEAD_DIM**-0.5)
     ctx_ref[:, :width] = jnp.dot(ctx_normed, wk_ref[...], preferred_element_type=F32).astype(BF16)
@@ -243,9 +271,13 @@
     sp_count, tp_count = lax.axis_size("sp"), lax.axis_size("tp")
     halo = HALO * GRID_W
 
-    partial = call(modulation_kernel, shape_of((MOD_ROWS, cols), F32))(
-        conditioning[None], ctx_vector[None], w_shift, w_scale, w_gate
-    )
+    mod_inputs = (conditioning, ctx_vector, w_shift, w_scale, w_gate)
+    partial = call(
+        modulation_kernel,
+        shape_of((MOD_ROWS, cols), F32),
+        scratch=[pltpu.VMEM(a.shape, a.dtype) for a in mod_inputs] + [pltpu.SemaphoreType.DMA((5,))],
+        in_specs=[ANY] * 5,
+    )(*mod_inputs)
     mod_own = total(partial, "sp")
     mod_pieces = pieces_of(mod_own, "tp")
 
@@ -257,6 +289,7 @@
         shape_of((2 * WIN_H - 2, heads * GRID_W, 2 * GRID_W), F32),
     )(pairs)
 
+    fetched = (context, w_key, w_value, w_query)
     query, key_value, send_a, send_b, ctx_own, resid = call(
         functools.partial(project_kernel, tp_count=tp_count, sp_axis="sp", tp_axis="tp"),
         (
@@ -267,8 +300,11 @@
             shape_of((context.shape[0], 2 * width), BF16),
             shape_of((tokens, cols), BF16),
         ),
-        scratch=(pltpu.VMEM((MOD_ROWS, model), F32), pltpu.VMEM((tokens, model), BF16)),
-    )(latent, context, norm_gain[None], w_query, w_key, w_value, *mod_pieces)
+        scratch=[pltpu.VMEM((MOD_ROWS, model), F32), pltpu.VMEM((tokens, model), BF16)]
+        + [pltpu.VMEM(a.shape, a.dtype) for a in fetched]
+        + [pltpu.SemaphoreType.DMA((4,))],
+        in_specs=[VMEM] * 2 + [ANY] * 4 + [VMEM] * tp_count,
+    )(latent, norm_gain[None], *fetched, *mod_pieces)
 
     recv_a = pairwise(send_a, "sp", 0)
     recv_b = pairwise(send_b, "sp", 1)

time: 50.7 us -> 52.6 us (1.037)
  Pallas kernels: 7.51 us -> 9.45 us
    broadcast_in_dim x2 -> x0, local copies, waits for them, and re-layouts: 1.48 us -> none  [the longest x1 0.8 us: local(): conditioning[None]]
    unnamed x21 -> x25, local copies, waits for them, and re-layouts: 7.65 us -> 9.13 us
    pallas_call x1, Pallas kernels: 3.43 us -> 4.9 us  [local(): call(functools.partial(project_kernel, tp_count=tp_count, sp_axis='sp', t...]
where the time goes in v2:
time: 52.6 us; the launch traced here: 52.1 us
  waiting for transfers between devices  18.2 us (35%)
  starting transfers between devices  14.4 us (27%)
  local copies, waits for them, and re-layouts  9.83 us (19%)
  Pallas kernels  9.45 us (18%)
    ppermute x12, waiting for transfers between devices, peer(): return lax.ppermute(block, axis, [(i, i ^ mask) for i in range(count)])  18.2 us
    ppermute x12, starting transfers between devices, peer(): return lax.ppermute(block, axis, [(i, i ^ mask) for i in range(count)])  13.7 us
    unnamed x25, local copies, waits for them, and re-layouts  9.13 us
    pallas_call x1, Pallas kernels, local(): call(functools.partial(project_kernel, tp_count=tp_count, sp_axis='sp', t...  4.9 us
    pallas_call x1, Pallas kernels, local(): call(functools.partial(attention_kernel, sp_axis='sp', sp_count=sp_count)...  1.96 us
    pallas_call x1, Pallas kernels, local(): call(functools.partial(output_kernel, masks=[mask for mask, _ in gathered...  1.32 us
  transfers between devices with their start and end apart: 14, of which 8 were waited for; matrix products, arithmetic and copies ran while one was open for 2% of the time, Pallas kernels for 1%

profile of v2, /device:TPU:0, one launch (start us, length us, event | category | flops | bytes accessed | tf_op | source)
XLA Modules:
  0.0 52.1 jit_solution(1437484731632785918)
XLA Ops:
  0.0 1.2 %copy-done.5 = bf16[512,512]{1,0:T(8,128)(2,1)S(1)} copy-done((bf16[512,512]{1,0:T(8,128)(2,1)S(1)}, bf16[512,512]{1,0:T(8,128)(2,1)}, u32[]{:S(2)}) %copy-start.5) | copy-done | bytes 524312
  1.2 1.0 %copy-done.6 = bf16[512,512]{1,0:T(8,128)(2,1)S(1)} copy-done((bf16[512,512]{1,0:T(8,128)(2,1)S(1)}, bf16[512,512]{1,0:T(8,128)(2,1)}, u32[]{:S(2)}) %copy-start.6) | copy-done | bytes 524312
  2.2 1.0 %copy-done.7 = bf16[512,512]{1,0:T(8,128)(2,1)S(1)} copy-done((bf16[512,512]{1,0:T(8,128)(2,1)S(1)}, bf16[512,512]{1,0:T(8,128)(2,1)}, u32[]{:S(2)}) %copy-start.7) | copy-done | bytes 524312
  3.3 0.7 %copy-done.9 = bf16[512]{0:T(512)(128)(2,1)S(1)} copy-done((bf16[512]{0:T(512)(128)(2,1)S(1)}, bf16[512]{0:T(512)(128)(2,1)}, u32[]{:S(2)}) %copy-start.9) | copy-done | bytes 1048
  3.9 0.7 %copy-done.10 = bf16[512]{0:T(512)(128)(2,1)S(1)} copy-done((bf16[512]{0:T(512)(128)(2,1)S(1)}, bf16[512]{0:T(512)(128)(2,1)}, u32[]{:S(2)}) %copy-start.10) | copy-done | bytes 1048
  4.6 0.7 %shard_map.127 = f32[8,512]{1,0:T(8,128)S(1)} custom-call(bf16[512]{0:T(512)(128)(2,1)S(1)} %copy-done.9, bf16[512]{0:T(512)(128)(2,1)S(1)} %copy-done.10, bf16[512,512]{1,0:T(8,128)(2,1)S(1)} %copy-done.5, bf16[512,512]{1,0:T(8,128)(2,1)S(1)} %copy-done.6, bf16[512,512]{1,0:T(8,128)(2,1)S(1)} %copy-done.7), custom_call_target="tpu_custom_call" | custom-call | tf_op jit(solution)/shard_map/pallas_call | solution.py:275
  5.3 5.1 %collective-permute-start.2 = (f32[8,512]{1,0:T(8,128)S(1)}, f32[8,512]{1,0:T(8,128)S(1)}, u32[]{:S(2)}, u32[]{:S(2)}) collective-permute-start(f32[8,512]{1,0:T(8,128)S(1)} %shard_map.127), channel_id=1, source_target_pairs={{0,12},{4,8},{8,4},{12,0},{1,13},{5,9},{9,5},{13,1},{2,14},{6,10},... | collective-permute-start | bytes 49160 | tf_op jit(solution)/shard_map/ppermute | solution.py:50
  10.5 0.6 %collective-permute-start = (f32[8,512]{1,0:T(8,128)S(1)}, f32[8,512]{1,0:T(8,128)S(1)}, u32[]{:S(2)}, u32[]{:S(2)}) collective-permute-start(f32[8,512]{1,0:T(8,128)S(1)} %shard_map.127), channel_id=1, source_target_pairs={{0,4},{4,0},{8,12},{12,8},{1,5},{5,1},{9,13},{13,9},{2,6},{6,2},{1... | collective-permute-start | bytes 49160 | tf_op jit(solution)/shard_map/ppermute | solution.py:50
  11.1 1.1 %collective-permute-done.2 = f32[8,512]{1,0:T(8,128)S(1)} collective-permute-done((f32[8,512]{1,0:T(8,128)S(1)}, f32[8,512]{1,0:T(8,128)S(1)}, u32[]{:S(2)}, u32[]{:S(2)}) %collective-permute-start.2) | collective-permute-done | bytes 16416 | tf_op jit(solution)/shard_map/ppermute | solution.py:50
  12.2 2.9 %collective-permute-done.1 = f32[8,512]{1,0:T(8,128)S(1)} collective-permute-done((f32[8,512]{1,0:T(8,128)S(1)}, f32[8,512]{1,0:T(8,128)S(1)}, u32[]{:S(2)}, u32[]{:S(2)}) %collective-permute-start.1) | collective-permute-done | bytes 16416 | tf_op jit(solution)/shard_map/ppermute | solution.py:50
  15.2 1.6 %collective-permute-start.4 = (f32[8,512]{1,0:T(8,128)S(1)}, f32[8,512]{1,0:T(8,128)S(1)}, u32[]{:S(2)}, u32[]{:S(2)}) collective-permute-start(f32[8,512]{1,0:T(8,128)S(1)} %add_add_fusion.refs_6_.refs_1_), channel_id=1, source_target_pairs={{0,2},{1,3},{2,0},{3,1},{4,6},{5,7},{6,4},{7,5},{8,10},{9,11},{10,... | collective-permute-start | bytes 49160 | tf_op jit(solution)/shard_map/ppermute | solution.py:50
  16.8 0.3 collective-permute-start.3
  17.1 0.7 %broadcast_in_dim.3.refs_1_ = bf16[1,2048]{1,0:T(2,128)(2,1)S(1)} reshape(bf16[2048]{0:T(1024)(128)(2,1)} %param.20) | data formatting | bytes 8192 | tf_op jit(solution)/shard_map/broadcast_in_dim | solution.py:307
  17.8 0.7 %collective-permute-done.5.refs_9_ = f32[8,512]{1,0:T(8,128)S(1)} collective-permute-done((f32[8,512]{1,0:T(8,128)S(1)}, f32[8,512]{1,0:T(8,128)S(1)}, u32[]{:S(2)}, u32[]{:S(2)}) %collective-permute-start.5) | collective-permute-done | bytes 16416 | tf_op jit(solution)/shard_map/ppermute | solution.py:50
  18.5 0.5 %collective-permute-done.4.refs_8_ = f32[8,512]{1,0:T(8,128)S(1)} collective-permute-done((f32[8,512]{1,0:T(8,128)S(1)}, f32[8,512]{1,0:T(8,128)S(1)}, u32[]{:S(2)}, u32[]{:S(2)}) %collective-permute-start.4) | collective-permute-done | bytes 16416 | tf_op jit(solution)/shard_map/ppermute | solution.py:50
  19.0 1.2 %copy-done.1 = bf16[2048,256]{1,0:T(8,128)(2,1)S(1)} copy-done((bf16[2048,256]{1,0:T(8,128)(2,1)S(1)}, bf16[2048,256]{1,0:T(8,128)(2,1)}, u32[]{:S(2)}) %copy-start.1) | copy-done | bytes 1048600
  20.3 1.2 %copy-done.2 = bf16[2048,256]{1,0:T(8,128)(2,1)S(1)} copy-done((bf16[2048,256]{1,0:T(8,128)(2,1)S(1)}, bf16[2048,256]{1,0:T(8,128)(2,1)}, u32[]{:S(2)}) %copy-start.2) | copy-done | bytes 1048600
  21.5 1.2 %copy-done.3 = bf16[2048,256]{1,0:T(8,128)(2,1)S(1)} copy-done((bf16[2048,256]{1,0:T(8,128)(2,1)S(1)}, bf16[2048,256]{1,0:T(8,128)(2,1)}, u32[]{:S(2)}) %copy-start.3) | copy-done | bytes 1048600
  22.7 0.8 %copy-done.8 = bf16[16,2048]{1,0:T(8,128)(2,1)S(1)} copy-done((bf16[16,2048]{1,0:T(8,128)(2,1)S(1)}, bf16[16,2048]{1,0:T(8,128)(2,1)}, u32[]{:S(2)}) %copy-start.8) | copy-done | bytes 65560
  23.6 4.9 %shard_map.128 = (bf16[384,256]{1,0:T(8,128)(2,1)S(1)}, bf16[384,512]{1,0:T(8,128)(2,1)S(1)}, bf16[256,512]{1,0:T(8,128)(2,1)S(1)}, bf16[256,512]{1,0:T(8,128)(2...) custom-call(bf16[384,2048]{1,0:T(8,128)(2,1)S(1)} %copy-done, ...), custom_call_target="tpu_custom_call" | custom-call | tf_op jit(solution)/shard_map/pallas_call | solution.py:293
  28.5 0.7 %collective-permute-start.7 = (bf16[256,512]{1,0:T(8,128)(2,1)S(1)}, bf16[256,512]{1,0:T(8,128)(2,1)S(1)}, u32[]{:S(2)}, u32[]{:S(2)}) collective-permute-start(bf16[256,512]{1,0:T(8,128)(2,1)S(1)} %get-tuple-element.15), channel_id=1, source_target_pairs={{4,8},{8,4},{5,9},{9,5},{6,10},{10,6},{7,11},{11,7},{20,24},{24,20... | collective-permute-start | bytes 786440 | tf_op jit(solution)/shard_map/ppermute | solution.py:82
  29.3 3.5 %collective-permute-start.10 = (bf16[16,512]{1,0:T(8,128)(2,1)S(1)}, bf16[16,512]{1,0:T(8,128)(2,1)S(1)}, u32[]{:S(2)}, u32[]{:S(2)}) collective-permute-start(bf16[16,512]{1,0:T(8,128)(2,1)S(1)} %get-tuple-element.16.refs_5_), channel_id=1, source_target_pairs={{0,12},{4,8},{8,4},{12,0},{1,13},{5,9},{9,5},{13,1},{2,14},{6,10},... | collective-permute-start | bytes 49160 | tf_op jit(solution)/shard_map/ppermute | solution.py:50
  32.7 1.8 %collective-permute-start.9 = (bf16[16,512]{1,0:T(8,128)(2,1)S(1)}, bf16[16,512]{1,0:T(8,128)(2,1)S(1)}, u32[]{:S(2)}, u32[]{:S(2)}) collective-permute-start(bf16[16,512]{1,0:T(8,128)(2,1)S(1)} %get-tuple-element.16.refs_5_), channel_id=1, source_target_pairs={{0,8},{4,12},{8,0},{12,4},{1,9},{5,13},{9,1},{13,5},{2,10},{6,14},... | collective-permute-start | bytes 49160 | tf_op jit(solution)/shard_map/ppermute | solution.py:50
  34.6 0.1 pad_maximum_fusion.pairs_ref
  34.7 0.5 %shard_map.129.refs_4_ = f32[14,256,128]{2,1,0:T(8,128)S(1)} custom-call(f32[4,14,128]{2,1,0:T(8,128)S(1)} %pad_maximum_fusion.pairs_ref), custom_call_target="tpu_custom_call" | custom-call | tf_op jit(solution)/shard_map/pallas_call | solution.py:287
  35.2 4.1 %collective-permute-done.10.refs_8_ = bf16[16,512]{1,0:T(8,128)(2,1)S(1)} collective-permute-done((bf16[16,512]{1,0:T(8,128)(2,1)S(1)}, bf16[16,512]{1,0:T(8,128)(2,1)S(1)}, u32[]{:S(2)}, u32[]{:S(2)}) %collective-permute-start.10) | collective-permute-done | bytes 16416 | tf_op jit(solution)/shard_map/ppermute | solution.py:50
  39.3 2.3 %collective-permute-done.9.refs_7_ = bf16[16,512]{1,0:T(8,128)(2,1)S(1)} collective-permute-done((bf16[16,512]{1,0:T(8,128)(2,1)S(1)}, bf16[16,512]{1,0:T(8,128)(2,1)S(1)}, u32[]{:S(2)}, u32[]{:S(2)}) %collective-permute-start.9) | collective-permute-done | bytes 16416 | tf_op jit(solution)/shard_map/ppermute | solution.py:50
  41.6 2.0 %shard_map.130.refs_3_ = bf16[384,256]{1,0:T(8,128)(2,1)S(1)} custom-call(bf16[384,256]{1,0:T(8,128)(2,1)S(1)} %get-tuple-element.12.refs_0_, bf16[384,512]{1,0:T(8,128)(2,1)S(1)} %get-tuple-element.13.refs_1_, bf16[256,512]{1,0:T(8,128)(2,1)S(1)} %collective-permute-done.6.refs_2_, bf16[256,512]{1,0:T(8,128)(2,1)S(1)} %collective-permute-done.7.refs_3_, ...), custom_call_target="tpu_custom_call" | custom-call | tf_op jit(solution)/shard_map/pallas_call | solution.py:313
  43.6 0.6 %collective-permute-start.11 = (bf16[384,256]{1,0:T(8,128)(2,1)S(1)}, bf16[384,256]{1,0:T(8,128)(2,1)S(1)}, u32[]{:S(2)}, u32[]{:S(2)}) collective-permute-start(bf16[384,256]{1,0:T(8,128)(2,1)S(1)} %shard_map.130.refs_3_), channel_id=1, source_target_pairs={{0,2},{1,3},{2,0},{3,1},{4,6},{5,7},{6,4},{7,5},{8,10},{9,11},{10,... | collective-permute-start | bytes 589832 | tf_op jit(solution)/shard_map/ppermute | solution.py:50
  44.2 5.2 %collective-permute-done.11.refs_4_ = bf16[384,256]{1,0:T(8,128)(2,1)S(1)} collective-permute-done((bf16[384,256]{1,0:T(8,128)(2,1)S(1)}, bf16[384,256]{1,0:T(8,128)(2,1)S(1)}, u32[]{:S(2)}, u32[]{:S(2)}) %collective-permute-start.11) | collective-permute-done | bytes 196640 | tf_op jit(solution)/shard_map/ppermute | solution.py:50
  49.4 1.4 %collective-permute-done.13.refs_6_ = bf16[384,256]{1,0:T(8,128)(2,1)S(1)} collective-permute-done((bf16[384,256]{1,0:T(8,128)(2,1)S(1)}, bf16[384,256]{1,0:T(8,128)(2,1)S(1)}, u32[]{:S(2)}, u32[]{:S(2)}) %collective-permute-start.13) | collective-permute-done | bytes 196640 | tf_op jit(solution)/shard_map/ppermute | solution.py:50
  50.8 1.3 %shard_map.131 = bf16[384,512]{1,0:T(8,128)(2,1)} custom-call(bf16[384,512]{1,0:T(8,128)(2,1)S(1)} %get-tuple-element.11.refs_0_, f32[8,512]{1,0:T(8,128)S(1)} %add_add_fusion.refs_6_.refs_1_, bf16[1024,512]{1,0:T(8,128)(2,1)S(1)} %copy-done.4, bf16[384,256]{1,0:T(8,128)(2,1)S(1)} %shard_map.130.refs_3_, ...), custom_call_target="tpu_custom_call" | custom-call | tf_op jit(solution)/shard_map/pallas_call | solution.py:320
  (30 shorter events, 0.3 us)
Async XLA Ops:
  0.0 19.0 %copy-start = (bf16[384,2048]{1,0:T(8,128)(2,1)S(1)}, bf16[384,2048]{1,0:T(8,128)(2,1)}, u32[]{:S(2)}) copy-start(bf16[384,2048]{1,0:T(8,128)(2,1)} %refs_0_.1) | copy-start | bytes 4718596
  0.0 1.2 %copy-start.5 = (bf16[512,512]{1,0:T(8,128)(2,1)S(1)}, bf16[512,512]{1,0:T(8,128)(2,1)}, u32[]{:S(2)}) copy-start(bf16[512,512]{1,0:T(8,128)(2,1)} %w_shift_hbm.1) | copy-start | bytes 1572868
  1.2 1.0 %copy-start.6 = (bf16[512,512]{1,0:T(8,128)(2,1)S(1)}, bf16[512,512]{1,0:T(8,128)(2,1)}, u32[]{:S(2)}) copy-start(bf16[512,512]{1,0:T(8,128)(2,1)} %w_scale_hbm.1) | copy-start | bytes 1572868
  2.2 1.0 %copy-start.7 = (bf16[512,512]{1,0:T(8,128)(2,1)S(1)}, bf16[512,512]{1,0:T(8,128)(2,1)}, u32[]{:S(2)}) copy-start(bf16[512,512]{1,0:T(8,128)(2,1)} %w_gate_hbm.1) | copy-start | bytes 1572868
  3.2 0.7 %copy-start.9 = (bf16[512]{0:T(512)(128)(2,1)S(1)}, bf16[512]{0:T(512)(128)(2,1)}, u32[]{:S(2)}) copy-start(bf16[512]{0:T(512)(128)(2,1)} %cond_hbm.1) | copy-start | bytes 3076
  3.9 0.7 %copy-start.10 = (bf16[512]{0:T(512)(128)(2,1)S(1)}, bf16[512]{0:T(512)(128)(2,1)}, u32[]{:S(2)}) copy-start(bf16[512]{0:T(512)(128)(2,1)} %ctx_hbm.1) | copy-start | bytes 3076
  5.3 6.9 %collective-permute-start.2 = (f32[8,512]{1,0:T(8,128)S(1)}, f32[8,512]{1,0:T(8,128)S(1)}, u32[]{:S(2)}, u32[]{:S(2)}) collective-permute-start(f32[8,512]{1,0:T(8,128)S(1)} %shard_map.127), channel_id=1, source_target_pairs={{0,12},{4,8},{8,4},{12,0},{1,13},{5,9},{9,5},{13,1},{2,14},{6,10},... | collective-permute-start | bytes 49160 | tf_op jit(solution)/shard_map/ppermute | solution.py:50
  10.5 4.6 %collective-permute-start.1 = (f32[8,512]{1,0:T(8,128)S(1)}, f32[8,512]{1,0:T(8,128)S(1)}, u32[]{:S(2)}, u32[]{:S(2)}) collective-permute-start(f32[8,512]{1,0:T(8,128)S(1)} %shard_map.127), channel_id=1, source_target_pairs={{0,8},{4,12},{8,0},{12,4},{1,9},{5,13},{9,1},{13,5},{2,10},{6,14},... | collective-permute-start | bytes 49160 | tf_op jit(solution)/shard_map/ppermute | solution.py:50
  10.5 4.6 %collective-permute-start = (f32[8,512]{1,0:T(8,128)S(1)}, f32[8,512]{1,0:T(8,128)S(1)}, u32[]{:S(2)}, u32[]{:S(2)}) collective-permute-start(f32[8,512]{1,0:T(8,128)S(1)} %shard_map.127), channel_id=1, source_target_pairs={{0,4},{4,0},{8,12},{12,8},{1,5},{5,1},{9,13},{13,9},{2,6},{6,2},{1... | collective-permute-start | bytes 49160 | tf_op jit(solution)/shard_map/ppermute | solution.py:50
  15.1 3.4 %collective-permute-start.5 = (f32[8,512]{1,0:T(8,128)S(1)}, f32[8,512]{1,0:T(8,128)S(1)}, u32[]{:S(2)}, u32[]{:S(2)}) collective-permute-start(f32[8,512]{1,0:T(8,128)S(1)} %add_add_fusion.refs_6_.refs_1_), channel_id=1, source_target_pairs={{0,3},{1,2},{2,1},{3,0},{4,7},{5,6},{6,5},{7,4},{8,11},{9,10},{10,... | collective-permute-start | bytes 49160 | tf_op jit(solution)/shard_map/ppermute | solution.py:50
  15.2 3.8 %collective-permute-start.4 = (f32[8,512]{1,0:T(8,128)S(1)}, f32[8,512]{1,0:T(8,128)S(1)}, u32[]{:S(2)}, u32[]{:S(2)}) collective-permute-start(f32[8,512]{1,0:T(8,128)S(1)} %add_add_fusion.refs_6_.refs_1_), channel_id=1, source_target_pairs={{0,2},{1,3},{2,0},{3,1},{4,6},{5,7},{6,4},{7,5},{8,10},{9,11},{10,... | collective-permute-start | bytes 49160 | tf_op jit(solution)/shard_map/ppermute | solution.py:50
  16.8 2.3 %collective-permute-start.3 = (f32[8,512]{1,0:T(8,128)S(1)}, f32[8,512]{1,0:T(8,128)S(1)}, u32[]{:S(2)}, u32[]{:S(2)}) collective-permute-start(f32[8,512]{1,0:T(8,128)S(1)} %add_add_fusion.refs_6_.refs_1_), channel_id=1, source_target_pairs={{0,1},{1,0},{2,3},{3,2},{4,5},{5,4},{6,7},{7,6},{8,9},{9,8},{10,11... | collective-permute-start | bytes 49160 | tf_op jit(solution)/shard_map/ppermute | solution.py:50
  19.0 1.2 %copy-start.1 = (bf16[2048,256]{1,0:T(8,128)(2,1)S(1)}, bf16[2048,256]{1,0:T(8,128)(2,1)}, u32[]{:S(2)}) copy-start(bf16[2048,256]{1,0:T(8,128)(2,1)} %refs_3_.1) | copy-start | bytes 3145732
  20.3 1.2 %copy-start.2 = (bf16[2048,256]{1,0:T(8,128)(2,1)S(1)}, bf16[2048,256]{1,0:T(8,128)(2,1)}, u32[]{:S(2)}) copy-start(bf16[2048,256]{1,0:T(8,128)(2,1)} %refs_4_.1) | copy-start | bytes 3145732
  21.5 1.2 %copy-start.3 = (bf16[2048,256]{1,0:T(8,128)(2,1)S(1)}, bf16[2048,256]{1,0:T(8,128)(2,1)}, u32[]{:S(2)}) copy-start(bf16[2048,256]{1,0:T(8,128)(2,1)} %refs_5_.1) | copy-start | bytes 3145732
  22.7 0.8 %copy-start.8 = (bf16[16,2048]{1,0:T(8,128)(2,1)S(1)}, bf16[16,2048]{1,0:T(8,128)(2,1)}, u32[]{:S(2)}) copy-start(bf16[16,2048]{1,0:T(8,128)(2,1)} %refs_2_.2) | copy-start | bytes 196612
  23.6 5.7 %copy-start.11 = (f32[4,15,31]{2,0,1:T(4,128)S(1)}, f32[4,15,31]{2,0,1:T(4,128)}, u32[]{:S(2)}) copy-start(f32[4,15,31]{2,0,1:T(4,128)} %param.24) | copy-start | bytes 22324
  28.5 13.1 %collective-permute-start.6 = (bf16[256,512]{1,0:T(8,128)(2,1)S(1)}, bf16[256,512]{1,0:T(8,128)(2,1)S(1)}, u32[]{:S(2)}, u32[]{:S(2)}) collective-permute-start(bf16[256,512]{1,0:T(8,128)(2,1)S(1)} %get-tuple-element.14), channel_id=1, source_target_pairs={{0,4},{4,0},{8,12},{12,8},{1,5},{5,1},{9,13},{13,9},{2,6},{6,2},{1... | collective-permute-start | bytes 786440 | tf_op jit(solution)/shard_map/ppermute | solution.py:82
  28.5 13.1 %collective-permute-start.7 = (bf16[256,512]{1,0:T(8,128)(2,1)S(1)}, bf16[256,512]{1,0:T(8,128)(2,1)S(1)}, u32[]{:S(2)}, u32[]{:S(2)}) collective-permute-start(bf16[256,512]{1,0:T(8,128)(2,1)S(1)} %get-tuple-element.15), channel_id=1, source_target_pairs={{4,8},{8,4},{5,9},{9,5},{6,10},{10,6},{7,11},{11,7},{20,24},{24,20... | collective-permute-start | bytes 786440 | tf_op jit(solution)/shard_map/ppermute | solution.py:82
  29.3 10.0 %collective-permute-start.10 = (bf16[16,512]{1,0:T(8,128)(2,1)S(1)}, bf16[16,512]{1,0:T(8,128)(2,1)S(1)}, u32[]{:S(2)}, u32[]{:S(2)}) collective-permute-start(bf16[16,512]{1,0:T(8,128)(2,1)S(1)} %get-tuple-element.16.refs_5_), channel_id=1, source_target_pairs={{0,12},{4,8},{8,4},{12,0},{1,13},{5,9},{9,5},{13,1},{2,14},{6,10},... | collective-permute-start | bytes 49160 | tf_op jit(solution)/shard_map/ppermute | solution.py:50
  32.7 8.9 %collective-permute-start.9 = (bf16[16,512]{1,0:T(8,128)(2,1)S(1)}, bf16[16,512]{1,0:T(8,128)(2,1)S(1)}, u32[]{:S(2)}, u32[]{:S(2)}) collective-permute-start(bf16[16,512]{1,0:T(8,128)(2,1)S(1)} %get-tuple-element.16.refs_5_), channel_id=1, source_target_pairs={{0,8},{4,12},{8,0},{12,4},{1,9},{5,13},{9,1},{13,5},{2,10},{6,14},... | collective-permute-start | bytes 49160 | tf_op jit(solution)/shard_map/ppermute | solution.py:50
  34.5 7.0 %collective-permute-start.8 = (bf16[16,512]{1,0:T(8,128)(2,1)S(1)}, bf16[16,512]{1,0:T(8,128)(2,1)S(1)}, u32[]{:S(2)}, u32[]{:S(2)}) collective-permute-start(bf16[16,512]{1,0:T(8,128)(2,1)S(1)} %get-tuple-element.16.refs_5_), channel_id=1, source_target_pairs={{0,4},{4,0},{8,12},{12,8},{1,5},{5,1},{9,13},{13,9},{2,6},{6,2},{1... | collective-permute-start | bytes 49160 | tf_op jit(solution)/shard_map/ppermute | solution.py:50
  35.2 15.6 %copy-start.4 = (bf16[1024,512]{1,0:T(8,128)(2,1)S(1)}, bf16[1024,512]{1,0:T(8,128)(2,1)}, u32[]{:S(2)}) copy-start(bf16[1024,512]{1,0:T(8,128)(2,1)} %refs_2_.3) | copy-start | bytes 3145732
  43.6 5.8 %collective-permute-start.11 = (bf16[384,256]{1,0:T(8,128)(2,1)S(1)}, bf16[384,256]{1,0:T(8,128)(2,1)S(1)}, u32[]{:S(2)}, u32[]{:S(2)}) collective-permute-start(bf16[384,256]{1,0:T(8,128)(2,1)S(1)} %shard_map.130.refs_3_), channel_id=1, source_target_pairs={{0,2},{1,3},{2,0},{3,1},{4,6},{5,7},{6,4},{7,5},{8,10},{9,11},{10,... | collective-permute-start | bytes 589832 | tf_op jit(solution)/shard_map/ppermute | solution.py:50
  44.2 5.2 %collective-permute-start.12 = (bf16[384,256]{1,0:T(8,128)(2,1)S(1)}, bf16[384,256]{1,0:T(8,128)(2,1)S(1)}, u32[]{:S(2)}, u32[]{:S(2)}) collective-permute-start(bf16[384,256]{1,0:T(8,128)(2,1)S(1)} %shard_map.130.refs_3_), channel_id=1, source_target_pairs={{0,1},{1,0},{2,3},{3,2},{4,5},{5,4},{6,7},{7,6},{8,9},{9,8},{10,11... | collective-permute-start | bytes 589832 | tf_op jit(solution)/shard_map/ppermute | solution.py:50
  49.4 1.4 %collective-permute-start.13 = (bf16[384,256]{1,0:T(8,128)(2,1)S(1)}, bf16[384,256]{1,0:T(8,128)(2,1)S(1)}, u32[]{:S(2)}, u32[]{:S(2)}) collective-permute-start(bf16[384,256]{1,0:T(8,128)(2,1)S(1)} %collective-permute-done.11.refs_4_), channel_id=1, source_target_pairs={{0,1},{1,0},{2,3},{3,2},{4,5},{5,4},{6,7},{7,6},{8,9},{9,8},{10,11... | collective-permute-start | bytes 589832 | tf_op jit(solution)/shard_map/ppermute | solution.py:50

commit v3 on v2

--- a/solution.py
+++ b/solution.py
@@ -16,7 +16,7 @@
 MASKED = -1e30
 SHIFT, CTX_SHIFT, SCALE, CTX_SCALE, GATE, MOD_ROWS = 0, 1, 2, 3, 4, 8
 
-ANY = pl.BlockSpec(memory_space=pl.ANY)
+HBM = pl.BlockSpec(memory_space=pltpu.HBM)
 VMEM = pl.BlockSpec(memory_space=pltpu.VMEM)
 F32 = jnp.float32
 BF16 = jnp.bfloat16
@@ -30,6 +30,10 @@
         compiler_params=pltpu.CompilerParams(vmem_limit_bytes=vmem_mib * 2**20),
         **kwargs,
     )
+
+
+def in_hbm(arrays):
+    return [pltpu.with_memory_space_constraint(a, pltpu.HBM) for a in arrays]
 
 
 def shape_of(shape, dtype):
@@ -276,8 +280,8 @@
         modulation_kernel,
         shape_of((MOD_ROWS, cols), F32),
         scratch=[pltpu.VMEM(a.shape, a.dtype) for a in mod_inputs] + [pltpu.SemaphoreType.DMA((5,))],
-        in_specs=[ANY] * 5,
-    )(*mod_inputs)
+        in_specs=[HBM] * 5,
+    )(*in_hbm(mod_inputs))
     mod_own = total(partial, "sp")
     mod_pieces = pieces_of(mod_own, "tp")
 
@@ -303,8 +307,8 @@
         scratch=[pltpu.VMEM((MOD_ROWS, model), F32), pltpu.VMEM((tokens, model), BF16)]
         + [pltpu.VMEM(a.shape, a.dtype) for a in fetched]
         + [pltpu.SemaphoreType.DMA((4,))],
-        in_specs=[VMEM] * 2 + [ANY] * 4 + [VMEM] * tp_count,
-    )(latent, norm_gain[None], *fetched, *mod_pieces)
+        in_specs=[VMEM] * 2 + [HBM] * 4 + [VMEM] * tp_count,
+    )(latent, norm_gain[None], *in_hbm(fetched), *mod_pieces)
 
     recv_a = pairwise(send_a, "sp", 0)
     recv_b = pairwise(send_b, "sp", 1)

time: 52.6 us -> 44 us (0.84)
  local copies, waits for them, and re-layouts: 9.83 us -> 0.72 us
  Pallas kernels: 9.45 us -> 10.2 us
    unnamed x25 -> x7, local copies, waits for them, and re-layouts: 9.13 us -> 0.02 us
    pallas_call x1, Pallas kernels: 0.73 us -> 1.79 us  [local(): call(modulation_kernel, shape_of((MOD_ROWS, cols), F32), scratch=[pltpu.V...]
where the time goes in v3:
time: 44 us; the launch traced here: 43.8 us
  waiting for transfers between devices  18.2 us (41%)
  starting transfers between devices  14.4 us (33%)
  Pallas kernels  10.2 us (23%)
  local copies, waits for them, and re-layouts  0.72 us (2%)
    ppermute x12, waiting for transfers between devices, peer(): return lax.ppermute(block, axis, [(i, i ^ mask) for i in range(count)])  18.2 us
    ppermute x12, starting transfers between devices, peer(): return lax.ppermute(block, axis, [(i, i ^ mask) for i in range(count)])  13.7 us
    pallas_call x1, Pallas kernels, local(): call(functools.partial(project_kernel, tp_count=tp_count, sp_axis='sp', t...  4.63 us
    pallas_call x1, Pallas kernels, local(): call(functools.partial(attention_kernel, sp_axis='sp', sp_count=sp_count)...  1.96 us
    pallas_call x1, Pallas kernels, local(): call(modulation_kernel, shape_of((MOD_ROWS, cols), F32), scratch=[pltpu.V...  1.79 us
    pallas_call x1, Pallas kernels, local(): call(functools.partial(output_kernel, masks=[mask for mask, _ in gathered...  1.32 us
  transfers between devices with their start and end apart: 14, of which 8 were waited for; matrix products, arithmetic and copies ran while one was open for 2% of the time, Pallas kernels for 1%

profile of v3, /device:TPU:0, one launch (start us, length us, event | category | flops | bytes accessed | tf_op | source)
XLA Modules:
  0.0 43.8 jit_solution(1460519003369528121)
XLA Ops:
  0.0 1.8 %shard_map.127 = f32[8,512]{1,0:T(8,128)S(1)} custom-call(bf16[512]{0:T(512)(128)(2,1)} %cond_hbm.1, bf16[512]{0:T(512)(128)(2,1)} %ctx_hbm.1, bf16[512,512]{1,0:T(8,128)(2,1)} %w_shift_hbm.1, bf16[512,512]{1,0:T(8,128)(2,1)} %w_scale_hbm.1, bf16[512,512]{1,0:T(8,128)(2,1)} %w_gate_hbm.1), custom_call_target="tpu_custom_call" | custom-call | tf_op jit(solution)/shard_map/pallas_call | solution.py:279
  1.8 5.1 %collective-permute-start.2 = (f32[8,512]{1,0:T(8,128)S(1)}, f32[8,512]{1,0:T(8,128)S(1)}, u32[]{:S(2)}, u32[]{:S(2)}) collective-permute-start(f32[8,512]{1,0:T(8,128)S(1)} %shard_map.127), channel_id=1, source_target_pairs={{0,12},{4,8},{8,4},{12,0},{1,13},{5,9},{9,5},{13,1},{2,14},{6,10},... | collective-permute-start | bytes 49160 | tf_op jit(solution)/shard_map/ppermute | solution.py:54
  6.9 0.0 collective-permute-start.1
  6.9 0.6 %collective-permute-start = (f32[8,512]{1,0:T(8,128)S(1)}, f32[8,512]{1,0:T(8,128)S(1)}, u32[]{:S(2)}, u32[]{:S(2)}) collective-permute-start(f32[8,512]{1,0:T(8,128)S(1)} %shard_map.127), channel_id=1, source_target_pairs={{0,4},{4,0},{8,12},{12,8},{1,5},{5,1},{9,13},{13,9},{2,6},{6,2},{1... | collective-permute-start | bytes 49160 | tf_op jit(solution)/shard_map/ppermute | solution.py:54
  7.6 1.1 %collective-permute-done.2 = f32[8,512]{1,0:T(8,128)S(1)} collective-permute-done((f32[8,512]{1,0:T(8,128)S(1)}, f32[8,512]{1,0:T(8,128)S(1)}, u32[]{:S(2)}, u32[]{:S(2)}) %collective-permute-start.2) | collective-permute-done | bytes 16416 | tf_op jit(solution)/shard_map/ppermute | solution.py:54
  8.7 2.9 %collective-permute-done.1 = f32[8,512]{1,0:T(8,128)S(1)} collective-permute-done((f32[8,512]{1,0:T(8,128)S(1)}, f32[8,512]{1,0:T(8,128)S(1)}, u32[]{:S(2)}, u32[]{:S(2)}) %collective-permute-start.1) | collective-permute-done | bytes 16416 | tf_op jit(solution)/shard_map/ppermute | solution.py:54
  11.6 0.0 collective-permute-done
  11.6 0.1 collective-permute-start.5
  11.7 1.6 %collective-permute-start.4 = (f32[8,512]{1,0:T(8,128)S(1)}, f32[8,512]{1,0:T(8,128)S(1)}, u32[]{:S(2)}, u32[]{:S(2)}) collective-permute-start(f32[8,512]{1,0:T(8,128)S(1)} %add_add_fusion.refs_6_.refs_1_), channel_id=1, source_target_pairs={{0,2},{1,3},{2,0},{3,1},{4,6},{5,7},{6,4},{7,5},{8,10},{9,11},{10,... | collective-permute-start | bytes 49160 | tf_op jit(solution)/shard_map/ppermute | solution.py:54
  13.2 0.3 collective-permute-start.3
  13.5 0.7 %broadcast_in_dim.3.refs_1_ = bf16[1,2048]{1,0:T(2,128)(2,1)S(1)} reshape(bf16[2048]{0:T(1024)(128)(2,1)} %param.20) | data formatting | bytes 8192 | tf_op jit(solution)/shard_map/broadcast_in_dim | solution.py:311
  14.2 0.7 %collective-permute-done.5.refs_9_ = f32[8,512]{1,0:T(8,128)S(1)} collective-permute-done((f32[8,512]{1,0:T(8,128)S(1)}, f32[8,512]{1,0:T(8,128)S(1)}, u32[]{:S(2)}, u32[]{:S(2)}) %collective-permute-start.5) | collective-permute-done | bytes 16416 | tf_op jit(solution)/shard_map/ppermute | solution.py:54
  14.9 0.5 %collective-permute-done.4.refs_8_ = f32[8,512]{1,0:T(8,128)S(1)} collective-permute-done((f32[8,512]{1,0:T(8,128)S(1)}, f32[8,512]{1,0:T(8,128)S(1)}, u32[]{:S(2)}, u32[]{:S(2)}) %collective-permute-start.4) | collective-permute-done | bytes 16416 | tf_op jit(solution)/shard_map/ppermute | solution.py:54
  15.5 0.0 collective-permute-done.3.refs_7_
  15.5 4.6 %shard_map.128 = (bf16[384,256]{1,0:T(8,128)(2,1)S(1)}, bf16[384,512]{1,0:T(8,128)(2,1)S(1)}, bf16[256,512]{1,0:T(8,128)(2,1)S(1)}, bf16[256,512]{1,0:T(8,128)(2...) custom-call(bf16[384,2048]{1,0:T(8,128)(2,1)S(1)} %copy-done, ...), custom_call_target="tpu_custom_call" | custom-call | tf_op jit(solution)/shard_map/pallas_call | solution.py:297
  20.1 0.1 collective-permute-start.6
  20.2 0.7 %collective-permute-start.7 = (bf16[256,512]{1,0:T(8,128)(2,1)S(1)}, bf16[256,512]{1,0:T(8,128)(2,1)S(1)}, u32[]{:S(2)}, u32[]{:S(2)}) collective-permute-start(bf16[256,512]{1,0:T(8,128)(2,1)S(1)} %get-tuple-element.15), channel_id=1, source_target_pairs={{4,8},{8,4},{5,9},{9,5},{6,10},{10,6},{7,11},{11,7},{20,24},{24,20... | collective-permute-start | bytes 786440 | tf_op jit(solution)/shard_map/ppermute | solution.py:86
  20.9 3.5 %collective-permute-start.10 = (bf16[16,512]{1,0:T(8,128)(2,1)S(1)}, bf16[16,512]{1,0:T(8,128)(2,1)S(1)}, u32[]{:S(2)}, u32[]{:S(2)}) collective-permute-start(bf16[16,512]{1,0:T(8,128)(2,1)S(1)} %get-tuple-element.16.refs_5_), channel_id=1, source_target_pairs={{0,12},{4,8},{8,4},{12,0},{1,13},{5,9},{9,5},{13,1},{2,14},{6,10},... | collective-permute-start | bytes 49160 | tf_op jit(solution)/shard_map/ppermute | solution.py:54
  24.4 1.8 %collective-permute-start.9 = (bf16[16,512]{1,0:T(8,128)(2,1)S(1)}, bf16[16,512]{1,0:T(8,128)(2,1)S(1)}, u32[]{:S(2)}, u32[]{:S(2)}) collective-permute-start(bf16[16,512]{1,0:T(8,128)(2,1)S(1)} %get-tuple-element.16.refs_5_), channel_id=1, source_target_pairs={{0,8},{4,12},{8,0},{12,4},{1,9},{5,13},{9,1},{13,5},{2,10},{6,14},... | collective-permute-start | bytes 49160 | tf_op jit(solution)/shard_map/ppermute | solution.py:54
  26.2 0.1 collective-permute-start.8
  26.2 0.1 pad_maximum_fusion.pairs_ref
  26.3 0.5 %shard_map.129.refs_4_ = f32[14,256,128]{2,1,0:T(8,128)S(1)} custom-call(f32[4,14,128]{2,1,0:T(8,128)S(1)} %pad_maximum_fusion.pairs_ref), custom_call_target="tpu_custom_call" | custom-call | tf_op jit(solution)/shard_map/pallas_call | solution.py:291
  26.9 0.0 copy-start.1
  26.9 4.1 %collective-permute-done.10.refs_8_ = bf16[16,512]{1,0:T(8,128)(2,1)S(1)} collective-permute-done((bf16[16,512]{1,0:T(8,128)(2,1)S(1)}, bf16[16,512]{1,0:T(8,128)(2,1)S(1)}, u32[]{:S(2)}, u32[]{:S(2)}) %collective-permute-start.10) | collective-permute-done | bytes 16416 | tf_op jit(solution)/shard_map/ppermute | solution.py:54
  31.0 2.3 %collective-permute-done.9.refs_7_ = bf16[16,512]{1,0:T(8,128)(2,1)S(1)} collective-permute-done((bf16[16,512]{1,0:T(8,128)(2,1)S(1)}, bf16[16,512]{1,0:T(8,128)(2,1)S(1)}, u32[]{:S(2)}, u32[]{:S(2)}) %collective-permute-start.9) | collective-permute-done | bytes 16416 | tf_op jit(solution)/shard_map/ppermute | solution.py:54
  33.2 0.0 collective-permute-done.8.refs_6_
  33.2 0.0 collective-permute-done.6.refs_2_
  33.3 2.0 %shard_map.130.refs_3_ = bf16[384,256]{1,0:T(8,128)(2,1)S(1)} custom-call(bf16[384,256]{1,0:T(8,128)(2,1)S(1)} %get-tuple-element.12.refs_0_, bf16[384,512]{1,0:T(8,128)(2,1)S(1)} %get-tuple-element.13.refs_1_, bf16[256,512]{1,0:T(8,128)(2,1)S(1)} %collective-permute-done.6.refs_2_, bf16[256,512]{1,0:T(8,128)(2,1)S(1)} %collective-permute-done.7.refs_3_, ...), custom_call_target="tpu_custom_call" | custom-call | tf_op jit(solution)/shard_map/pallas_call | solution.py:317
  35.2 0.6 %collective-permute-start.11 = (bf16[384,256]{1,0:T(8,128)(2,1)S(1)}, bf16[384,256]{1,0:T(8,128)(2,1)S(1)}, u32[]{:S(2)}, u32[]{:S(2)}) collective-permute-start(bf16[384,256]{1,0:T(8,128)(2,1)S(1)} %shard_map.130.refs_3_), channel_id=1, source_target_pairs={{0,2},{1,3},{2,0},{3,1},{4,6},{5,7},{6,4},{7,5},{8,10},{9,11},{10,... | collective-permute-start | bytes 589832 | tf_op jit(solution)/shard_map/ppermute | solution.py:54
  35.9 5.2 %collective-permute-done.11.refs_4_ = bf16[384,256]{1,0:T(8,128)(2,1)S(1)} collective-permute-done((bf16[384,256]{1,0:T(8,128)(2,1)S(1)}, bf16[384,256]{1,0:T(8,128)(2,1)S(1)}, u32[]{:S(2)}, u32[]{:S(2)}) %collective-permute-start.11) | collective-permute-done | bytes 196640 | tf_op jit(solution)/shard_map/ppermute | solution.py:54
  41.0 1.4 %collective-permute-done.13.refs_6_ = bf16[384,256]{1,0:T(8,128)(2,1)S(1)} collective-permute-done((bf16[384,256]{1,0:T(8,128)(2,1)S(1)}, bf16[384,256]{1,0:T(8,128)(2,1)S(1)}, u32[]{:S(2)}, u32[]{:S(2)}) %collective-permute-start.13) | collective-permute-done | bytes 196640 | tf_op jit(solution)/shard_map/ppermute | solution.py:54
  42.5 1.3 %shard_map.131 = bf16[384,512]{1,0:T(8,128)(2,1)} custom-call(bf16[384,512]{1,0:T(8,128)(2,1)S(1)} %get-tuple-element.11.refs_0_, f32[8,512]{1,0:T(8,128)S(1)} %add_add_fusion.refs_6_.refs_1_, bf16[1024,512]{1,0:T(8,128)(2,1)S(1)} %copy-done.1, bf16[384,256]{1,0:T(8,128)(2,1)S(1)} %shard_map.130.refs_3_, ...), custom_call_target="tpu_custom_call" | custom-call | tf_op jit(solution)/shard_map/pallas_call | solution.py:324
  (12 shorter events, 0.0 us)
Async XLA Ops:
  0.0 15.5 %copy-start = (bf16[384,2048]{1,0:T(8,128)(2,1)S(1)}, bf16[384,2048]{1,0:T(8,128)(2,1)}, u32[]{:S(2)}) copy-start(bf16[384,2048]{1,0:T(8,128)(2,1)} %refs_0_.1) | copy-start | bytes 4718596
  1.8 6.9 %collective-permute-start.2 = (f32[8,512]{1,0:T(8,128)S(1)}, f32[8,512]{1,0:T(8,128)S(1)}, u32[]{:S(2)}, u32[]{:S(2)}) collective-permute-start(f32[8,512]{1,0:T(8,128)S(1)} %shard_map.127), channel_id=1, source_target_pairs={{0,12},{4,8},{8,4},{12,0},{1,13},{5,9},{9,5},{13,1},{2,14},{6,10},... | collective-permute-start | bytes 49160 | tf_op jit(solution)/shard_map/ppermute | solution.py:54
  6.9 4.6 %collective-permute-start.1 = (f32[8,512]{1,0:T(8,128)S(1)}, f32[8,512]{1,0:T(8,128)S(1)}, u32[]{:S(2)}, u32[]{:S(2)}) collective-permute-start(f32[8,512]{1,0:T(8,128)S(1)} %shard_map.127), channel_id=1, source_target_pairs={{0,8},{4,12},{8,0},{12,4},{1,9},{5,13},{9,1},{13,5},{2,10},{6,14},... | collective-permute-start | bytes 49160 | tf_op jit(solution)/shard_map/ppermute | solution.py:54
  6.9 4.6 %collective-permute-start = (f32[8,512]{1,0:T(8,128)S(1)}, f32[8,512]{1,0:T(8,128)S(1)}, u32[]{:S(2)}, u32[]{:S(2)}) collective-permute-start(f32[8,512]{1,0:T(8,128)S(1)} %shard_map.127), channel_id=1, source_target_pairs={{0,4},{4,0},{8,12},{12,8},{1,5},{5,1},{9,13},{13,9},{2,6},{6,2},{1... | collective-permute-start | bytes 49160 | tf_op jit(solution)/shard_map/ppermute | solution.py:54
  11.6 3.4 %collective-permute-start.5 = (f32[8,512]{1,0:T(8,128)S(1)}, f32[8,512]{1,0:T(8,128)S(1)}, u32[]{:S(2)}, u32[]{:S(2)}) collective-permute-start(f32[8,512]{1,0:T(8,128)S(1)} %add_add_fusion.refs_6_.refs_1_), channel_id=1, source_target_pairs={{0,3},{1,2},{2,1},{3,0},{4,7},{5,6},{6,5},{7,4},{8,11},{9,10},{10,... | collective-permute-start | bytes 49160 | tf_op jit(solution)/shard_map/ppermute | solution.py:54
  11.7 3.8 %collective-permute-start.4 = (f32[8,512]{1,0:T(8,128)S(1)}, f32[8,512]{1,0:T(8,128)S(1)}, u32[]{:S(2)}, u32[]{:S(2)}) collective-permute-start(f32[8,512]{1,0:T(8,128)S(1)} %add_add_fusion.refs_6_.refs_1_), channel_id=1, source_target_pairs={{0,2},{1,3},{2,0},{3,1},{4,6},{5,7},{6,4},{7,5},{8,10},{9,11},{10,... | collective-permute-start | bytes 49160 | tf_op jit(solution)/shard_map/ppermute | solution.py:54
  13.2 2.3 %collective-permute-start.3 = (f32[8,512]{1,0:T(8,128)S(1)}, f32[8,512]{1,0:T(8,128)S(1)}, u32[]{:S(2)}, u32[]{:S(2)}) collective-permute-start(f32[8,512]{1,0:T(8,128)S(1)} %add_add_fusion.refs_6_.refs_1_), channel_id=1, source_target_pairs={{0,1},{1,0},{2,3},{3,2},{4,5},{5,4},{6,7},{7,6},{8,9},{9,8},{10,11... | collective-permute-start | bytes 49160 | tf_op jit(solution)/shard_map/ppermute | solution.py:54
  14.2 6.7 %copy-start.2 = (f32[4,15,31]{2,0,1:T(4,128)S(1)}, f32[4,15,31]{2,0,1:T(4,128)}, u32[]{:S(2)}) copy-start(f32[4,15,31]{2,0,1:T(4,128)} %param.24) | copy-start | bytes 22324
  20.1 13.1 %collective-permute-start.6 = (bf16[256,512]{1,0:T(8,128)(2,1)S(1)}, bf16[256,512]{1,0:T(8,128)(2,1)S(1)}, u32[]{:S(2)}, u32[]{:S(2)}) collective-permute-start(bf16[256,512]{1,0:T(8,128)(2,1)S(1)} %get-tuple-element.14), channel_id=1, source_target_pairs={{0,4},{4,0},{8,12},{12,8},{1,5},{5,1},{9,13},{13,9},{2,6},{6,2},{1... | collective-permute-start | bytes 786440 | tf_op jit(solution)/shard_map/ppermute | solution.py:86
  20.2 13.1 %collective-permute-start.7 = (bf16[256,512]{1,0:T(8,128)(2,1)S(1)}, bf16[256,512]{1,0:T(8,128)(2,1)S(1)}, u32[]{:S(2)}, u32[]{:S(2)}) collective-permute-start(bf16[256,512]{1,0:T(8,128)(2,1)S(1)} %get-tuple-element.15), channel_id=1, source_target_pairs={{4,8},{8,4},{5,9},{9,5},{6,10},{10,6},{7,11},{11,7},{20,24},{24,20... | collective-permute-start | bytes 786440 | tf_op jit(solution)/shard_map/ppermute | solution.py:86
  20.9 10.0 %collective-permute-start.10 = (bf16[16,512]{1,0:T(8,128)(2,1)S(1)}, bf16[16,512]{1,0:T(8,128)(2,1)S(1)}, u32[]{:S(2)}, u32[]{:S(2)}) collective-permute-start(bf16[16,512]{1,0:T(8,128)(2,1)S(1)} %get-tuple-element.16.refs_5_), channel_id=1, source_target_pairs={{0,12},{4,8},{8,4},{12,0},{1,13},{5,9},{9,5},{13,1},{2,14},{6,10},... | collective-permute-start | bytes 49160 | tf_op jit(solution)/shard_map/ppermute | solution.py:54
  24.4 8.9 %collective-permute-start.9 = (bf16[16,512]{1,0:T(8,128)(2,1)S(1)}, bf16[16,512]{1,0:T(8,128)(2,1)S(1)}, u32[]{:S(2)}, u32[]{:S(2)}) collective-permute-start(bf16[16,512]{1,0:T(8,128)(2,1)S(1)} %get-tuple-element.16.refs_5_), channel_id=1, source_target_pairs={{0,8},{4,12},{8,0},{12,4},{1,9},{5,13},{9,1},{13,5},{2,10},{6,14},... | collective-permute-start | bytes 49160 | tf_op jit(solution)/shard_map/ppermute | solution.py:54
  26.2 7.0 %collective-permute-start.8 = (bf16[16,512]{1,0:T(8,128)(2,1)S(1)}, bf16[16,512]{1,0:T(8,128)(2,1)S(1)}, u32[]{:S(2)}, u32[]{:S(2)}) collective-permute-start(bf16[16,512]{1,0:T(8,128)(2,1)S(1)} %get-tuple-element.16.refs_5_), channel_id=1, source_target_pairs={{0,4},{4,0},{8,12},{12,8},{1,5},{5,1},{9,13},{13,9},{2,6},{6,2},{1... | collective-permute-start | bytes 49160 | tf_op jit(solution)/shard_map/ppermute | solution.py:54
  26.9 15.6 %copy-start.1 = (bf16[1024,512]{1,0:T(8,128)(2,1)S(1)}, bf16[1024,512]{1,0:T(8,128)(2,1)}, u32[]{:S(2)}) copy-start(bf16[1024,512]{1,0:T(8,128)(2,1)} %refs_2_.3) | copy-start | bytes 3145732
  35.2 5.8 %collective-permute-start.11 = (bf16[384,256]{1,0:T(8,128)(2,1)S(1)}, bf16[384,256]{1,0:T(8,128)(2,1)S(1)}, u32[]{:S(2)}, u32[]{:S(2)}) collective-permute-start(bf16[384,256]{1,0:T(8,128)(2,1)S(1)} %shard_map.130.refs_3_), channel_id=1, source_target_pairs={{0,2},{1,3},{2,0},{3,1},{4,6},{5,7},{6,4},{7,5},{8,10},{9,11},{10,... | collective-permute-start | bytes 589832 | tf_op jit(solution)/shard_map/ppermute | solution.py:54
  35.9 5.2 %collective-permute-start.12 = (bf16[384,256]{1,0:T(8,128)(2,1)S(1)}, bf16[384,256]{1,0:T(8,128)(2,1)S(1)}, u32[]{:S(2)}, u32[]{:S(2)}) collective-permute-start(bf16[384,256]{1,0:T(8,128)(2,1)S(1)} %shard_map.130.refs_3_), channel_id=1, source_target_pairs={{0,1},{1,0},{2,3},{3,2},{4,5},{5,4},{6,7},{7,6},{8,9},{9,8},{10,11... | collective-permute-start | bytes 589832 | tf_op jit(solution)/shard_map/ppermute | solution.py:54
  41.0 1.4 %collective-permute-start.13 = (bf16[384,256]{1,0:T(8,128)(2,1)S(1)}, bf16[384,256]{1,0:T(8,128)(2,1)S(1)}, u32[]{:S(2)}, u32[]{:S(2)}) collective-permute-start(bf16[384,256]{1,0:T(8,128)(2,1)S(1)} %collective-permute-done.11.refs_4_), channel_id=1, source_target_pairs={{0,1},{1,0},{2,3},{3,2},{4,5},{5,4},{6,7},{7,6},{8,9},{9,8},{10,11... | collective-permute-start | bytes 589832 | tf_op jit(solution)/shard_map/ppermute | solution.py:54

commit v4 on v3

v4 whole, which is shorter than its diff:
```python
import functools

import jax
import jax.numpy as jnp
from jax import lax
from jax.experimental import pallas as pl
from jax.experimental.pallas import tpu as pltpu
from jax.sharding import PartitionSpec as P

HEAD_DIM = 64
GRID_W = 64
WIN_H = 8
WIN_W = 16
EPSILON = 1e-06
HALO = WIN_H // 2
MASKED = -1e30
SHIFT, CTX_SHIFT, SCALE, CTX_SCALE, GATE, MOD_ROWS = 0, 1, 2, 3, 4, 8

HBM = pl.BlockSpec(memory_space=pltpu.HBM)
VMEM = pl.BlockSpec(memory_space=pltpu.VMEM)
F32 = jnp.float32
BF16 = jnp.bfloat16


def call(kernel, out_shape, scratch=(), vmem_mib=24, **kwargs):
    return pl.pallas_call(
        kernel,
        out_shape=out_shape,
        scratch_shapes=list(scratch),
        compiler_params=pltpu.CompilerParams(vmem_limit_bytes=vmem_mib * 2**20),
        **kwargs,
    )


def in_hbm(arrays):
    return [pltpu.with_memory_space_constraint(a, pltpu.HBM) for a in arrays]


def shape_of(shape, dtype):
    return jax.ShapeDtypeStruct(shape, dtype)


def digits(count):
    unit, found = 1, []
    while unit < count:
        radix = 4 if count // unit % 4 == 0 else 2
        found.append((unit, radix))
        unit *= radix
    return found


def peer(block, axis, mask):
    count = lax.axis_size(axis)
    return lax.ppermute(block, axis, [(i, i ^ mask) for i in range(count)])


def joined(parts):
    sums = None
    for part in parts:
        rows = part[:MOD_ROWS].astype(F32) + part[MOD_ROWS : 2 * MOD_ROWS].astype(F32)
        sums = rows if sums is None else sums + rows
    return sums, jnp.concatenate([part[2 * MOD_ROWS :] for part in parts], axis=0)


def total_and_context(block, axis):
    steps = digits(lax.axis_size(axis))
    for i, (unit, radix) in enumerate(steps):
        far_first = [peer(block, axis, unit * k) for k in reversed(range(1, radix))]
        sums, context = joined([block] + far_first)
        if i + 1 < len(steps):
            high = lax.reduce_precision(sums, 8, 7)
            block = jnp.concatenate([high, sums - high], axis=0).astype(BF16)
            block = jnp.concatenate([block, context], axis=0)
    return sums, context


def pieces_of(block, axis):
    pieces = [block]
    for unit, radix in digits(lax.axis_size(axis)):
        pieces = pieces + [peer(p, axis, unit * k) for k in range(1, radix) for p in pieces]
    return pieces


def pieces_by_bits(block, axis):
    pieces = [(0, block)]
    bit = lax.axis_size(axis) // 2
    while bit:
        pieces = pieces + [(mask ^ bit, peer(p, axis, bit)) for mask, p in pieces]
        bit //= 2
    return pieces


def pairwise(block, axis, first):
    count = lax.axis_size(axis)
    pairs = []
    for low in range(first, count - 1, 2):
        pairs += [(low, low + 1), (low + 1, low)]
    return lax.ppermute(block, axis, pairs)


def silu(v):
    return v / (1.0 + jnp.exp(-v))


def fetch(pairs, sems):
    copies = [
        pltpu.make_async_copy(source, target, sems.at[i]) for i, (source, target) in enumerate(pairs)
    ]
    for copy in copies:
        copy.start()
    return copies


def modulation_kernel(
    cond_hbm, ctx_hbm, w_shift_hbm, w_scale_hbm, w_gate_hbm, context_hbm, out_ref, *scratch
):
    cond_ref, ctx_ref, w_shift_ref, w_scale_ref, w_gate_ref, context_ref, sems = scratch
    cols = w_shift_ref.shape[1]
    own = pl.ds(pl.multiple_of(lax.axis_index("tp") * cols, 128), cols)
    sources = (cond_hbm, ctx_hbm, w_shift_hbm, w_scale_hbm, w_gate_hbm, context_hbm.at[:, own])
    copies = fetch(list(zip(sources, scratch[:-1])), sems)
    copies[0].wait()
    copies[1].wait()
    cond = silu(cond_ref[...].astype(F32)).reshape(1, -1)
    ctx = silu(ctx_ref[...].astype(F32)).reshape(1, -1)
    row = lax.broadcasted_iota(jnp.int32, (MOD_ROWS, cond.shape[1]), 0)
    acts = jnp.where(row % 2 == 0, cond, ctx).astype(BF16)
    copies[2].wait()
    shifts = jnp.dot(acts, w_shift_ref[...], preferred_element_type=F32)
    copies[3].wait()
    scales = jnp.dot(acts, w_scale_ref[...], preferred_element_type=F32)
    copies[4].wait()
    gates = jnp.dot(acts, w_gate_ref[...], preferred_element_type=F32)
    out_row = lax.broadcasted_iota(jnp.int32, shifts.shape, 0)
    sums = jnp.where(out_row < SCALE, shifts, jnp.where(out_row < GATE, scales, gates))
    high = sums.astype(BF16).astype(F32)
    out_ref[: 2 * MOD_ROWS, :] = jnp.concatenate([high, sums - high], axis=0).astype(BF16)
    copies[5].wait()
    out_ref[2 * MOD_ROWS :, :] = context_ref[...]


def bias_kernel(pairs_ref, out_ref, *, heads):
    query = lax.broadcasted_iota(jnp.int32, (GRID_W, 2 * GRID_W), 0)
    key = lax.broadcasted_iota(jnp.int32, (GRID_W, 2 * GRID_W), 1) % GRID_W
    first = jnp.clip(query - WIN_W // 2, 0, GRID_W - WIN_W)
    inside = (key >= first) & (key < first + WIN_W)
    for h in range(heads):
        for p in range(2 * WIN_H - 2):
            row = pairs_ref[h, p : p + 1, :]
            table = pltpu.roll(
                jnp.broadcast_to(row, (GRID_W, 2 * GRID_W)),
                2 * GRID_W - (WIN_W - 1),
                1,
                stride=1,
                stride_axis=0,
            )
            out_ref[p, h * GRID_W : (h + 1) * GRID_W, :] = jnp.where(inside, table, MASKED)


def inverse_rms(floats):
    return lax.rsqrt(jnp.mean(floats * floats, axis=-1, keepdims=True) + EPSILON)


def send_halo(kv_ref, send_a_ref, send_b_ref):
    halo = HALO * GRID_W
    last = kv_ref.shape[0] - halo
    odd = lax.axis_index("sp") % 2
    send_a_ref[...] = kv_ref[pl.ds(pl.multiple_of((1 - odd) * last, GRID_W), halo), :]
    send_b_ref[...] = kv_ref[pl.ds(pl.multiple_of(odd * last, GRID_W), halo), :]


def norm_kernel(*refs, tp_count, chunks):
    latent_ref, gain_hbm, wk_hbm, wv_hbm = refs[:4]
    piece_refs = refs[4 : 4 + tp_count]
    outs = refs[4 + tp_count : -4]
    normed_ref, kv_ref, send_a_ref, send_b_ref, mod_ref, gain_out_ref = outs[:6]
    weight_refs = outs[6:]
    gain_ref, factor_ref, offset_ref, sems = refs[-4:]
    tokens, _ = latent_ref.shape
    cols = piece_refs[0].shape[1]
    each = weight_refs[0].shape[1] // 2
    pairs = [(gain_hbm, gain_ref)]
    for c, weight in enumerate(weight_refs):
        at = pl.ds(c * each, each)
        pairs += [(wk_hbm.at[:, at], weight.at[:, :each]), (wv_hbm.at[:, at], weight.at[:, each:])]
    copies = fetch(pairs, sems)
    tp_index = lax.axis_index("tp")
    for k, piece in enumerate(piece_refs):
        offset = pl.multiple_of((tp_index ^ k) * cols, 128)
        mod_ref[:, pl.ds(offset, cols)] = piece[...]
    copies[0].wait()
    gain = gain_ref[...].astype(F32).reshape(1, -1)
    gain_out_ref[...] = jnp.broadcast_to(gain, gain_out_ref.shape)
    factor_ref[...] = jnp.broadcast_to(gain * (1.0 + mod_ref[SCALE : SCALE + 1, :]), factor_ref.shape)
    offset_ref[...] = jnp.broadcast_to(mod_ref[SHIFT : SHIFT + 1, :], offset_ref.shape)
    step = 16

    def body(i, carry):
        at = pl.ds(pl.multiple_of(i * step, step), step)
        floats = latent_ref[at, :].astype(F32)
        scaled = (floats * inverse_rms(floats)).reshape(step // 8, 8, -1)
        result = scaled * factor_ref[...][None] + offset_ref[...][None]
        normed_ref[at, :] = result.reshape(step, -1).astype(BF16)
        return carry

    lax.fori_loop(0, tokens // step, body, 0, unroll=2)
    copies[1].wait()
    copies[2].wait()
    kv_ref[...] = jnp.dot(
        normed_ref[...], weight_refs[0][...], preferred_element_type=F32
    ).astype(BF16)
    send_halo(kv_ref, send_a_ref, send_b_ref)
    for copy in copies[3:]:
        copy.wait()


def chunk_kernel(normed_ref, weight_ref, kv_ref, send_a_ref, send_b_ref):
    kv_ref[...] = jnp.dot(
        normed_ref[...], weight_ref[...], preferred_element_type=F32
    ).astype(BF16)
    send_halo(kv_ref, send_a_ref, send_b_ref)


def query_kernel(normed_ref, wq_ref, latent_ref, q_ref, resid_ref):
    cols = resid_ref.shape[1]
    query = jnp.dot(normed_ref[...], wq_ref[...], preferred_element_type=F32).astype(BF16)
    q_ref[...] = query * BF16(HEAD_DIM**-0.5)
    own = pl.ds(pl.multiple_of(lax.axis_index("tp") * cols, 128), cols)
    resid_ref[...] = latent_ref[:, own]


def context_kernel(*refs, masks, chunks):
    mod_ref, gain_ref = refs[:2]
    piece_refs = refs[2 : 2 + len(masks)]
    weight_refs = refs[2 + len(masks) : 2 + len(masks) + chunks]
    out_refs, whole_ref = refs[2 + len(masks) + chunks : -1], refs[-1]
    cols = piece_refs[0].shape[1]
    tp_index = lax.axis_index("tp")
    for mask, piece in zip(masks, piece_refs):
        whole_ref[:, pl.ds(pl.multiple_of((tp_index ^ mask) * cols, 128), cols)] = piece[...]
    floats = whole_ref[...].astype(F32)
    factor = gain_ref[0:1, :] * (1.0 + mod_ref[CTX_SCALE : CTX_SCALE + 1, :])
    shift = mod_ref[CTX_SHIFT : CTX_SHIFT + 1, :]
    normed = (floats * inverse_rms(floats) * factor + shift).astype(BF16)
    for weight, out in zip(weight_refs, out_refs):
        out[...] = jnp.dot(normed, weight[...], preferred_element_type=F32).astype(BF16)


def attention_kernel(
    q_ref, kv_ref, recv_a_ref, recv_b_ref, table_ref, ctx_ref, out_ref, pad_ref, *, chunk, sp_count
):
    tokens, width = out_ref.shape
    heads = width // HEAD_DIM
    rows = tokens // GRID_W
    halo = HALO * GRID_W
    sp_index = lax.axis_index("sp")
    odd = sp_index % 2
    far = halo + tokens
    pad_ref[pl.ds(pl.multiple_of((1 - odd) * far, GRID_W), halo), :] = recv_a_ref[...]
    pad_ref[pl.ds(pl.multiple_of(odd * far, GRID_W), halo), :] = recv_b_ref[...]
    pad_ref[halo : halo + tokens, :] = kv_ref[...]
    ctx_keys, ctx_values = ctx_ref[:, :width], ctx_ref[:, width:]
    lane_head = lax.broadcasted_iota(jnp.int32, (1, width), 1) // HEAD_DIM
    picks = [(lane_head == h) for h in range(heads)]
    table_rows = slice(chunk * heads * GRID_W, (chunk + 1) * heads * GRID_W)
    nt = (((1,), (1,)), ((), ()))
    for l in range(rows):
        at = l * GRID_W
        grid_row = sp_index * rows + l
        first = jnp.clip(grid_row - HALO, 0, sp_count * rows - WIN_H)
        start = first - sp_index * rows + HALO
        offset = first - grid_row + WIN_H - 1
        query = q_ref[at : at + GRID_W, chunk * width : (chunk + 1) * width]
        left = jnp.concatenate([jnp.where(pick, query, BF16(0)) for pick in picks], axis=0)
        window = pl.ds(pl.multiple_of(start * GRID_W, GRID_W), WIN_H * GRID_W)
        scores = lax.dot_general(left, pad_ref[window, :width], nt, preferred_element_type=F32)
        ctx_scores = lax.dot_general(left, ctx_keys, nt, preferred_element_type=F32)
        bias = jnp.concatenate(
            [table_ref[offset + 2 * k, table_rows, :] for k in range(WIN_H // 2)], axis=1
        )
        scores = scores + bias
        highest = jnp.maximum(
            jnp.max(scores, axis=1, keepdims=True), jnp.max(ctx_scores, axis=1, keepdims=True)
        )
        win_exp = jnp.exp(scores - highest)
        ctx_exp = jnp.exp(ctx_scores - highest)
        totals = jnp.sum(win_exp, axis=1, keepdims=True) + jnp.sum(ctx_exp, axis=1, keepdims=True)
        mixed = jnp.dot(
            win_exp.astype(BF16), pad_ref[window, width:], preferred_element_type=F32
        ) + jnp.dot(ctx_exp.astype(BF16), ctx_values, preferred_element_type=F32)
        mixed = mixed * (1.0 / totals)
        result = mixed[:GRID_W]
        for h in range(1, heads):
            result = jnp.where(picks[h], mixed[h * GRID_W : (h + 1) * GRID_W], result)
        out_ref[at : at + GRID_W, :] = result.astype(BF16)


def output_kernel(*refs, masks, chunks):
    resid_ref, mod_ref, w_out_ref = refs[:3]
    piece_refs, out_ref = refs[3:-1], refs[-1]
    tp_index = lax.axis_index("tp")
    count = len(masks)
    width = chunks * piece_refs[0].shape[1]
    branch = None
    for i, mask in enumerate(masks):
        offset = pl.multiple_of((tp_index ^ mask) * width, 128)
        piece = jnp.concatenate([piece_refs[c * count + i][...] for c in range(chunks)], axis=1)
        part = jnp.dot(piece, w_out_ref[pl.ds(offset, width), :], preferred_element_type=F32)
        branch = part if branch is None else branch + part
    out_ref[...] = (resid_ref[...].astype(F32) + mod_ref[GATE : GATE + 1, :] * branch).astype(BF16)


def local(
    latent,
    conditioning,
    context,
    ctx_vector,
    w_shift,
    w_scale,
    w_gate,
    norm_gain,
    w_query,
    w_key,
    w_value,
    offset_bias,
    w_out,
):
    tokens, model = latent.shape
    cols = w_shift.shape[1]
    width = w_query.shape[1]
    heads = width // HEAD_DIM
    chunks = width // 128 if width % 128 == 0 else 1
    each = width // chunks
    sp_count, tp_count = lax.axis_size("sp"), lax.axis_size("tp")
    halo = HALO * GRID_W

    own_context = shape_of((context.shape[0], cols), BF16)
    mod_inputs = (conditioning, ctx_vector, w_shift, w_scale, w_gate)
    partial = call(
        modulation_kernel,
        shape_of((2 * MOD_ROWS + context.shape[0], cols), BF16),
        scratch=[pltpu.VMEM(a.shape, a.dtype) for a in mod_inputs + (own_context,)]
        + [pltpu.SemaphoreType.DMA((6,))],
        in_specs=[HBM] * 6,
    )(*in_hbm(mod_inputs + (context,)))
    mod_own, ctx_own = total_and_context(partial, "sp")
    mod_pieces = pieces_of(mod_own, "tp")

    lanes = GRID_W - offset_bias.shape[2]
    padded = jnp.pad(offset_bias, ((0, 0), (0, 0), (0, lanes)))
    pairs = jnp.concatenate([padded[:, :-1], padded[:, 1:]], axis=2)
    table = call(
        functools.partial(bias_kernel, heads=heads),
        shape_of((2 * WIN_H - 2, heads * GRID_W, 2 * GRID_W), F32),
    )(pairs)

    kv_shapes = (
        shape_of((tokens, 2 * each), BF16),
        shape_of((halo, 2 * each), BF16),
        shape_of((halo, 2 * each), BF16),
    )
    normed, kv_0, send_a_0, send_b_0, mod, gain, *weights = call(
        functools.partial(norm_kernel, tp_count=tp_count, chunks=chunks),
        (shape_of((tokens, model), BF16),)
        + kv_shapes
        + (shape_of((MOD_ROWS, model), F32), shape_of((8, model), F32))
        + (shape_of((model, 2 * each), BF16),) * chunks,
        scratch=[
            pltpu.VMEM((model,), BF16),
            pltpu.VMEM((8, model), F32),
            pltpu.VMEM((8, model), F32),
            pltpu.SemaphoreType.DMA((1 + 2 * chunks,)),
        ],
        in_specs=[VMEM] + [HBM] * 3 + [VMEM] * tp_count,
    )(latent, *in_hbm((norm_gain, w_key, w_value)), *mod_pieces)

    keys_values = [(kv_0, send_a_0, send_b_0)] + [
        call(chunk_kernel, kv_shapes)(normed, weight) for weight in weights[1:]
    ]
    halos = [(pairwise(a, "sp", 0), pairwise(b, "sp", 1)) for _, a, b in keys_values]

    query, resid = call(
        query_kernel, (shape_of((tokens, width), BF16), shape_of((tokens, cols), BF16))
    )(normed, w_query, latent)

    ctx_pieces = pieces_by_bits(ctx_own, "tp")
    ctx_rows = ctx_own.shape[0]
    ctx_all = call(
        functools.partial(context_kernel, masks=[m for m, _ in ctx_pieces], chunks=chunks),
        (shape_of((ctx_rows, 2 * each), BF16),) * chunks,
        scratch=[pltpu.VMEM((ctx_rows, model), BF16)],
    )(mod, gain, *[p for _, p in ctx_pieces], *weights)

    gathered = []
    for c in range(chunks):
        attended = call(
            functools.partial(attention_kernel, chunk=c, sp_count=sp_count),
            shape_of((tokens, each), BF16),
            scratch=[pltpu.VMEM((tokens + 2 * halo, 2 * each), BF16)],
        )(query, keys_values[c][0], *halos[c], table, ctx_all[c])
        found = pieces_by_bits(attended, "tp")
        masks = [mask for mask, _ in found]
        gathered += [piece for _, piece in found]

    return call(
        functools.partial(output_kernel, masks=masks, chunks=chunks),
        shape_of((tokens, cols), BF16),
    )(resid, mod_own, w_out, *gathered)


def solution(mesh):
    return jax.shard_map(
        local,
        mesh=mesh,
        in_specs=(
            P(("grp", "sp"), None),
            P(("grp", "sp")),
            P(("grp", "sp"), None),
            P("sp"),
            P("sp", "tp"),
            P("sp", "tp"),
            P("sp", "tp"),
            P(),
            P(None, "tp"),
            P(None, "tp"),
            P(None, "tp"),
            P("tp", None, None),
            P(None, "tp"),
        ),
        out_specs=P(("grp", "sp"), "tp"),
        check_vma=False,
    )
```

time: 44 us -> 41.7 us (0.948)
  waiting for transfers between devices: 18.2 us -> 10.9 us
  starting transfers between devices: 14.4 us -> 17.8 us
  Pallas kernels: 10.2 us -> 12.6 us
  local copies, waits for them, and re-layouts: 0.72 us -> 0.04 us
    ppermute x12 -> x15, waiting for transfers between devices: 18.2 us -> 10.9 us  [peer(): return lax.ppermute(block, axis, [(i, i ^ mask) for i in range(count)])]
    ppermute x2 -> x4, starting transfers between devices: 0.75 us -> 5.41 us  [pairwise(): return lax.ppermute(block, axis, pairs)]
    pallas_call x4 -> x8, Pallas kernels: 9.69 us -> 12 us  [the longest x2 4.13 us: local(): call(functools.partial(attention_kernel, chunk=c, sp_count=sp_count), sha...]
    ppermute x12 -> x15, starting transfers between devices: 13.7 us -> 12.4 us  [peer(): return lax.ppermute(block, axis, [(i, i ^ mask) for i in range(count)])]
    broadcast_in_dim x1 -> x0, local copies, waits for them, and re-layouts: 0.69 us -> none  [local(): norm_gain[None]]
  transfers between devices with their start and end apart: 14 -> 19, of which waited for: 8 -> 6; matrix products, arithmetic and copies ran while one was open for 2% -> 0% of each run, Pallas kernels for 1% -> 23%
where the time goes in v4:
time: 41.7 us; the launch traced here: 41.6 us
  starting transfers between devices  17.8 us (43%)
  Pallas kernels  12.6 us (30%)
  waiting for transfers between devices  10.9 us (26%)
    ppermute x15, starting transfers between devices, peer(): return lax.ppermute(block, axis, [(i, i ^ mask) for i in range(count)])  12.4 us
    ppermute x15, waiting for transfers between devices, peer(): return lax.ppermute(block, axis, [(i, i ^ mask) for i in range(count)])  10.9 us
    ppermute x4, starting transfers between devices, pairwise(): return lax.ppermute(block, axis, pairs)  5.41 us
    pallas_call x2, Pallas kernels, local(): call(functools.partial(attention_kernel, chunk=c, sp_count=sp_count), sha...  4.13 us
    pallas_call x1, Pallas kernels, local(): call(functools.partial(norm_kernel, tp_count=tp_count, chunks=chunks), (s...  2.99 us
    pallas_call x1, Pallas kernels, local(): call(modulation_kernel, shape_of((2 * MOD_ROWS + context.shape[0], cols),...  1.8 us
    pallas_call x1, Pallas kernels, local(): call(functools.partial(output_kernel, masks=masks, chunks=chunks), shape_...  1.32 us
  transfers between devices with their start and end apart: 19, of which 6 were waited for; matrix products, arithmetic and copies ran while one was open for 0% of the time, Pallas kernels for 23%

profile of v4, /device:TPU:0, one launch (start us, length us, event | category | flops | bytes accessed | tf_op | source)
XLA Modules:
  0.0 41.6 jit_solution(119821858798213957)
XLA Ops:
  0.0 1.8 %shard_map.127 = bf16[32,512]{1,0:T(8,128)(2,1)S(1)} custom-call(bf16[512]{0:T(512)(128)(2,1)} %cond_hbm.1, bf16[512]{0:T(512)(128)(2,1)} %ctx_hbm.1, bf16[512,512]{1,0:T(8,128)(2,1)} %w_shift_hbm.1, bf16[512,512]{1,0:T(8,128)(2,1)} %w_scale_hbm.1, bf16[512,512]{1,0:T(8,128)(2,1)} %w_gate_hbm.1, bf16[16,2048]{1,0:T(8,128)(2,1)} %context_hbm.1), custom_call_target="tpu_custom_call" | custom-call | tf_op jit(solution)/shard_map/pallas_call | solution.py:339
  1.8 5.1 %collective-permute-start = (bf16[32,512]{1,0:T(8,128)(2,1)S(1)}, bf16[32,512]{1,0:T(8,128)(2,1)S(1)}, u32[]{:S(2)}, u32[]{:S(2)}) collective-permute-start(bf16[32,512]{1,0:T(8,128)(2,1)S(1)} %shard_map.127), channel_id=1, source_target_pairs={{0,12},{4,8},{8,4},{12,0},{1,13},{5,9},{9,5},{13,1},{2,14},{6,10},... | collective-permute-start | bytes 98312 | tf_op jit(solution)/shard_map/ppermute | solution.py:54
  7.0 0.6 %collective-permute-start.2 = (bf16[32,512]{1,0:T(8,128)(2,1)S(1)}, bf16[32,512]{1,0:T(8,128)(2,1)S(1)}, u32[]{:S(2)}, u32[]{:S(2)}) collective-permute-start(bf16[32,512]{1,0:T(8,128)(2,1)S(1)} %shard_map.127), channel_id=1, source_target_pairs={{0,4},{4,0},{8,12},{12,8},{1,5},{5,1},{9,13},{13,9},{2,6},{6,2},{1... | collective-permute-start | bytes 98312 | tf_op jit(solution)/shard_map/ppermute | solution.py:54
  7.6 1.2 %collective-permute-done = bf16[32,512]{1,0:T(8,128)(2,1)S(1)} collective-permute-done((bf16[32,512]{1,0:T(8,128)(2,1)S(1)}, bf16[32,512]{1,0:T(8,128)(2,1)S(1)}, u32[]{:S(2)}, u32[]{:S(2)}) %collective-permute-start) | collective-permute-done | bytes 32800 | tf_op jit(solution)/shard_map/ppermute | solution.py:54
  8.9 2.9 %collective-permute-done.1 = bf16[32,512]{1,0:T(8,128)(2,1)S(1)} collective-permute-done((bf16[32,512]{1,0:T(8,128)(2,1)S(1)}, bf16[32,512]{1,0:T(8,128)(2,1)S(1)}, u32[]{:S(2)}, u32[]{:S(2)}) %collective-permute-start.1) | collective-permute-done | bytes 32800 | tf_op jit(solution)/shard_map/ppermute | solution.py:54
  11.8 1.6 %collective-permute-start.8 = (bf16[64,512]{1,0:T(8,128)(2,1)S(1)}, bf16[64,512]{1,0:T(8,128)(2,1)S(1)}, u32[]{:S(2)}, u32[]{:S(2)}) collective-permute-start(bf16[64,512]{1,0:T(8,128)(2,1)S(1)} %pad_maximum_fusion.refs_2_), channel_id=1, source_target_pairs={{0,2},{1,3},{2,0},{3,1},{4,6},{5,7},{6,4},{7,5},{8,10},{9,11},{10,... | collective-permute-start | bytes 196616 | tf_op jit(solution)/shard_map/ppermute | solution.py:54
  13.4 0.1 collective-permute-start.3
  13.4 0.6 %collective-permute-start.4 = (f32[8,512]{1,0:T(8,128)S(1)}, f32[8,512]{1,0:T(8,128)S(1)}, u32[]{:S(2)}, u32[]{:S(2)}) collective-permute-start(f32[8,512]{1,0:T(8,128)S(1)} %add_add_fusion.refs_4_.refs_1_), channel_id=1, source_target_pairs={{0,2},{1,3},{2,0},{3,1},{4,6},{5,7},{6,4},{7,5},{8,10},{9,11},{10,... | collective-permute-start | bytes 49160 | tf_op jit(solution)/shard_map/ppermute | solution.py:54
  14.0 1.2 %collective-permute-start.5 = (f32[8,512]{1,0:T(8,128)S(1)}, f32[8,512]{1,0:T(8,128)S(1)}, u32[]{:S(2)}, u32[]{:S(2)}) collective-permute-start(f32[8,512]{1,0:T(8,128)S(1)} %add_add_fusion.refs_4_.refs_1_), channel_id=1, source_target_pairs={{0,3},{1,2},{2,1},{3,0},{4,7},{5,6},{6,5},{7,4},{8,11},{9,10},{10,... | collective-permute-start | bytes 49160 | tf_op jit(solution)/shard_map/ppermute | solution.py:54
  15.3 0.4 collective-permute-start.9
  15.7 1.7 %collective-permute-done.4.refs_6_ = f32[8,512]{1,0:T(8,128)S(1)} collective-permute-done((f32[8,512]{1,0:T(8,128)S(1)}, f32[8,512]{1,0:T(8,128)S(1)}, u32[]{:S(2)}, u32[]{:S(2)}) %collective-permute-start.4) | collective-permute-done | bytes 16416 | tf_op jit(solution)/shard_map/ppermute | solution.py:54
  17.4 3.0 %shard_map.128 = (bf16[384,2048]{1,0:T(8,128)(2,1)S(1)}, bf16[384,256]{1,0:T(8,128)(2,1)S(1)}, bf16[256,256]{1,0:T(8,128)(2,1)S(1)}, bf16[256,256]{1,0:T(8,128)(...) custom-call(bf16[384,2048]{1,0:T(8,128)(2,1)S(1)} %copy-done, ...), custom_call_target="tpu_custom_call" | custom-call | tf_op jit(solution)/shard_map/pallas_call | solution.py:362
  20.4 0.6 %shard_map.133 = (bf16[384,256]{1,0:T(8,128)(2,1)S(1)}, bf16[256,256]{1,0:T(8,128)(2,1)S(1)}, bf16[256,256]{1,0:T(8,128)(2,1)S(1)}) custom-call(bf16[384,2048]{1,0:T(8,128)(2,1)S(1)} %get-tuple-element.20.normed_ref, bf16[2048,256]{1,0:T(8,128)(2,1)S(1)} %get-tuple-element.29.refs_7_.weight_ref), custom_call_target="tpu_custom_call" | custom-call | tf_op jit(solution)/shard_map/pallas_call | solution.py:378
  21.0 0.1 collective-permute-start.14
  21.1 0.8 %collective-permute-start.15 = (bf16[256,256]{1,0:T(8,128)(2,1)S(1)}, bf16[256,256]{1,0:T(8,128)(2,1)S(1)}, u32[]{:S(2)}, u32[]{:S(2)}) collective-permute-start(bf16[256,256]{1,0:T(8,128)(2,1)S(1)} %get-tuple-element.33), channel_id=1, source_target_pairs={{4,8},{8,4},{5,9},{9,5},{6,10},{10,6},{7,11},{11,7},{20,24},{24,20... | collective-permute-start | bytes 393224 | tf_op jit(solution)/shard_map/ppermute | solution.py:98
  21.9 3.9 %collective-permute-start.6 = (bf16[256,256]{1,0:T(8,128)(2,1)S(1)}, bf16[256,256]{1,0:T(8,128)(2,1)S(1)}, u32[]{:S(2)}, u32[]{:S(2)}) collective-permute-start(bf16[256,256]{1,0:T(8,128)(2,1)S(1)} %get-tuple-element.24), channel_id=1, source_target_pairs={{0,4},{4,0},{8,12},{12,8},{1,5},{5,1},{9,13},{13,9},{2,6},{6,2},{1... | collective-permute-start | bytes 393224 | tf_op jit(solution)/shard_map/ppermute | solution.py:98
  25.8 0.7 %collective-permute-start.7 = (bf16[256,256]{1,0:T(8,128)(2,1)S(1)}, bf16[256,256]{1,0:T(8,128)(2,1)S(1)}, u32[]{:S(2)}, u32[]{:S(2)}) collective-permute-start(bf16[256,256]{1,0:T(8,128)(2,1)S(1)} %get-tuple-element.25), channel_id=1, source_target_pairs={{4,8},{8,4},{5,9},{9,5},{6,10},{10,6},{7,11},{11,7},{20,24},{24,20... | collective-permute-start | bytes 393224 | tf_op jit(solution)/shard_map/ppermute | solution.py:98
  26.5 0.1 collective-permute-start.10
  26.6 0.1 pad_maximum_fusion.1.pairs_ref
  26.6 0.5 %shard_map.130.table_ref = f32[14,256,128]{2,1,0:T(8,128)S(1)} custom-call(f32[4,14,128]{2,1,0:T(8,128)S(1)} %pad_maximum_fusion.1.pairs_ref), custom_call_target="tpu_custom_call" | custom-call | tf_op jit(solution)/shard_map/pallas_call | solution.py:352
  27.2 0.6 %shard_map.129 = (bf16[384,256]{1,0:T(8,128)(2,1)S(1)}, bf16[384,512]{1,0:T(8,128)(2,1)S(1)}) custom-call(bf16[384,2048]{1,0:T(8,128)(2,1)S(1)} %get-tuple-element.20.normed_ref, bf16[2048,256]{1,0:T(8,128)(2,1)S(1)} %copy-done.2, bf16[384,2048]{1,0:T(8,128)(2,1)S(1)} %copy-done), custom_call_target="tpu_custom_call" | custom-call | tf_op jit(solution)/shard_map/pallas_call | solution.py:382
  27.8 0.0 collective-permute-done.10.refs_5_
  27.8 0.6 %shard_map.131 = (bf16[64,256]{1,0:T(8,128)(2,1)S(1)}, bf16[64,256]{1,0:T(8,128)(2,1)S(1)}) custom-call(f32[8,2048]{1,0:T(8,128)S(1)} %get-tuple-element.26.refs_0_, f32[8,2048]{1,0:T(8,128)S(1)} %get-tuple-element.27.refs_1_, bf16[64,512]{1,0:T(8,128)(2,1)S(1)} %pad_maximum_fusion.refs_2_, bf16[64,512]{1,0:T(8,128)(2,1)S(1)} %collective-permute-done.8.refs_3_, ...), custom_call_target="tpu_custom_call" | custom-call | tf_op jit(solution)/shard_map/pallas_call | solution.py:388
  28.4 2.1 %shard_map.134.refs_7_ = bf16[384,128]{1,0:T(8,128)(2,1)S(1)} custom-call(bf16[384,256]{1,0:T(8,128)(2,1)S(1)} %get-tuple-element.22.q_ref, bf16[384,256]{1,0:T(8,128)(2,1)S(1)} %get-tuple-element.31.kv_ref, bf16[256,256]{1,0:T(8,128)(2,1)S(1)} %collective-permute-done.14.recv_a_ref, bf16[256,256]{1,0:T(8,128)(2,1)S(1)} %collective-permute-done.15.recv_b_ref, ...), custom_call_target="tpu_custom_call" | custom-call | tf_op jit(solution)/shard_map/pallas_call | solution.py:396
  30.5 1.4 %collective-permute-start.16 = (bf16[384,128]{1,0:T(8,128)(2,1)S(1)}, bf16[384,128]{1,0:T(8,128)(2,1)S(1)}, u32[]{:S(2)}, u32[]{:S(2)}) collective-permute-start(bf16[384,128]{1,0:T(8,128)(2,1)S(1)} %shard_map.134.refs_7_), channel_id=1, source_target_pairs={{0,2},{1,3},{2,0},{3,1},{4,6},{5,7},{6,4},{7,5},{8,10},{9,11},{10,... | collective-permute-start | bytes 294920 | tf_op jit(solution)/shard_map/ppermute | solution.py:54
  31.9 2.1 %shard_map.132.refs_3_ = bf16[384,128]{1,0:T(8,128)(2,1)S(1)} custom-call(bf16[384,256]{1,0:T(8,128)(2,1)S(1)} %get-tuple-element.22.q_ref, bf16[384,256]{1,0:T(8,128)(2,1)S(1)} %get-tuple-element.23.kv_ref, bf16[256,256]{1,0:T(8,128)(2,1)S(1)} %collective-permute-done.6.recv_a_ref, bf16[256,256]{1,0:T(8,128)(2,1)S(1)} %collective-permute-done.7.recv_b_ref, ...), custom_call_target="tpu_custom_call" | custom-call | tf_op jit(solution)/shard_map/pallas_call | solution.py:396
  34.0 0.8 %collective-permute-start.11 = (bf16[384,128]{1,0:T(8,128)(2,1)S(1)}, bf16[384,128]{1,0:T(8,128)(2,1)S(1)}, u32[]{:S(2)}, u32[]{:S(2)}) collective-permute-start(bf16[384,128]{1,0:T(8,128)(2,1)S(1)} %shard_map.132.refs_3_), channel_id=1, source_target_pairs={{0,2},{1,3},{2,0},{3,1},{4,6},{5,7},{6,4},{7,5},{8,10},{9,11},{10,... | collective-permute-start | bytes 294920 | tf_op jit(solution)/shard_map/ppermute | solution.py:54
  34.7 0.5 %collective-permute-start.12 = (bf16[384,128]{1,0:T(8,128)(2,1)S(1)}, bf16[384,128]{1,0:T(8,128)(2,1)S(1)}, u32[]{:S(2)}, u32[]{:S(2)}) collective-permute-start(bf16[384,128]{1,0:T(8,128)(2,1)S(1)} %shard_map.132.refs_3_), channel_id=1, source_target_pairs={{0,1},{1,0},{2,3},{3,2},{4,5},{5,4},{6,7},{7,6},{8,9},{9,8},{10,11... | collective-permute-start | bytes 294920 | tf_op jit(solution)/shard_map/ppermute | solution.py:54
  35.2 0.5 %collective-permute-done.16.refs_8_ = bf16[384,128]{1,0:T(8,128)(2,1)S(1)} collective-permute-done((bf16[384,128]{1,0:T(8,128)(2,1)S(1)}, bf16[384,128]{1,0:T(8,128)(2,1)S(1)}, u32[]{:S(2)}, u32[]{:S(2)}) %collective-permute-start.16) | collective-permute-done | bytes 98336 | tf_op jit(solution)/shard_map/ppermute | solution.py:54
  35.8 3.2 %collective-permute-done.11.refs_4_ = bf16[384,128]{1,0:T(8,128)(2,1)S(1)} collective-permute-done((bf16[384,128]{1,0:T(8,128)(2,1)S(1)}, bf16[384,128]{1,0:T(8,128)(2,1)S(1)}, u32[]{:S(2)}, u32[]{:S(2)}) %collective-permute-start.11) | collective-permute-done | bytes 98336 | tf_op jit(solution)/shard_map/ppermute | solution.py:54
  39.0 1.3 %collective-permute-done.13.refs_6_ = bf16[384,128]{1,0:T(8,128)(2,1)S(1)} collective-permute-done((bf16[384,128]{1,0:T(8,128)(2,1)S(1)}, bf16[384,128]{1,0:T(8,128)(2,1)S(1)}, u32[]{:S(2)}, u32[]{:S(2)}) %collective-permute-start.13) | collective-permute-done | bytes 98336 | tf_op jit(solution)/shard_map/ppermute | solution.py:54
  40.2 1.3 %shard_map.135 = bf16[384,512]{1,0:T(8,128)(2,1)} custom-call(bf16[384,512]{1,0:T(8,128)(2,1)S(1)} %get-tuple-element.21.refs_0_, f32[8,512]{1,0:T(8,128)S(1)} %add_add_fusion.refs_4_.refs_1_, bf16[1024,512]{1,0:T(8,128)(2,1)S(1)} %copy-done.1, bf16[384,128]{1,0:T(8,128)(2,1)S(1)} %shard_map.132.refs_3_, ...), custom_call_target="tpu_custom_call" | custom-call | tf_op jit(solution)/shard_map/pallas_call | solution.py:405
  (32 shorter events, 0.1 us)
Async XLA Ops:
  0.0 15.3 %copy-start.3 = (f32[4,15,31]{2,0,1:T(4,128)S(1)}, f32[4,15,31]{2,0,1:T(4,128)}, u32[]{:S(2)}) copy-start(f32[4,15,31]{2,0,1:T(4,128)} %param.24) | copy-start | bytes 22324
  0.0 17.4 %copy-start = (bf16[384,2048]{1,0:T(8,128)(2,1)S(1)}, bf16[384,2048]{1,0:T(8,128)(2,1)}, u32[]{:S(2)}) copy-start(bf16[384,2048]{1,0:T(8,128)(2,1)} %latent_ref.1) | copy-start | bytes 4718596
  1.8 7.0 %collective-permute-start = (bf16[32,512]{1,0:T(8,128)(2,1)S(1)}, bf16[32,512]{1,0:T(8,128)(2,1)S(1)}, u32[]{:S(2)}, u32[]{:S(2)}) collective-permute-start(bf16[32,512]{1,0:T(8,128)(2,1)S(1)} %shard_map.127), channel_id=1, source_target_pairs={{0,12},{4,8},{8,4},{12,0},{1,13},{5,9},{9,5},{13,1},{2,14},{6,10},... | collective-permute-start | bytes 98312 | tf_op jit(solution)/shard_map/ppermute | solution.py:54
  7.0 4.8 %collective-permute-start.1 = (bf16[32,512]{1,0:T(8,128)(2,1)S(1)}, bf16[32,512]{1,0:T(8,128)(2,1)S(1)}, u32[]{:S(2)}, u32[]{:S(2)}) collective-permute-start(bf16[32,512]{1,0:T(8,128)(2,1)S(1)} %shard_map.127), channel_id=1, source_target_pairs={{0,8},{4,12},{8,0},{12,4},{1,9},{5,13},{9,1},{13,5},{2,10},{6,14},... | collective-permute-start | bytes 98312 | tf_op jit(solution)/shard_map/ppermute | solution.py:54
  7.0 4.8 %collective-permute-start.2 = (bf16[32,512]{1,0:T(8,128)(2,1)S(1)}, bf16[32,512]{1,0:T(8,128)(2,1)S(1)}, u32[]{:S(2)}, u32[]{:S(2)}) collective-permute-start(bf16[32,512]{1,0:T(8,128)(2,1)S(1)} %shard_map.127), channel_id=1, source_target_pairs={{0,4},{4,0},{8,12},{12,8},{1,5},{5,1},{9,13},{13,9},{2,6},{6,2},{1... | collective-permute-start | bytes 98312 | tf_op jit(solution)/shard_map/ppermute | solution.py:54
  11.8 14.0 %collective-permute-start.8 = (bf16[64,512]{1,0:T(8,128)(2,1)S(1)}, bf16[64,512]{1,0:T(8,128)(2,1)S(1)}, u32[]{:S(2)}, u32[]{:S(2)}) collective-permute-start(bf16[64,512]{1,0:T(8,128)(2,1)S(1)} %pad_maximum_fusion.refs_2_), channel_id=1, source_target_pairs={{0,2},{1,3},{2,0},{3,1},{4,6},{5,7},{6,4},{7,5},{8,10},{9,11},{10,... | collective-permute-start | bytes 196616 | tf_op jit(solution)/shard_map/ppermute | solution.py:54
  13.4 2.3 %collective-permute-start.3 = (f32[8,512]{1,0:T(8,128)S(1)}, f32[8,512]{1,0:T(8,128)S(1)}, u32[]{:S(2)}, u32[]{:S(2)}) collective-permute-start(f32[8,512]{1,0:T(8,128)S(1)} %add_add_fusion.refs_4_.refs_1_), channel_id=1, source_target_pairs={{0,1},{1,0},{2,3},{3,2},{4,5},{5,4},{6,7},{7,6},{8,9},{9,8},{10,11... | collective-permute-start | bytes 49160 | tf_op jit(solution)/shard_map/ppermute | solution.py:54
  13.4 3.9 %collective-permute-start.4 = (f32[8,512]{1,0:T(8,128)S(1)}, f32[8,512]{1,0:T(8,128)S(1)}, u32[]{:S(2)}, u32[]{:S(2)}) collective-permute-start(f32[8,512]{1,0:T(8,128)S(1)} %add_add_fusion.refs_4_.refs_1_), channel_id=1, source_target_pairs={{0,2},{1,3},{2,0},{3,1},{4,6},{5,7},{6,4},{7,5},{8,10},{9,11},{10,... | collective-permute-start | bytes 49160 | tf_op jit(solution)/shard_map/ppermute | solution.py:54
  14.0 3.3 %collective-permute-start.5 = (f32[8,512]{1,0:T(8,128)S(1)}, f32[8,512]{1,0:T(8,128)S(1)}, u32[]{:S(2)}, u32[]{:S(2)}) collective-permute-start(f32[8,512]{1,0:T(8,128)S(1)} %add_add_fusion.refs_4_.refs_1_), channel_id=1, source_target_pairs={{0,3},{1,2},{2,1},{3,0},{4,7},{5,6},{6,5},{7,4},{8,11},{9,10},{10,... | collective-permute-start | bytes 49160 | tf_op jit(solution)/shard_map/ppermute | solution.py:54
  15.3 11.2 %collective-permute-start.9 = (bf16[64,512]{1,0:T(8,128)(2,1)S(1)}, bf16[64,512]{1,0:T(8,128)(2,1)S(1)}, u32[]{:S(2)}, u32[]{:S(2)}) collective-permute-start(bf16[64,512]{1,0:T(8,128)(2,1)S(1)} %pad_maximum_fusion.refs_2_), channel_id=1, source_target_pairs={{0,1},{1,0},{2,3},{3,2},{4,5},{5,4},{6,7},{7,6},{8,9},{9,8},{10,11... | collective-permute-start | bytes 196616 | tf_op jit(solution)/shard_map/ppermute | solution.py:54
  21.0 6.2 %copy-start.2 = (bf16[2048,256]{1,0:T(8,128)(2,1)S(1)}, bf16[2048,256]{1,0:T(8,128)(2,1)}, u32[]{:S(2)}) copy-start(bf16[2048,256]{1,0:T(8,128)(2,1)} %wq_ref.1) | copy-start | bytes 3145732
  21.0 7.4 %collective-permute-start.14 = (bf16[256,256]{1,0:T(8,128)(2,1)S(1)}, bf16[256,256]{1,0:T(8,128)(2,1)S(1)}, u32[]{:S(2)}, u32[]{:S(2)}) collective-permute-start(bf16[256,256]{1,0:T(8,128)(2,1)S(1)} %get-tuple-element.32), channel_id=1, source_target_pairs={{0,4},{4,0},{8,12},{12,8},{1,5},{5,1},{9,13},{13,9},{2,6},{6,2},{1... | collective-permute-start | bytes 393224 | tf_op jit(solution)/shard_map/ppermute | solution.py:98
  21.1 7.3 %collective-permute-start.15 = (bf16[256,256]{1,0:T(8,128)(2,1)S(1)}, bf16[256,256]{1,0:T(8,128)(2,1)S(1)}, u32[]{:S(2)}, u32[]{:S(2)}) collective-permute-start(bf16[256,256]{1,0:T(8,128)(2,1)S(1)} %get-tuple-element.33), channel_id=1, source_target_pairs={{4,8},{8,4},{5,9},{9,5},{6,10},{10,6},{7,11},{11,7},{20,24},{24,20... | collective-permute-start | bytes 393224 | tf_op jit(solution)/shard_map/ppermute | solution.py:98
  21.9 10.0 %collective-permute-start.6 = (bf16[256,256]{1,0:T(8,128)(2,1)S(1)}, bf16[256,256]{1,0:T(8,128)(2,1)S(1)}, u32[]{:S(2)}, u32[]{:S(2)}) collective-permute-start(bf16[256,256]{1,0:T(8,128)(2,1)S(1)} %get-tuple-element.24), channel_id=1, source_target_pairs={{0,4},{4,0},{8,12},{12,8},{1,5},{5,1},{9,13},{13,9},{2,6},{6,2},{1... | collective-permute-start | bytes 393224 | tf_op jit(solution)/shard_map/ppermute | solution.py:98
  25.8 6.1 %collective-permute-start.7 = (bf16[256,256]{1,0:T(8,128)(2,1)S(1)}, bf16[256,256]{1,0:T(8,128)(2,1)S(1)}, u32[]{:S(2)}, u32[]{:S(2)}) collective-permute-start(bf16[256,256]{1,0:T(8,128)(2,1)S(1)} %get-tuple-element.25), channel_id=1, source_target_pairs={{4,8},{8,4},{5,9},{9,5},{6,10},{10,6},{7,11},{11,7},{20,24},{24,20... | collective-permute-start | bytes 393224 | tf_op jit(solution)/shard_map/ppermute | solution.py:98
  26.5 1.3 %collective-permute-start.10 = (bf16[64,512]{1,0:T(8,128)(2,1)S(1)}, bf16[64,512]{1,0:T(8,128)(2,1)S(1)}, u32[]{:S(2)}, u32[]{:S(2)}) collective-permute-start(bf16[64,512]{1,0:T(8,128)(2,1)S(1)} %collective-permute-done.8.refs_3_), channel_id=1, source_target_pairs={{0,1},{1,0},{2,3},{3,2},{4,5},{5,4},{6,7},{7,6},{8,9},{9,8},{10,11... | collective-permute-start | bytes 196616 | tf_op jit(solution)/shard_map/ppermute | solution.py:54
  30.5 9.7 %copy-start.1 = (bf16[1024,512]{1,0:T(8,128)(2,1)S(1)}, bf16[1024,512]{1,0:T(8,128)(2,1)}, u32[]{:S(2)}) copy-start(bf16[1024,512]{1,0:T(8,128)(2,1)} %refs_2_.3) | copy-start | bytes 3145732
  30.5 5.2 %collective-permute-start.16 = (bf16[384,128]{1,0:T(8,128)(2,1)S(1)}, bf16[384,128]{1,0:T(8,128)(2,1)S(1)}, u32[]{:S(2)}, u32[]{:S(2)}) collective-permute-start(bf16[384,128]{1,0:T(8,128)(2,1)S(1)} %shard_map.134.refs_7_), channel_id=1, source_target_pairs={{0,2},{1,3},{2,0},{3,1},{4,6},{5,7},{6,4},{7,5},{8,10},{9,11},{10,... | collective-permute-start | bytes 294920 | tf_op jit(solution)/shard_map/ppermute | solution.py:54
  34.0 5.0 %collective-permute-start.11 = (bf16[384,128]{1,0:T(8,128)(2,1)S(1)}, bf16[384,128]{1,0:T(8,128)(2,1)S(1)}, u32[]{:S(2)}, u32[]{:S(2)}) collective-permute-start(bf16[384,128]{1,0:T(8,128)(2,1)S(1)} %shard_map.132.refs_3_), channel_id=1, source_target_pairs={{0,2},{1,3},{2,0},{3,1},{4,6},{5,7},{6,4},{7,5},{8,10},{9,11},{10,... | collective-permute-start | bytes 294920 | tf_op jit(solution)/shard_map/ppermute | solution.py:54
  34.7 4.2 %collective-permute-start.17 = (bf16[384,128]{1,0:T(8,128)(2,1)S(1)}, bf16[384,128]{1,0:T(8,128)(2,1)S(1)}, u32[]{:S(2)}, u32[]{:S(2)}) collective-permute-start(bf16[384,128]{1,0:T(8,128)(2,1)S(1)} %shard_map.134.refs_7_), channel_id=1, source_target_pairs={{0,1},{1,0},{2,3},{3,2},{4,5},{5,4},{6,7},{7,6},{8,9},{9,8},{10,11... | collective-permute-start | bytes 294920 | tf_op jit(solution)/shard_map/ppermute | solution.py:54
  34.7 4.2 %collective-permute-start.12 = (bf16[384,128]{1,0:T(8,128)(2,1)S(1)}, bf16[384,128]{1,0:T(8,128)(2,1)S(1)}, u32[]{:S(2)}, u32[]{:S(2)}) collective-permute-start(bf16[384,128]{1,0:T(8,128)(2,1)S(1)} %shard_map.132.refs_3_), channel_id=1, source_target_pairs={{0,1},{1,0},{2,3},{3,2},{4,5},{5,4},{6,7},{7,6},{8,9},{9,8},{10,11... | collective-permute-start | bytes 294920 | tf_op jit(solution)/shard_map/ppermute | solution.py:54
  35.7 3.2 %collective-permute-start.18 = (bf16[384,128]{1,0:T(8,128)(2,1)S(1)}, bf16[384,128]{1,0:T(8,128)(2,1)S(1)}, u32[]{:S(2)}, u32[]{:S(2)}) collective-permute-start(bf16[384,128]{1,0:T(8,128)(2,1)S(1)} %collective-permute-done.16.refs_8_), channel_id=1, source_target_pairs={{0,1},{1,0},{2,3},{3,2},{4,5},{5,4},{6,7},{7,6},{8,9},{9,8},{10,11... | collective-permute-start | bytes 294920 | tf_op jit(solution)/shard_map/ppermute | solution.py:54
  38.9 1.3 %collective-permute-start.13 = (bf16[384,128]{1,0:T(8,128)(2,1)S(1)}, bf16[384,128]{1,0:T(8,128)(2,1)S(1)}, u32[]{:S(2)}, u32[]{:S(2)}) collective-permute-start(bf16[384,128]{1,0:T(8,128)(2,1)S(1)} %collective-permute-done.11.refs_4_), channel_id=1, source_target_pairs={{0,1},{1,0},{2,3},{3,2},{4,5},{5,4},{6,7},{7,6},{8,9},{9,8},{10,11... | collective-permute-start | bytes 294920 | tf_op jit(solution)/shard_map/ppermute | solution.py:54

commit v5 on v4

--- a/solution.py
+++ b/solution.py
@@ -139,22 +139,27 @@
     out_ref[2 * MOD_ROWS :, :] = context_ref[...]
 
 
-def bias_kernel(pairs_ref, out_ref, *, heads):
-    query = lax.broadcasted_iota(jnp.int32, (GRID_W, 2 * GRID_W), 0)
-    key = lax.broadcasted_iota(jnp.int32, (GRID_W, 2 * GRID_W), 1) % GRID_W
+def bias_table(vectors_ref, out_ref):
+    lanes = out_ref.shape[1]
+    key = lax.broadcasted_iota(jnp.int32, (GRID_W, lanes), 0)
+    query = lax.broadcasted_iota(jnp.int32, (GRID_W, lanes), 1) % GRID_W
     first = jnp.clip(query - WIN_W // 2, 0, GRID_W - WIN_W)
     inside = (key >= first) & (key < first + WIN_W)
-    for h in range(heads):
-        for p in range(2 * WIN_H - 2):
-            row = pairs_ref[h, p : p + 1, :]
-            table = pltpu.roll(
-                jnp.broadcast_to(row, (GRID_W, 2 * GRID_W)),
-                2 * GRID_W - (WIN_W - 1),
-                1,
-                stride=1,
-                stride_axis=0,
-            )
-            out_ref[p, h * GRID_W : (h + 1) * GRID_W, :] = jnp.where(inside, table, MASKED)
+    for r in range(2 * WIN_H - 1):
+        table = pltpu.roll(
+            jnp.broadcast_to(vectors_ref[r : r + 1, :], (GRID_W, lanes)),
+            lanes - (WIN_W - 1),
+            1,
+            stride=1,
+            stride_axis=0,
+        )
+        out_ref[r * GRID_W : (r + 1) * GRID_W, :] = jnp.where(inside, table, MASKED)
+
+
+def bias_kernel(*refs):
+    half = len(refs) // 2
+    for vectors_ref, out_ref in zip(refs[:half], refs[half:]):
+        bias_table(vectors_ref, out_ref)
 
 
 def inverse_rms(floats):
@@ -247,52 +252,109 @@
 
 
 def attention_kernel(
-    q_ref, kv_ref, recv_a_ref, recv_b_ref, table_ref, ctx_ref, out_ref, pad_ref, *, chunk, sp_count
+    q_ref,
+    kv_ref,
+    recv_a_ref,
+    recv_b_ref,
+    table_ref,
+    ctx_ref,
+    out_ref,
+    pad_ref,
+    score_ref,
+    weight_ref,
+    *,
+    chunk,
+    sp_count,
 ):
     tokens, width = out_ref.shape
     heads = width // HEAD_DIM
     rows = tokens // GRID_W
     halo = HALO * GRID_W
+    groups, keys, _ = score_ref.shape
+    group = rows // groups
+    ctx_rows = ctx_ref.shape[0]
+    span = keys - ctx_rows
     sp_index = lax.axis_index("sp")
     odd = sp_index % 2
     far = halo + tokens
-    pad_ref[pl.ds(pl.multiple_of((1 - odd) * far, GRID_W), halo), :] = recv_a_ref[...]
-    pad_ref[pl.ds(pl.multiple_of(odd * far, GRID_W), halo), :] = recv_b_ref[...]
-    pad_ref[halo : halo + tokens, :] = kv_ref[...]
-    ctx_keys, ctx_values = ctx_ref[:, :width], ctx_ref[:, width:]
+    pad_ref[pl.ds(pl.multiple_of((1 - odd) * far, GRID_W), halo), : 2 * width] = recv_a_ref[...]
+    pad_ref[pl.ds(pl.multiple_of(odd * far, GRID_W), halo), : 2 * width] = recv_b_ref[...]
+    pad_ref[halo : halo + tokens, : 2 * width] = kv_ref[...]
+    pad_ref[:, 2 * width :] = jnp.ones((tokens + 2 * halo, width), BF16)
     lane_head = lax.broadcasted_iota(jnp.int32, (1, width), 1) // HEAD_DIM
     picks = [(lane_head == h) for h in range(heads)]
-    table_rows = slice(chunk * heads * GRID_W, (chunk + 1) * heads * GRID_W)
     nt = (((1,), (1,)), ((), ()))
-    for l in range(rows):
-        at = l * GRID_W
+    tn = (((0,), (0,)), ((), ()))
+
+    def start_of(l):
         grid_row = sp_index * rows + l
         first = jnp.clip(grid_row - HALO, 0, sp_count * rows - WIN_H)
-        start = first - sp_index * rows + HALO
-        offset = first - grid_row + WIN_H - 1
-        query = q_ref[at : at + GRID_W, chunk * width : (chunk + 1) * width]
-        left = jnp.concatenate([jnp.where(pick, query, BF16(0)) for pick in picks], axis=0)
-        window = pl.ds(pl.multiple_of(start * GRID_W, GRID_W), WIN_H * GRID_W)
-        scores = lax.dot_general(left, pad_ref[window, :width], nt, preferred_element_type=F32)
-        ctx_scores = lax.dot_general(left, ctx_keys, nt, preferred_element_type=F32)
-        bias = jnp.concatenate(
-            [table_ref[offset + 2 * k, table_rows, :] for k in range(WIN_H // 2)], axis=1
+        return first - sp_index * rows + HALO, first - grid_row + WIN_H - 1
+
+    def window_of(g):
+        return pl.ds(pl.multiple_of(start_of(g * group)[0] * GRID_W, GRID_W), span)
+
+    def score(g):
+        left = []
+        for l in range(g * group, (g + 1) * group):
+            query = q_ref[l * GRID_W : (l + 1) * GRID_W, chunk * width : (chunk + 1) * width]
+            left += [jnp.where(pick, query, BF16(0)) for pick in picks]
+        left = jnp.concatenate(left, axis=0)
+        score_ref[g, :span, :] = lax.dot_general(
+            pad_ref[window_of(g), :width], left, nt, preferred_element_type=F32
         )
-        scores = scores + bias
-        highest = jnp.maximum(
-            jnp.max(scores, axis=1, keepdims=True), jnp.max(ctx_scores, axis=1, keepdims=True)
+        score_ref[g, span:, :] = lax.dot_general(
+            ctx_ref[:, :width], left, nt, preferred_element_type=F32
         )
-        win_exp = jnp.exp(scores - highest)
-        ctx_exp = jnp.exp(ctx_scores - highest)
-        totals = jnp.sum(win_exp, axis=1, keepdims=True) + jnp.sum(ctx_exp, axis=1, keepdims=True)
-        mixed = jnp.dot(
-            win_exp.astype(BF16), pad_ref[window, width:], preferred_element_type=F32
-        ) + jnp.dot(ctx_exp.astype(BF16), ctx_values, preferred_element_type=F32)
-        mixed = mixed * (1.0 / totals)
-        result = mixed[:GRID_W]
-        for h in range(1, heads):
-            result = jnp.where(picks[h], mixed[h * GRID_W : (h + 1) * GRID_W], result)
-        out_ref[at : at + GRID_W, :] = result.astype(BF16)
+
+    def weigh(g):
+        for k in range(group):
+            start, offset = start_of(g * group + k)
+            shift = start - start_of(g * group)[0]
+            lanes = slice(k * width, (k + 1) * width)
+            highest = jnp.max(score_ref[g, span:, lanes], axis=0, keepdims=True)
+            blocks = []
+            for u in range(span // GRID_W):
+                row = jnp.clip(u - shift, 0, WIN_H - 1) + offset
+                block = table_ref[pl.ds(pl.multiple_of(row * GRID_W, GRID_W), GRID_W), :]
+                if u < k or u >= WIN_H:
+                    block = jnp.where((u >= shift) & (u < shift + WIN_H), block, MASKED)
+                block = block + score_ref[g, u * GRID_W : (u + 1) * GRID_W, lanes]
+                blocks.append(block)
+                highest = jnp.maximum(highest, jnp.max(block, axis=0, keepdims=True))
+            for u, block in enumerate(blocks):
+                weight_ref[g, u * GRID_W : (u + 1) * GRID_W, lanes] = jnp.exp(
+                    block - highest
+                ).astype(BF16)
+            weight_ref[g, span:, lanes] = jnp.exp(score_ref[g, span:, lanes] - highest).astype(BF16)
+
+    def mix(g):
+        ctx_values = jnp.concatenate(
+            [ctx_ref[:, width:], jnp.ones((ctx_rows, width), BF16)], axis=1
+        )
+        mixed = lax.dot_general(
+            weight_ref[g, :span, :],
+            pad_ref[window_of(g), width:],
+            tn,
+            preferred_element_type=F32,
+        ) + lax.dot_general(weight_ref[g, span:, :], ctx_values, tn, preferred_element_type=F32)
+        mixed = mixed[:, :width] / mixed[:, width:]
+        for k in range(group):
+            low = k * heads * GRID_W
+            result = mixed[low : low + GRID_W]
+            for h in range(1, heads):
+                low += GRID_W
+                result = jnp.where(picks[h], mixed[low : low + GRID_W], result)
+            l = g * group + k
+            out_ref[l * GRID_W : (l + 1) * GRID_W, :] = result.astype(BF16)
+
+    for g in range(groups):
+        score(g)
+    for g in range(groups):
+        weigh(g)
+        if g > 0:
+            mix(g - 1)
+    mix(groups - 1)
 
 
 def output_kernel(*refs, masks, chunks):
@@ -346,13 +408,14 @@
     mod_own, ctx_own = total_and_context(partial, "sp")
     mod_pieces = pieces_of(mod_own, "tp")
 
-    lanes = GRID_W - offset_bias.shape[2]
-    padded = jnp.pad(offset_bias, ((0, 0), (0, 0), (0, lanes)))
-    pairs = jnp.concatenate([padded[:, :-1], padded[:, 1:]], axis=2)
-    table = call(
-        functools.partial(bias_kernel, heads=heads),
-        shape_of((2 * WIN_H - 2, heads * GRID_W, 2 * GRID_W), F32),
-    )(pairs)
+    fill = GRID_W - offset_bias.shape[2]
+    flipped = jnp.pad(offset_bias[:, :, ::-1], ((0, 0), (0, 0), (0, fill)))
+    vectors = [
+        jnp.concatenate(list(flipped[c * heads // chunks : (c + 1) * heads // chunks]), axis=1)
+        for c in range(chunks)
+    ]
+    table_shape = shape_of(((2 * WIN_H - 1) * GRID_W, each), F32)
+    tables = call(bias_kernel, (table_shape,) * chunks)(*vectors)
 
     kv_shapes = (
         shape_of((tokens, 2 * each), BF16),
@@ -391,13 +454,20 @@
         scratch=[pltpu.VMEM((ctx_rows, model), BF16)],
     )(mod, gain, *[p for _, p in ctx_pieces], *weights)
 
+    rows = tokens // GRID_W
+    group = 2 if rows % 2 == 0 else 1
+    keys = (WIN_H + group - 1) * GRID_W + ctx_rows
     gathered = []
     for c in range(chunks):
         attended = call(
             functools.partial(attention_kernel, chunk=c, sp_count=sp_count),
             shape_of((tokens, each), BF16),
-            scratch=[pltpu.VMEM((tokens + 2 * halo, 2 * each), BF16)],
-        )(query, keys_values[c][0], *halos[c], table, ctx_all[c])
+            scratch=[
+                pltpu.VMEM((tokens + 2 * halo, 3 * each), BF16),
+                pltpu.VMEM((rows // group, keys, group * each), F32),
+                pltpu.VMEM((rows // group, keys, group * each), BF16),
+            ],
+        )(query, keys_values[c][0], *halos[c], tables[c], ctx_all[c])
         found = pieces_by_bits(attended, "tp")
         masks = [mask for mask, _ in found]
         gathered += [piece for _, piece in found]

time: 41.7 us -> 40 us (0.959)
  Pallas kernels: 12.6 us -> 11 us
    pallas_call x2, Pallas kernels: 4.13 us -> 2.8 us  [local(): call(functools.partial(attention_kernel, chunk=c, sp_count=sp_count), sha...]
  transfers between devices with their start and end apart: 19 -> 19, of which waited for: 6 -> 7; matrix products, arithmetic and copies ran while one was open for 0% -> 0% of each run, Pallas kernels for 23% -> 20%
where the time goes in v5:
time: 40 us; the launch traced here: 39.9 us
  starting transfers between devices  17.6 us (44%)
  Pallas kernels  11 us (28%)
  waiting for transfers between devices  10.8 us (27%)
    ppermute x15, starting transfers between devices, peer(): return lax.ppermute(block, axis, [(i, i ^ mask) for i in range(count)])  12.4 us
    ppermute x15, waiting for transfers between devices, peer(): return lax.ppermute(block, axis, [(i, i ^ mask) for i in range(count)])  10.8 us
    ppermute x4, starting transfers between devices, pairwise(): return lax.ppermute(block, axis, pairs)  5.28 us
    pallas_call x1, Pallas kernels, local(): call(functools.partial(norm_kernel, tp_count=tp_count, chunks=chunks), (s...  2.99 us
    pallas_call x2, Pallas kernels, local(): call(functools.partial(attention_kernel, chunk=c, sp_count=sp_count), sha...  2.8 us
    pallas_call x1, Pallas kernels, local(): call(modulation_kernel, shape_of((2 * MOD_ROWS + context.shape[0], cols),...  1.8 us
    pallas_call x1, Pallas kernels, local(): call(functools.partial(output_kernel, masks=masks, chunks=chunks), shape_...  1.32 us
  transfers between devices with their start and end apart: 19, of which 7 were waited for; matrix products, arithmetic and copies ran while one was open for 0% of the time, Pallas kernels for 20%

profile of v5, /device:TPU:0, one launch (start us, length us, event | category | flops | bytes accessed | tf_op | source)
XLA Modules:
  0.0 39.9 jit_solution(11927839948884799786)
XLA Ops:
  0.0 1.8 %shard_map.127 = bf16[32,512]{1,0:T(8,128)(2,1)S(1)} custom-call(bf16[512]{0:T(512)(128)(2,1)} %cond_hbm.1, bf16[512]{0:T(512)(128)(2,1)} %ctx_hbm.1, bf16[512,512]{1,0:T(8,128)(2,1)} %w_shift_hbm.1, bf16[512,512]{1,0:T(8,128)(2,1)} %w_scale_hbm.1, bf16[512,512]{1,0:T(8,128)(2,1)} %w_gate_hbm.1, bf16[16,2048]{1,0:T(8,128)(2,1)} %context_hbm.1), custom_call_target="tpu_custom_call" | custom-call | tf_op jit(solution)/shard_map/pallas_call | solution.py:401
  1.8 5.1 %collective-permute-start = (bf16[32,512]{1,0:T(8,128)(2,1)S(1)}, bf16[32,512]{1,0:T(8,128)(2,1)S(1)}, u32[]{:S(2)}, u32[]{:S(2)}) collective-permute-start(bf16[32,512]{1,0:T(8,128)(2,1)S(1)} %shard_map.127), channel_id=1, source_target_pairs={{0,12},{4,8},{8,4},{12,0},{1,13},{5,9},{9,5},{13,1},{2,14},{6,10},... | collective-permute-start | bytes 98312 | tf_op jit(solution)/shard_map/ppermute | solution.py:54
  7.0 0.6 %collective-permute-start.2 = (bf16[32,512]{1,0:T(8,128)(2,1)S(1)}, bf16[32,512]{1,0:T(8,128)(2,1)S(1)}, u32[]{:S(2)}, u32[]{:S(2)}) collective-permute-start(bf16[32,512]{1,0:T(8,128)(2,1)S(1)} %shard_map.127), channel_id=1, source_target_pairs={{0,4},{4,0},{8,12},{12,8},{1,5},{5,1},{9,13},{13,9},{2,6},{6,2},{1... | collective-permute-start | bytes 98312 | tf_op jit(solution)/shard_map/ppermute | solution.py:54
  7.6 1.2 %collective-permute-done = bf16[32,512]{1,0:T(8,128)(2,1)S(1)} collective-permute-done((bf16[32,512]{1,0:T(8,128)(2,1)S(1)}, bf16[32,512]{1,0:T(8,128)(2,1)S(1)}, u32[]{:S(2)}, u32[]{:S(2)}) %collective-permute-start) | collective-permute-done | bytes 32800 | tf_op jit(solution)/shard_map/ppermute | solution.py:54
  8.9 2.9 %collective-permute-done.1 = bf16[32,512]{1,0:T(8,128)(2,1)S(1)} collective-permute-done((bf16[32,512]{1,0:T(8,128)(2,1)S(1)}, bf16[32,512]{1,0:T(8,128)(2,1)S(1)}, u32[]{:S(2)}, u32[]{:S(2)}) %collective-permute-start.1) | collective-permute-done | bytes 32800 | tf_op jit(solution)/shard_map/ppermute | solution.py:54
  11.8 1.6 %collective-permute-start.8 = (bf16[64,512]{1,0:T(8,128)(2,1)S(1)}, bf16[64,512]{1,0:T(8,128)(2,1)S(1)}, u32[]{:S(2)}, u32[]{:S(2)}) collective-permute-start(bf16[64,512]{1,0:T(8,128)(2,1)S(1)} %pad_maximum_fusion.refs_2_), channel_id=1, source_target_pairs={{0,2},{1,3},{2,0},{3,1},{4,6},{5,7},{6,4},{7,5},{8,10},{9,11},{10,... | collective-permute-start | bytes 196616 | tf_op jit(solution)/shard_map/ppermute | solution.py:54
  13.4 0.6 %collective-permute-start.4 = (f32[8,512]{1,0:T(8,128)S(1)}, f32[8,512]{1,0:T(8,128)S(1)}, u32[]{:S(2)}, u32[]{:S(2)}) collective-permute-start(f32[8,512]{1,0:T(8,128)S(1)} %add_add_fusion.refs_4_.refs_1_), channel_id=1, source_target_pairs={{0,2},{1,3},{2,0},{3,1},{4,6},{5,7},{6,4},{7,5},{8,10},{9,11},{10,... | collective-permute-start | bytes 49160 | tf_op jit(solution)/shard_map/ppermute | solution.py:54
  14.0 1.2 %collective-permute-start.5 = (f32[8,512]{1,0:T(8,128)S(1)}, f32[8,512]{1,0:T(8,128)S(1)}, u32[]{:S(2)}, u32[]{:S(2)}) collective-permute-start(f32[8,512]{1,0:T(8,128)S(1)} %add_add_fusion.refs_4_.refs_1_), channel_id=1, source_target_pairs={{0,3},{1,2},{2,1},{3,0},{4,7},{5,6},{6,5},{7,4},{8,11},{9,10},{10,... | collective-permute-start | bytes 49160 | tf_op jit(solution)/shard_map/ppermute | solution.py:54
  15.3 0.1 rev.3
  15.4 0.4 collective-permute-start.9
  15.7 1.6 %collective-permute-done.4.refs_6_ = f32[8,512]{1,0:T(8,128)S(1)} collective-permute-done((f32[8,512]{1,0:T(8,128)S(1)}, f32[8,512]{1,0:T(8,128)S(1)}, u32[]{:S(2)}, u32[]{:S(2)}) %collective-permute-start.4) | collective-permute-done | bytes 16416 | tf_op jit(solution)/shard_map/ppermute | solution.py:54
  17.4 3.0 %shard_map.128 = (bf16[384,2048]{1,0:T(8,128)(2,1)S(1)}, bf16[384,256]{1,0:T(8,128)(2,1)S(1)}, bf16[256,256]{1,0:T(8,128)(2,1)S(1)}, bf16[256,256]{1,0:T(8,128)(...) custom-call(bf16[384,2048]{1,0:T(8,128)(2,1)S(1)} %copy-done, ...), custom_call_target="tpu_custom_call" | custom-call | tf_op jit(solution)/shard_map/pallas_call | solution.py:425
  20.4 0.6 %shard_map.133 = (bf16[384,256]{1,0:T(8,128)(2,1)S(1)}, bf16[256,256]{1,0:T(8,128)(2,1)S(1)}, bf16[256,256]{1,0:T(8,128)(2,1)S(1)}) custom-call(bf16[384,2048]{1,0:T(8,128)(2,1)S(1)} %get-tuple-element.22.normed_ref, bf16[2048,256]{1,0:T(8,128)(2,1)S(1)} %get-tuple-element.32.refs_7_.weight_ref), custom_call_target="tpu_custom_call" | custom-call | tf_op jit(solution)/shard_map/pallas_call | solution.py:441
  21.0 0.1 collective-permute-start.14
  21.1 0.7 %collective-permute-start.15 = (bf16[256,256]{1,0:T(8,128)(2,1)S(1)}, bf16[256,256]{1,0:T(8,128)(2,1)S(1)}, u32[]{:S(2)}, u32[]{:S(2)}) collective-permute-start(bf16[256,256]{1,0:T(8,128)(2,1)S(1)} %get-tuple-element.36), channel_id=1, source_target_pairs={{4,8},{8,4},{5,9},{9,5},{6,10},{10,6},{7,11},{11,7},{20,24},{24,20... | collective-permute-start | bytes 393224 | tf_op jit(solution)/shard_map/ppermute | solution.py:98
  21.8 3.9 %collective-permute-start.6 = (bf16[256,256]{1,0:T(8,128)(2,1)S(1)}, bf16[256,256]{1,0:T(8,128)(2,1)S(1)}, u32[]{:S(2)}, u32[]{:S(2)}) collective-permute-start(bf16[256,256]{1,0:T(8,128)(2,1)S(1)} %get-tuple-element.26), channel_id=1, source_target_pairs={{0,4},{4,0},{8,12},{12,8},{1,5},{5,1},{9,13},{13,9},{2,6},{6,2},{1... | collective-permute-start | bytes 393224 | tf_op jit(solution)/shard_map/ppermute | solution.py:98
  25.7 0.7 %collective-permute-start.7 = (bf16[256,256]{1,0:T(8,128)(2,1)S(1)}, bf16[256,256]{1,0:T(8,128)(2,1)S(1)}, u32[]{:S(2)}, u32[]{:S(2)}) collective-permute-start(bf16[256,256]{1,0:T(8,128)(2,1)S(1)} %get-tuple-element.27), channel_id=1, source_target_pairs={{4,8},{8,4},{5,9},{9,5},{6,10},{10,6},{7,11},{11,7},{20,24},{24,20... | collective-permute-start | bytes 393224 | tf_op jit(solution)/shard_map/ppermute | solution.py:98
  26.4 0.1 collective-permute-start.10
  26.4 0.1 pad_maximum_fusion.1
  26.5 0.3 shard_map.130
  26.8 0.6 %shard_map.129 = (bf16[384,256]{1,0:T(8,128)(2,1)S(1)}, bf16[384,512]{1,0:T(8,128)(2,1)S(1)}) custom-call(bf16[384,2048]{1,0:T(8,128)(2,1)S(1)} %get-tuple-element.22.normed_ref, bf16[2048,256]{1,0:T(8,128)(2,1)S(1)} %copy-done.2, bf16[384,2048]{1,0:T(8,128)(2,1)S(1)} %copy-done), custom_call_target="tpu_custom_call" | custom-call | tf_op jit(solution)/shard_map/pallas_call | solution.py:445
  27.4 0.2 collective-permute-done.10.refs_5_
  27.7 0.6 %shard_map.131 = (bf16[64,256]{1,0:T(8,128)(2,1)S(1)}, bf16[64,256]{1,0:T(8,128)(2,1)S(1)}) custom-call(f32[8,2048]{1,0:T(8,128)S(1)} %get-tuple-element.29.refs_0_, f32[8,2048]{1,0:T(8,128)S(1)} %get-tuple-element.30.refs_1_, bf16[64,512]{1,0:T(8,128)(2,1)S(1)} %pad_maximum_fusion.refs_2_, bf16[64,512]{1,0:T(8,128)(2,1)S(1)} %collective-permute-done.8.refs_3_, ...), custom_call_target="tpu_custom_call" | custom-call | tf_op jit(solution)/shard_map/pallas_call | solution.py:451
  28.3 1.4 %shard_map.134.refs_7_ = bf16[384,128]{1,0:T(8,128)(2,1)S(1)} custom-call(bf16[384,256]{1,0:T(8,128)(2,1)S(1)} %get-tuple-element.24.q_ref, bf16[384,256]{1,0:T(8,128)(2,1)S(1)} %get-tuple-element.34.kv_ref, bf16[256,256]{1,0:T(8,128)(2,1)S(1)} %collective-permute-done.14.recv_a_ref, bf16[256,256]{1,0:T(8,128)(2,1)S(1)} %collective-permute-done.15.recv_b_ref, ...), custom_call_target="tpu_custom_call" | custom-call | tf_op jit(solution)/shard_map/pallas_call | solution.py:462
  29.7 1.4 %collective-permute-start.16 = (bf16[384,128]{1,0:T(8,128)(2,1)S(1)}, bf16[384,128]{1,0:T(8,128)(2,1)S(1)}, u32[]{:S(2)}, u32[]{:S(2)}) collective-permute-start(bf16[384,128]{1,0:T(8,128)(2,1)S(1)} %shard_map.134.refs_7_), channel_id=1, source_target_pairs={{0,2},{1,3},{2,0},{3,1},{4,6},{5,7},{6,4},{7,5},{8,10},{9,11},{10,... | collective-permute-start | bytes 294920 | tf_op jit(solution)/shard_map/ppermute | solution.py:54
  31.1 1.4 %shard_map.132.refs_3_ = bf16[384,128]{1,0:T(8,128)(2,1)S(1)} custom-call(bf16[384,256]{1,0:T(8,128)(2,1)S(1)} %get-tuple-element.24.q_ref, bf16[384,256]{1,0:T(8,128)(2,1)S(1)} %get-tuple-element.25.kv_ref, bf16[256,256]{1,0:T(8,128)(2,1)S(1)} %collective-permute-done.6.recv_a_ref, bf16[256,256]{1,0:T(8,128)(2,1)S(1)} %collective-permute-done.7.recv_b_ref, ...), custom_call_target="tpu_custom_call" | custom-call | tf_op jit(solution)/shard_map/pallas_call | solution.py:462
  32.5 0.8 %collective-permute-start.11 = (bf16[384,128]{1,0:T(8,128)(2,1)S(1)}, bf16[384,128]{1,0:T(8,128)(2,1)S(1)}, u32[]{:S(2)}, u32[]{:S(2)}) collective-permute-start(bf16[384,128]{1,0:T(8,128)(2,1)S(1)} %shard_map.132.refs_3_), channel_id=1, source_target_pairs={{0,2},{1,3},{2,0},{3,1},{4,6},{5,7},{6,4},{7,5},{8,10},{9,11},{10,... | collective-permute-start | bytes 294920 | tf_op jit(solution)/shard_map/ppermute | solution.py:54
  33.3 0.5 %collective-permute-start.12 = (bf16[384,128]{1,0:T(8,128)(2,1)S(1)}, bf16[384,128]{1,0:T(8,128)(2,1)S(1)}, u32[]{:S(2)}, u32[]{:S(2)}) collective-permute-start(bf16[384,128]{1,0:T(8,128)(2,1)S(1)} %shard_map.132.refs_3_), channel_id=1, source_target_pairs={{0,1},{1,0},{2,3},{3,2},{4,5},{5,4},{6,7},{7,6},{8,9},{9,8},{10,11... | collective-permute-start | bytes 294920 | tf_op jit(solution)/shard_map/ppermute | solution.py:54
  33.8 0.9 %collective-permute-done.16.refs_8_ = bf16[384,128]{1,0:T(8,128)(2,1)S(1)} collective-permute-done((bf16[384,128]{1,0:T(8,128)(2,1)S(1)}, bf16[384,128]{1,0:T(8,128)(2,1)S(1)}, u32[]{:S(2)}, u32[]{:S(2)}) %collective-permute-start.16) | collective-permute-done | bytes 98336 | tf_op jit(solution)/shard_map/ppermute | solution.py:54
  34.7 2.5 %collective-permute-done.11.refs_4_ = bf16[384,128]{1,0:T(8,128)(2,1)S(1)} collective-permute-done((bf16[384,128]{1,0:T(8,128)(2,1)S(1)}, bf16[384,128]{1,0:T(8,128)(2,1)S(1)}, u32[]{:S(2)}, u32[]{:S(2)}) %collective-permute-start.11) | collective-permute-done | bytes 98336 | tf_op jit(solution)/shard_map/ppermute | solution.py:54
  37.3 1.3 %collective-permute-done.13.refs_6_ = bf16[384,128]{1,0:T(8,128)(2,1)S(1)} collective-permute-done((bf16[384,128]{1,0:T(8,128)(2,1)S(1)}, bf16[384,128]{1,0:T(8,128)(2,1)S(1)}, u32[]{:S(2)}, u32[]{:S(2)}) %collective-permute-start.13) | collective-permute-done | bytes 98336 | tf_op jit(solution)/shard_map/ppermute | solution.py:54
  38.5 1.3 %shard_map.135 = bf16[384,512]{1,0:T(8,128)(2,1)} custom-call(bf16[384,512]{1,0:T(8,128)(2,1)S(1)} %get-tuple-element.23.refs_0_, f32[8,512]{1,0:T(8,128)S(1)} %add_add_fusion.refs_4_.refs_1_, bf16[1024,512]{1,0:T(8,128)(2,1)S(1)} %copy-done.1, bf16[384,128]{1,0:T(8,128)(2,1)S(1)} %shard_map.132.refs_3_, ...), custom_call_target="tpu_custom_call" | custom-call | tf_op jit(solution)/shard_map/pallas_call | solution.py:475
  (33 shorter events, 0.2 us)
Async XLA Ops:
  0.0 15.3 %copy-start.3 = (f32[4,15,31]{2,0,1:T(4,128)S(1)}, f32[4,15,31]{2,0,1:T(4,128)}, u32[]{:S(2)}) copy-start(f32[4,15,31]{2,0,1:T(4,128)} %param.24) | copy-start | bytes 22324
  0.0 17.4 %copy-start = (bf16[384,2048]{1,0:T(8,128)(2,1)S(1)}, bf16[384,2048]{1,0:T(8,128)(2,1)}, u32[]{:S(2)}) copy-start(bf16[384,2048]{1,0:T(8,128)(2,1)} %latent_ref.1) | copy-start | bytes 4718596
  1.8 7.0 %collective-permute-start = (bf16[32,512]{1,0:T(8,128)(2,1)S(1)}, bf16[32,512]{1,0:T(8,128)(2,1)S(1)}, u32[]{:S(2)}, u32[]{:S(2)}) collective-permute-start(bf16[32,512]{1,0:T(8,128)(2,1)S(1)} %shard_map.127), channel_id=1, source_target_pairs={{0,12},{4,8},{8,4},{12,0},{1,13},{5,9},{9,5},{13,1},{2,14},{6,10},... | collective-permute-start | bytes 98312 | tf_op jit(solution)/shard_map/ppermute | solution.py:54
  7.0 4.8 %collective-permute-start.1 = (bf16[32,512]{1,0:T(8,128)(2,1)S(1)}, bf16[32,512]{1,0:T(8,128)(2,1)S(1)}, u32[]{:S(2)}, u32[]{:S(2)}) collective-permute-start(bf16[32,512]{1,0:T(8,128)(2,1)S(1)} %shard_map.127), channel_id=1, source_target_pairs={{0,8},{4,12},{8,0},{12,4},{1,9},{5,13},{9,1},{13,5},{2,10},{6,14},... | collective-permute-start | bytes 98312 | tf_op jit(solution)/shard_map/ppermute | solution.py:54
  7.0 4.8 %collective-permute-start.2 = (bf16[32,512]{1,0:T(8,128)(2,1)S(1)}, bf16[32,512]{1,0:T(8,128)(2,1)S(1)}, u32[]{:S(2)}, u32[]{:S(2)}) collective-permute-start(bf16[32,512]{1,0:T(8,128)(2,1)S(1)} %shard_map.127), channel_id=1, source_target_pairs={{0,4},{4,0},{8,12},{12,8},{1,5},{5,1},{9,13},{13,9},{2,6},{6,2},{1... | collective-permute-start | bytes 98312 | tf_op jit(solution)/shard_map/ppermute | solution.py:54
  11.8 13.9 %collective-permute-start.8 = (bf16[64,512]{1,0:T(8,128)(2,1)S(1)}, bf16[64,512]{1,0:T(8,128)(2,1)S(1)}, u32[]{:S(2)}, u32[]{:S(2)}) collective-permute-start(bf16[64,512]{1,0:T(8,128)(2,1)S(1)} %pad_maximum_fusion.refs_2_), channel_id=1, source_target_pairs={{0,2},{1,3},{2,0},{3,1},{4,6},{5,7},{6,4},{7,5},{8,10},{9,11},{10,... | collective-permute-start | bytes 196616 | tf_op jit(solution)/shard_map/ppermute | solution.py:54
  13.4 2.4 %collective-permute-start.3 = (f32[8,512]{1,0:T(8,128)S(1)}, f32[8,512]{1,0:T(8,128)S(1)}, u32[]{:S(2)}, u32[]{:S(2)}) collective-permute-start(f32[8,512]{1,0:T(8,128)S(1)} %add_add_fusion.refs_4_.refs_1_), channel_id=1, source_target_pairs={{0,1},{1,0},{2,3},{3,2},{4,5},{5,4},{6,7},{7,6},{8,9},{9,8},{10,11... | collective-permute-start | bytes 49160 | tf_op jit(solution)/shard_map/ppermute | solution.py:54
  13.4 3.9 %collective-permute-start.4 = (f32[8,512]{1,0:T(8,128)S(1)}, f32[8,512]{1,0:T(8,128)S(1)}, u32[]{:S(2)}, u32[]{:S(2)}) collective-permute-start(f32[8,512]{1,0:T(8,128)S(1)} %add_add_fusion.refs_4_.refs_1_), channel_id=1, source_target_pairs={{0,2},{1,3},{2,0},{3,1},{4,6},{5,7},{6,4},{7,5},{8,10},{9,11},{10,... | collective-permute-start | bytes 49160 | tf_op jit(solution)/shard_map/ppermute | solution.py:54
  14.0 3.3 %collective-permute-start.5 = (f32[8,512]{1,0:T(8,128)S(1)}, f32[8,512]{1,0:T(8,128)S(1)}, u32[]{:S(2)}, u32[]{:S(2)}) collective-permute-start(f32[8,512]{1,0:T(8,128)S(1)} %add_add_fusion.refs_4_.refs_1_), channel_id=1, source_target_pairs={{0,3},{1,2},{2,1},{3,0},{4,7},{5,6},{6,5},{7,4},{8,11},{9,10},{10,... | collective-permute-start | bytes 49160 | tf_op jit(solution)/shard_map/ppermute | solution.py:54
  15.4 11.0 %collective-permute-start.9 = (bf16[64,512]{1,0:T(8,128)(2,1)S(1)}, bf16[64,512]{1,0:T(8,128)(2,1)S(1)}, u32[]{:S(2)}, u32[]{:S(2)}) collective-permute-start(bf16[64,512]{1,0:T(8,128)(2,1)S(1)} %pad_maximum_fusion.refs_2_), channel_id=1, source_target_pairs={{0,1},{1,0},{2,3},{3,2},{4,5},{5,4},{6,7},{7,6},{8,9},{9,8},{10,11... | collective-permute-start | bytes 196616 | tf_op jit(solution)/shard_map/ppermute | solution.py:54
  20.4 6.4 %copy-start.2 = (bf16[2048,256]{1,0:T(8,128)(2,1)S(1)}, bf16[2048,256]{1,0:T(8,128)(2,1)}, u32[]{:S(2)}) copy-start(bf16[2048,256]{1,0:T(8,128)(2,1)} %wq_ref.1) | copy-start | bytes 3145732
  21.0 7.3 %collective-permute-start.14 = (bf16[256,256]{1,0:T(8,128)(2,1)S(1)}, bf16[256,256]{1,0:T(8,128)(2,1)S(1)}, u32[]{:S(2)}, u32[]{:S(2)}) collective-permute-start(bf16[256,256]{1,0:T(8,128)(2,1)S(1)} %get-tuple-element.35), channel_id=1, source_target_pairs={{0,4},{4,0},{8,12},{12,8},{1,5},{5,1},{9,13},{13,9},{2,6},{6,2},{1... | collective-permute-start | bytes 393224 | tf_op jit(solution)/shard_map/ppermute | solution.py:98
  21.1 7.2 %collective-permute-start.15 = (bf16[256,256]{1,0:T(8,128)(2,1)S(1)}, bf16[256,256]{1,0:T(8,128)(2,1)S(1)}, u32[]{:S(2)}, u32[]{:S(2)}) collective-permute-start(bf16[256,256]{1,0:T(8,128)(2,1)S(1)} %get-tuple-element.36), channel_id=1, source_target_pairs={{4,8},{8,4},{5,9},{9,5},{6,10},{10,6},{7,11},{11,7},{20,24},{24,20... | collective-permute-start | bytes 393224 | tf_op jit(solution)/shard_map/ppermute | solution.py:98
  21.8 9.3 %collective-permute-start.6 = (bf16[256,256]{1,0:T(8,128)(2,1)S(1)}, bf16[256,256]{1,0:T(8,128)(2,1)S(1)}, u32[]{:S(2)}, u32[]{:S(2)}) collective-permute-start(bf16[256,256]{1,0:T(8,128)(2,1)S(1)} %get-tuple-element.26), channel_id=1, source_target_pairs={{0,4},{4,0},{8,12},{12,8},{1,5},{5,1},{9,13},{13,9},{2,6},{6,2},{1... | collective-permute-start | bytes 393224 | tf_op jit(solution)/shard_map/ppermute | solution.py:98
  25.7 5.4 %collective-permute-start.7 = (bf16[256,256]{1,0:T(8,128)(2,1)S(1)}, bf16[256,256]{1,0:T(8,128)(2,1)S(1)}, u32[]{:S(2)}, u32[]{:S(2)}) collective-permute-start(bf16[256,256]{1,0:T(8,128)(2,1)S(1)} %get-tuple-element.27), channel_id=1, source_target_pairs={{4,8},{8,4},{5,9},{9,5},{6,10},{10,6},{7,11},{11,7},{20,24},{24,20... | collective-permute-start | bytes 393224 | tf_op jit(solution)/shard_map/ppermute | solution.py:98
  26.4 1.3 %collective-permute-start.10 = (bf16[64,512]{1,0:T(8,128)(2,1)S(1)}, bf16[64,512]{1,0:T(8,128)(2,1)S(1)}, u32[]{:S(2)}, u32[]{:S(2)}) collective-permute-start(bf16[64,512]{1,0:T(8,128)(2,1)S(1)} %collective-permute-done.8.refs_3_), channel_id=1, source_target_pairs={{0,1},{1,0},{2,3},{3,2},{4,5},{5,4},{6,7},{7,6},{8,9},{9,8},{10,11... | collective-permute-start | bytes 196616 | tf_op jit(solution)/shard_map/ppermute | solution.py:54
  28.3 10.3 %copy-start.1 = (bf16[1024,512]{1,0:T(8,128)(2,1)S(1)}, bf16[1024,512]{1,0:T(8,128)(2,1)}, u32[]{:S(2)}) copy-start(bf16[1024,512]{1,0:T(8,128)(2,1)} %refs_2_.3) | copy-start | bytes 3145732
  29.7 5.0 %collective-permute-start.16 = (bf16[384,128]{1,0:T(8,128)(2,1)S(1)}, bf16[384,128]{1,0:T(8,128)(2,1)S(1)}, u32[]{:S(2)}, u32[]{:S(2)}) collective-permute-start(bf16[384,128]{1,0:T(8,128)(2,1)S(1)} %shard_map.134.refs_7_), channel_id=1, source_target_pairs={{0,2},{1,3},{2,0},{3,1},{4,6},{5,7},{6,4},{7,5},{8,10},{9,11},{10,... | collective-permute-start | bytes 294920 | tf_op jit(solution)/shard_map/ppermute | solution.py:54
  32.5 4.7 %collective-permute-start.11 = (bf16[384,128]{1,0:T(8,128)(2,1)S(1)}, bf16[384,128]{1,0:T(8,128)(2,1)S(1)}, u32[]{:S(2)}, u32[]{:S(2)}) collective-permute-start(bf16[384,128]{1,0:T(8,128)(2,1)S(1)} %shard_map.132.refs_3_), channel_id=1, source_target_pairs={{0,2},{1,3},{2,0},{3,1},{4,6},{5,7},{6,4},{7,5},{8,10},{9,11},{10,... | collective-permute-start | bytes 294920 | tf_op jit(solution)/shard_map/ppermute | solution.py:54
  33.3 4.0 %collective-permute-start.17 = (bf16[384,128]{1,0:T(8,128)(2,1)S(1)}, bf16[384,128]{1,0:T(8,128)(2,1)S(1)}, u32[]{:S(2)}, u32[]{:S(2)}) collective-permute-start(bf16[384,128]{1,0:T(8,128)(2,1)S(1)} %shard_map.134.refs_7_), channel_id=1, source_target_pairs={{0,1},{1,0},{2,3},{3,2},{4,5},{5,4},{6,7},{7,6},{8,9},{9,8},{10,11... | collective-permute-start | bytes 294920 | tf_op jit(solution)/shard_map/ppermute | solution.py:54
  33.3 4.0 %collective-permute-start.12 = (bf16[384,128]{1,0:T(8,128)(2,1)S(1)}, bf16[384,128]{1,0:T(8,128)(2,1)S(1)}, u32[]{:S(2)}, u32[]{:S(2)}) collective-permute-start(bf16[384,128]{1,0:T(8,128)(2,1)S(1)} %shard_map.132.refs_3_), channel_id=1, source_target_pairs={{0,1},{1,0},{2,3},{3,2},{4,5},{5,4},{6,7},{7,6},{8,9},{9,8},{10,11... | collective-permute-start | bytes 294920 | tf_op jit(solution)/shard_map/ppermute | solution.py:54
  34.7 2.5 %collective-permute-start.18 = (bf16[384,128]{1,0:T(8,128)(2,1)S(1)}, bf16[384,128]{1,0:T(8,128)(2,1)S(1)}, u32[]{:S(2)}, u32[]{:S(2)}) collective-permute-start(bf16[384,128]{1,0:T(8,128)(2,1)S(1)} %collective-permute-done.16.refs_8_), channel_id=1, source_target_pairs={{0,1},{1,0},{2,3},{3,2},{4,5},{5,4},{6,7},{7,6},{8,9},{9,8},{10,11... | collective-permute-start | bytes 294920 | tf_op jit(solution)/shard_map/ppermute | solution.py:54
  37.2 1.3 %collective-permute-start.13 = (bf16[384,128]{1,0:T(8,128)(2,1)S(1)}, bf16[384,128]{1,0:T(8,128)(2,1)S(1)}, u32[]{:S(2)}, u32[]{:S(2)}) collective-permute-start(bf16[384,128]{1,0:T(8,128)(2,1)S(1)} %collective-permute-done.11.refs_4_), channel_id=1, source_target_pairs={{0,1},{1,0},{2,3},{3,2},{4,5},{5,4},{6,7},{7,6},{8,9},{9,8},{10,11... | collective-permute-start | bytes 294920 | tf_op jit(solution)/shard_map/ppermute | solution.py:54

commit v6 on v5

--- a/solution.py
+++ b/solution.py
@@ -6,6 +6,7 @@
 from jax.experimental import pallas as pl
 from jax.experimental.pallas import tpu as pltpu
 from jax.sharding import PartitionSpec as P
+
 
 HEAD_DIM = 64
 GRID_W = 64
@@ -156,12 +157,6 @@
         out_ref[r * GRID_W : (r + 1) * GRID_W, :] = jnp.where(inside, table, MASKED)
 
 
-def bias_kernel(*refs):
-    half = len(refs) // 2
-    for vectors_ref, out_ref in zip(refs[:half], refs[half:]):
-        bias_table(vectors_ref, out_ref)
-
-
 def inverse_rms(floats):
     return lax.rsqrt(jnp.mean(floats * floats, axis=-1, keepdims=True) + EPSILON)
 
@@ -174,49 +169,67 @@
     send_b_ref[...] = kv_ref[pl.ds(pl.multiple_of(odd * last, GRID_W), halo), :]
 
 
-def norm_kernel(*refs, tp_count, chunks):
+def prepare_kernel(*refs, chunks):
     latent_ref, gain_hbm, wk_hbm, wv_hbm = refs[:4]
-    piece_refs = refs[4 : 4 + tp_count]
-    outs = refs[4 + tp_count : -4]
-    normed_ref, kv_ref, send_a_ref, send_b_ref, mod_ref, gain_out_ref = outs[:6]
-    weight_refs = outs[6:]
-    gain_ref, factor_ref, offset_ref, sems = refs[-4:]
+    vector_refs = refs[4 : 4 + chunks]
+    inverse_ref, gain_out_ref = refs[4 + chunks : 6 + chunks]
+    weight_refs = refs[6 + chunks : 6 + 2 * chunks]
+    table_refs = refs[6 + 2 * chunks : -2]
+    gain_ref, sems = refs[-2:]
     tokens, _ = latent_ref.shape
-    cols = piece_refs[0].shape[1]
     each = weight_refs[0].shape[1] // 2
     pairs = [(gain_hbm, gain_ref)]
     for c, weight in enumerate(weight_refs):
         at = pl.ds(c * each, each)
         pairs += [(wk_hbm.at[:, at], weight.at[:, :each]), (wv_hbm.at[:, at], weight.at[:, each:])]
     copies = fetch(pairs, sems)
+    for vectors_ref, table_ref in zip(vector_refs, table_refs):
+        bias_table(vectors_ref, table_ref)
+    step = 16
+
+    def body(i, carry):
+        at = pl.ds(pl.multiple_of(i * step, step), step)
+        inverse = inverse_rms(latent_ref[at, :].astype(F32))
+        inverse_ref[at, :] = jnp.broadcast_to(inverse, (step, 128))
+        return carry
+
+    lax.fori_loop(0, tokens // step, body, 0, unroll=2)
+    copies[0].wait()
+    gain = gain_ref[...].astype(F32).reshape(1, -1)
+    gain_out_ref[...] = jnp.broadcast_to(gain, gain_out_ref.shape)
+    for copy in copies[1:]:
+        copy.wait()
+
+
+def norm_kernel(*refs):
+    latent_ref, inverse_ref, gain_ref, weight_ref = refs[:4]
+    piece_refs = refs[4:-7]
+    normed_ref, kv_ref, send_a_ref, send_b_ref, mod_ref, factor_ref, offset_ref = refs[-7:]
+    tokens, model = latent_ref.shape
+    cols = piece_refs[0].shape[1]
     tp_index = lax.axis_index("tp")
     for k, piece in enumerate(piece_refs):
         offset = pl.multiple_of((tp_index ^ k) * cols, 128)
         mod_ref[:, pl.ds(offset, cols)] = piece[...]
-    copies[0].wait()
-    gain = gain_ref[...].astype(F32).reshape(1, -1)
-    gain_out_ref[...] = jnp.broadcast_to(gain, gain_out_ref.shape)
-    factor_ref[...] = jnp.broadcast_to(gain * (1.0 + mod_ref[SCALE : SCALE + 1, :]), factor_ref.shape)
+    factor_ref[...] = gain_ref[...] * (1.0 + mod_ref[SCALE : SCALE + 1, :])
     offset_ref[...] = jnp.broadcast_to(mod_ref[SHIFT : SHIFT + 1, :], offset_ref.shape)
     step = 16
 
     def body(i, carry):
         at = pl.ds(pl.multiple_of(i * step, step), step)
-        floats = latent_ref[at, :].astype(F32)
-        scaled = (floats * inverse_rms(floats)).reshape(step // 8, 8, -1)
-        result = scaled * factor_ref[...][None] + offset_ref[...][None]
-        normed_ref[at, :] = result.reshape(step, -1).astype(BF16)
+        inverse = inverse_ref[at, :].reshape(step // 8, 8, 128)
+        for j in range(0, model, 128):
+            lanes = slice(j, j + 128)
+            floats = latent_ref[at, lanes].astype(F32).reshape(step // 8, 8, 128)
+            result = floats * inverse * factor_ref[:, lanes][None] + offset_ref[:, lanes][None]
+            normed_ref[at, lanes] = result.reshape(step, 128).astype(BF16)
         return carry
 
-    lax.fori_loop(0, tokens // step, body, 0, unroll=2)
-    copies[1].wait()
-    copies[2].wait()
+    lax.fori_loop(0, tokens // step, body, 0, unroll=4)
     kv_ref[...] = jnp.dot(
-        normed_ref[...], weight_refs[0][...], preferred_element_type=F32
+        normed_ref[...], weight_ref[...], preferred_element_type=F32
     ).astype(BF16)
     send_halo(kv_ref, send_a_ref, send_b_ref)
-    for copy in copies[3:]:
-        copy.wait()
 
 
 def chunk_kernel(normed_ref, weight_ref, kv_ref, send_a_ref, send_b_ref):
@@ -357,19 +370,27 @@
     mix(groups - 1)
 
 
-def output_kernel(*refs, masks, chunks):
-    resid_ref, mod_ref, w_out_ref = refs[:3]
-    piece_refs, out_ref = refs[3:-1], refs[-1]
+def output_kernel(*refs, masks, chunk, chunks):
+    count = len(masks)
+    w_out_ref, piece_refs = refs[0], refs[1 : 1 + count]
+    more, out_ref = list(refs[1 + count : -1]), refs[-1]
     tp_index = lax.axis_index("tp")
-    count = len(masks)
-    width = chunks * piece_refs[0].shape[1]
-    branch = None
-    for i, mask in enumerate(masks):
-        offset = pl.multiple_of((tp_index ^ mask) * width, 128)
-        piece = jnp.concatenate([piece_refs[c * count + i][...] for c in range(chunks)], axis=1)
-        part = jnp.dot(piece, w_out_ref[pl.ds(offset, width), :], preferred_element_type=F32)
-        branch = part if branch is None else branch + part
-    out_ref[...] = (resid_ref[...].astype(F32) + mod_ref[GATE : GATE + 1, :] * branch).astype(BF16)
+    each = piece_refs[0].shape[1]
+    rows = [
+        w_out_ref[pl.ds(pl.multiple_of(((tp_index ^ m) * chunks + chunk) * each, 128), each), :]
+        for m in masks
+    ]
+    branch = jnp.dot(
+        jnp.concatenate([piece[...] for piece in piece_refs], axis=1),
+        jnp.concatenate(rows, axis=0),
+        preferred_element_type=F32,
+    )
+    if chunk > 0:
+        branch = branch + more.pop(0)[...]
+    if chunk == chunks - 1:
+        resid_ref, mod_ref = more
+        branch = resid_ref[...].astype(F32) + mod_ref[GATE : GATE + 1, :] * branch
+    out_ref[...] = branch.astype(out_ref.dtype)
 
 
 def local(
@@ -393,7 +414,7 @@
     heads = width // HEAD_DIM
     chunks = width // 128 if width % 128 == 0 else 1
     each = width // chunks
-    sp_count, tp_count = lax.axis_size("sp"), lax.axis_size("tp")
+    sp_count = lax.axis_size("sp")
     halo = HALO * GRID_W
 
     own_context = shape_of((context.shape[0], cols), BF16)
@@ -415,32 +436,34 @@
         for c in range(chunks)
     ]
     table_shape = shape_of(((2 * WIN_H - 1) * GRID_W, each), F32)
-    tables = call(bias_kernel, (table_shape,) * chunks)(*vectors)
+    inverse, gain, *prepared = call(
+        functools.partial(prepare_kernel, chunks=chunks),
+        (shape_of((tokens, 128), F32), shape_of((8, model), F32))
+        + (shape_of((model, 2 * each), BF16),) * chunks
+        + (table_shape,) * chunks,
+        scratch=[pltpu.VMEM((model,), BF16), pltpu.SemaphoreType.DMA((1 + 2 * chunks,))],
+        in_specs=[VMEM] + [HBM] * 3 + [VMEM] * chunks,
+    )(latent, *in_hbm((norm_gain, w_key, w_value)), *vectors)
+    weights, tables = prepared[:chunks], prepared[chunks:]
 
     kv_shapes = (
         shape_of((tokens, 2 * each), BF16),
         shape_of((halo, 2 * each), BF16),
         shape_of((halo, 2 * each), BF16),
     )
-    normed, kv_0, send_a_0, send_b_0, mod, gain, *weights = call(
-        functools.partial(norm_kernel, tp_count=tp_count, chunks=chunks),
-        (shape_of((tokens, model), BF16),)
-        + kv_shapes
-        + (shape_of((MOD_ROWS, model), F32), shape_of((8, model), F32))
-        + (shape_of((model, 2 * each), BF16),) * chunks,
-        scratch=[
-            pltpu.VMEM((model,), BF16),
-            pltpu.VMEM((8, model), F32),
-            pltpu.VMEM((8, model), F32),
-            pltpu.SemaphoreType.DMA((1 + 2 * chunks,)),
-        ],
-        in_specs=[VMEM] + [HBM] * 3 + [VMEM] * tp_count,
-    )(latent, *in_hbm((norm_gain, w_key, w_value)), *mod_pieces)
-
-    keys_values = [(kv_0, send_a_0, send_b_0)] + [
-        call(chunk_kernel, kv_shapes)(normed, weight) for weight in weights[1:]
+    normed, kv_0, send_a_0, send_b_0, mod = call(
+        norm_kernel,
+        (shape_of((tokens, model), BF16),) + kv_shapes + (shape_of((MOD_ROWS, model), F32),),
+        scratch=[pltpu.VMEM((8, model), F32), pltpu.VMEM((8, model), F32)],
+    )(latent, inverse, gain, weights[0], *mod_pieces)
+
+    keys_values = [(kv_0, send_a_0, send_b_0)]
+    for c in range(1, chunks):
+        keys_values.append(call(chunk_kernel, kv_shapes)(normed, weights[c]))
+    halos = [
+        (pairwise(a, "sp", 0), pairwise(b, "sp", 1))
+        for _, a, b in keys_values
     ]
-    halos = [(pairwise(a, "sp", 0), pairwise(b, "sp", 1)) for _, a, b in keys_values]
 
     query, resid = call(
         query_kernel, (shape_of((tokens, width), BF16), shape_of((tokens, cols), BF16))
@@ -448,16 +471,17 @@
 
     ctx_pieces = pieces_by_bits(ctx_own, "tp")
     ctx_rows = ctx_own.shape[0]
-    ctx_all = call(
+    ctx_call = call(
         functools.partial(context_kernel, masks=[m for m, _ in ctx_pieces], chunks=chunks),
         (shape_of((ctx_rows, 2 * each), BF16),) * chunks,
         scratch=[pltpu.VMEM((ctx_rows, model), BF16)],
-    )(mod, gain, *[p for _, p in ctx_pieces], *weights)
+    )
+    ctx_all = ctx_call(mod, gain, *[p for _, p in ctx_pieces], *weights)
 
     rows = tokens // GRID_W
     group = 2 if rows % 2 == 0 else 1
     keys = (WIN_H + group - 1) * GRID_W + ctx_rows
-    gathered = []
+    branch = []
     for c in range(chunks):
         attended = call(
             functools.partial(attention_kernel, chunk=c, sp_count=sp_count),
@@ -469,13 +493,16 @@
             ],
         )(query, keys_values[c][0], *halos[c], tables[c], ctx_all[c])
         found = pieces_by_bits(attended, "tp")
-        masks = [mask for mask, _ in found]
-        gathered += [piece for _, piece in found]
-
-    return call(
-        functools.partial(output_kernel, masks=masks, chunks=chunks),
-        shape_of((tokens, cols), BF16),
-    )(resid, mod_own, w_out, *gathered)
+        last = c == chunks - 1
+        branch = [
+            call(
+                functools.partial(
+                    output_kernel, masks=[m for m, _ in found], chunk=c, chunks=chunks
+                ),
+                shape_of((tokens, cols), BF16 if last else F32),
+            )(w_out, *[p for _, p in found], *branch, *([resid, mod_own] if last else []))
+        ]
+    return branch[0]
 
 
 def solution(mesh):

time: 40 us -> 37.7 us (0.943)
  waiting for transfers between devices: 10.8 us -> 8.58 us
    ppermute x15, waiting for transfers between devices: 10.8 us -> 8.57 us  [peer(): return lax.ppermute(block, axis, [(i, i ^ mask) for i in range(count)])]
    pallas_call x5 -> x6, Pallas kernels: 5.82 us -> 5.78 us  [the longest x1 1.79 us: local(): call(functools.partial(prepare_kernel, chunks=chunks), (shape_of((tokens,...]
  transfers between devices with their start and end apart: 19 -> 19, of which waited for: 7 -> 6; matrix products, arithmetic and copies ran while one was open for 0% -> 0% of each run, Pallas kernels for 20% -> 21%
where the time goes in v6:
time: 37.7 us; the launch traced here: 37.5 us
  starting transfers between devices  17.6 us (47%)
  Pallas kernels  11 us (29%)
  waiting for transfers between devices  8.58 us (23%)
    ppermute x15, starting transfers between devices, peer(): return lax.ppermute(block, axis, [(i, i ^ mask) for i in range(count)])  12.1 us
    ppermute x15, waiting for transfers between devices, peer(): return lax.ppermute(block, axis, [(i, i ^ mask) for i in range(count)])  8.57 us
    ppermute x4, starting transfers between devices, pairwise(): return lax.ppermute(block, axis, pairs)  5.42 us
    pallas_call x2, Pallas kernels, local(): call(functools.partial(attention_kernel, chunk=c, sp_count=sp_count), sha...  2.8 us
    pallas_call x1, Pallas kernels, local(): call(modulation_kernel, shape_of((2 * MOD_ROWS + context.shape[0], cols),...  1.8 us
    pallas_call x1, Pallas kernels, local(): call(functools.partial(prepare_kernel, chunks=chunks), (shape_of((tokens,...  1.79 us
    pallas_call x2, Pallas kernels, local(): call(functools.partial(output_kernel, masks=[m for m, _ in found], chunk=...  1.5 us
    pallas_call x1, Pallas kernels, local(): call(norm_kernel, (shape_of((tokens, model), BF16),) + kv_shapes + (shape...  1.29 us
  transfers between devices with their start and end apart: 19, of which 6 were waited for; matrix products, arithmetic and copies ran while one was open for 0% of the time, Pallas kernels for 21%

profile of v6, /device:TPU:0, one launch (start us, length us, event | category | flops | bytes accessed | tf_op | source)
XLA Modules:
  0.0 37.5 jit_solution(14085435705838062858)
XLA Ops:
  0.0 1.8 %shard_map.128 = bf16[32,512]{1,0:T(8,128)(2,1)S(1)} custom-call(bf16[512]{0:T(512)(128)(2,1)} %cond_hbm.1, bf16[512]{0:T(512)(128)(2,1)} %ctx_hbm.1, bf16[512,512]{1,0:T(8,128)(2,1)} %w_shift_hbm.1, bf16[512,512]{1,0:T(8,128)(2,1)} %w_scale_hbm.1, bf16[512,512]{1,0:T(8,128)(2,1)} %w_gate_hbm.1, bf16[16,2048]{1,0:T(8,128)(2,1)} %context_hbm.1), custom_call_target="tpu_custom_call" | custom-call | tf_op jit(solution)/shard_map/pallas_call | solution.py:422
  1.8 5.1 %collective-permute-start = (bf16[32,512]{1,0:T(8,128)(2,1)S(1)}, bf16[32,512]{1,0:T(8,128)(2,1)S(1)}, u32[]{:S(2)}, u32[]{:S(2)}) collective-permute-start(bf16[32,512]{1,0:T(8,128)(2,1)S(1)} %shard_map.128), channel_id=1, source_target_pairs={{0,12},{4,8},{8,4},{12,0},{1,13},{5,9},{9,5},{13,1},{2,14},{6,10},... | collective-permute-start | bytes 98312 | tf_op jit(solution)/shard_map/ppermute | solution.py:55
  7.0 0.6 %collective-permute-start.2 = (bf16[32,512]{1,0:T(8,128)(2,1)S(1)}, bf16[32,512]{1,0:T(8,128)(2,1)S(1)}, u32[]{:S(2)}, u32[]{:S(2)}) collective-permute-start(bf16[32,512]{1,0:T(8,128)(2,1)S(1)} %shard_map.128), channel_id=1, source_target_pairs={{0,4},{4,0},{8,12},{12,8},{1,5},{5,1},{9,13},{13,9},{2,6},{6,2},{1... | collective-permute-start | bytes 98312 | tf_op jit(solution)/shard_map/ppermute | solution.py:55
  7.6 0.1 rev.3
  7.7 1.1 %collective-permute-done = bf16[32,512]{1,0:T(8,128)(2,1)S(1)} collective-permute-done((bf16[32,512]{1,0:T(8,128)(2,1)S(1)}, bf16[32,512]{1,0:T(8,128)(2,1)S(1)}, u32[]{:S(2)}, u32[]{:S(2)}) %collective-permute-start) | collective-permute-done | bytes 32800 | tf_op jit(solution)/shard_map/ppermute | solution.py:55
  8.9 2.9 %collective-permute-done.1 = bf16[32,512]{1,0:T(8,128)(2,1)S(1)} collective-permute-done((bf16[32,512]{1,0:T(8,128)(2,1)S(1)}, bf16[32,512]{1,0:T(8,128)(2,1)S(1)}, u32[]{:S(2)}, u32[]{:S(2)}) %collective-permute-start.1) | collective-permute-done | bytes 32800 | tf_op jit(solution)/shard_map/ppermute | solution.py:55
  11.8 0.1 collective-permute-start.3
  11.9 1.6 %collective-permute-start.4 = (f32[8,512]{1,0:T(8,128)S(1)}, f32[8,512]{1,0:T(8,128)S(1)}, u32[]{:S(2)}, u32[]{:S(2)}) collective-permute-start(f32[8,512]{1,0:T(8,128)S(1)} %add_add_fusion.refs_4_.refs_7_), channel_id=1, source_target_pairs={{0,2},{1,3},{2,0},{3,1},{4,6},{5,7},{6,4},{7,5},{8,10},{9,11},{10,... | collective-permute-start | bytes 49160 | tf_op jit(solution)/shard_map/ppermute | solution.py:55
  13.4 0.3 collective-permute-start.5
  13.7 1.6 %collective-permute-start.8 = (bf16[64,512]{1,0:T(8,128)(2,1)S(1)}, bf16[64,512]{1,0:T(8,128)(2,1)S(1)}, u32[]{:S(2)}, u32[]{:S(2)}) collective-permute-start(bf16[64,512]{1,0:T(8,128)(2,1)S(1)} %pad_maximum_fusion.refs_2_), channel_id=1, source_target_pairs={{0,2},{1,3},{2,0},{3,1},{4,6},{5,7},{6,4},{7,5},{8,10},{9,11},{10,... | collective-permute-start | bytes 196616 | tf_op jit(solution)/shard_map/ppermute | solution.py:55
  15.3 0.1 pad_maximum_fusion.1
  15.4 1.8 %shard_map.127 = (f32[384,128]{1,0:T(8,128)S(1)}, f32[8,2048]{1,0:T(8,128)S(1)}, bf16[2048,256]{1,0:T(8,128)(2,1)S(1)}, bf16[2048,256]{1,0:T(8,128)(2,1)S(1)}, f...) custom-call(bf16[384,2048]{1,0:T(8,128)(2,1)S(1)} %copy-done, bf16[2048]{0:T(1024)(128)(2,1)} %refs_1_.1, ...), custom_call_target="tpu_custom_call" | custom-call | tf_op jit(solution)/shard_map/pallas_call | solution.py:439
  17.2 0.1 collective-permute-start.9
  17.3 1.3 %shard_map.129 = (bf16[384,2048]{1,0:T(8,128)(2,1)S(1)}, bf16[384,256]{1,0:T(8,128)(2,1)S(1)}, bf16[256,256]{1,0:T(8,128)(2,1)S(1)}, bf16[256,256]{1,0:T(8,128)(2,1)S(1)}, f32[8,2048]{1,0:T(8,128)S(1)}) custom-call(bf16[384,2048]{1,0:T(8,128)(2,1)S(1)} %copy-done, f32[384,128]{1,0:T(8,128)S(1)} %get-tuple-element.23.refs_1_, ...), custom_call_target="tpu_custom_call" | custom-call | tf_op jit(solution)/shard_map/pallas_call | solution.py:454
  18.7 0.8 %collective-permute-start.15 = (bf16[256,256]{1,0:T(8,128)(2,1)S(1)}, bf16[256,256]{1,0:T(8,128)(2,1)S(1)}, u32[]{:S(2)}, u32[]{:S(2)}) collective-permute-start(bf16[256,256]{1,0:T(8,128)(2,1)S(1)} %get-tuple-element.37), channel_id=1, source_target_pairs={{4,8},{8,4},{5,9},{9,5},{6,10},{10,6},{7,11},{11,7},{20,24},{24,20... | collective-permute-start | bytes 393224 | tf_op jit(solution)/shard_map/ppermute | solution.py:99
  19.5 0.6 %shard_map.131 = (bf16[384,256]{1,0:T(8,128)(2,1)S(1)}, bf16[256,256]{1,0:T(8,128)(2,1)S(1)}, bf16[256,256]{1,0:T(8,128)(2,1)S(1)}) custom-call(bf16[384,2048]{1,0:T(8,128)(2,1)S(1)} %get-tuple-element.26.normed_ref, bf16[2048,256]{1,0:T(8,128)(2,1)S(1)} %get-tuple-element.28.weight_ref.refs_7_), custom_call_target="tpu_custom_call" | custom-call | tf_op jit(solution)/shard_map/pallas_call | solution.py:462
  20.1 3.9 %collective-permute-start.6 = (bf16[256,256]{1,0:T(8,128)(2,1)S(1)}, bf16[256,256]{1,0:T(8,128)(2,1)S(1)}, u32[]{:S(2)}, u32[]{:S(2)}) collective-permute-start(bf16[256,256]{1,0:T(8,128)(2,1)S(1)} %get-tuple-element.30), channel_id=1, source_target_pairs={{0,4},{4,0},{8,12},{12,8},{1,5},{5,1},{9,13},{13,9},{2,6},{6,2},{1... | collective-permute-start | bytes 393224 | tf_op jit(solution)/shard_map/ppermute | solution.py:99
  24.0 0.7 %collective-permute-start.7 = (bf16[256,256]{1,0:T(8,128)(2,1)S(1)}, bf16[256,256]{1,0:T(8,128)(2,1)S(1)}, u32[]{:S(2)}, u32[]{:S(2)}) collective-permute-start(bf16[256,256]{1,0:T(8,128)(2,1)S(1)} %get-tuple-element.31), channel_id=1, source_target_pairs={{4,8},{8,4},{5,9},{9,5},{6,10},{10,6},{7,11},{11,7},{20,24},{24,20... | collective-permute-start | bytes 393224 | tf_op jit(solution)/shard_map/ppermute | solution.py:99
  24.7 0.1 collective-permute-start.10
  24.8 0.6 %shard_map.130 = (bf16[384,256]{1,0:T(8,128)(2,1)S(1)}, bf16[384,512]{1,0:T(8,128)(2,1)S(1)}) custom-call(bf16[384,2048]{1,0:T(8,128)(2,1)S(1)} %get-tuple-element.26.normed_ref, bf16[2048,256]{1,0:T(8,128)(2,1)S(1)} %copy-done.2, bf16[384,2048]{1,0:T(8,128)(2,1)S(1)} %copy-done), custom_call_target="tpu_custom_call" | custom-call | tf_op jit(solution)/shard_map/pallas_call | solution.py:468
  25.4 0.6 %collective-permute-done.10.refs_5_ = bf16[64,512]{1,0:T(8,128)(2,1)S(1)} collective-permute-done((bf16[64,512]{1,0:T(8,128)(2,1)S(1)}, bf16[64,512]{1,0:T(8,128)(2,1)S(1)}, u32[]{:S(2)}, u32[]{:S(2)}) %collective-permute-start.10) | collective-permute-done | bytes 65568 | tf_op jit(solution)/shard_map/ppermute | solution.py:55
  26.0 0.6 %shard_map.132 = (bf16[64,256]{1,0:T(8,128)(2,1)S(1)}, bf16[64,256]{1,0:T(8,128)(2,1)S(1)}) custom-call(f32[8,2048]{1,0:T(8,128)S(1)} %get-tuple-element.33.refs_0_, f32[8,2048]{1,0:T(8,128)S(1)} %get-tuple-element.24.refs_2_.refs_1_, bf16[64,512]{1,0:T(8,128)(2,1)S(1)} %pad_maximum_fusion.refs_2_, bf16[64,512]{1,0:T(8,128)(2,1)S(1)} %collective-permute-done.8.refs_3_, ...), custom_call_target="tpu_custom_call" | custom-call | tf_op jit(solution)/shard_map/pallas_call | solution.py:479
  26.6 1.4 %shard_map.134.refs_1_ = bf16[384,128]{1,0:T(8,128)(2,1)S(1)} custom-call(bf16[384,256]{1,0:T(8,128)(2,1)S(1)} %get-tuple-element.27.q_ref, bf16[384,256]{1,0:T(8,128)(2,1)S(1)} %get-tuple-element.35.kv_ref, bf16[256,256]{1,0:T(8,128)(2,1)S(1)} %collective-permute-done.14.recv_a_ref, bf16[256,256]{1,0:T(8,128)(2,1)S(1)} %collective-permute-done.15.recv_b_ref, ...), custom_call_target="tpu_custom_call" | custom-call | tf_op jit(solution)/shard_map/pallas_call | solution.py:486
  28.0 0.6 %collective-permute-start.16 = (bf16[384,128]{1,0:T(8,128)(2,1)S(1)}, bf16[384,128]{1,0:T(8,128)(2,1)S(1)}, u32[]{:S(2)}, u32[]{:S(2)}) collective-permute-start(bf16[384,128]{1,0:T(8,128)(2,1)S(1)} %shard_map.134.refs_1_), channel_id=1, source_target_pairs={{0,2},{1,3},{2,0},{3,1},{4,6},{5,7},{6,4},{7,5},{8,10},{9,11},{10,... | collective-permute-start | bytes 294920 | tf_op jit(solution)/shard_map/ppermute | solution.py:55
  28.7 1.4 %shard_map.133.refs_1_ = bf16[384,128]{1,0:T(8,128)(2,1)S(1)} custom-call(bf16[384,256]{1,0:T(8,128)(2,1)S(1)} %get-tuple-element.27.q_ref, bf16[384,256]{1,0:T(8,128)(2,1)S(1)} %get-tuple-element.29.kv_ref, bf16[256,256]{1,0:T(8,128)(2,1)S(1)} %collective-permute-done.6.recv_a_ref, bf16[256,256]{1,0:T(8,128)(2,1)S(1)} %collective-permute-done.7.recv_b_ref, ...), custom_call_target="tpu_custom_call" | custom-call | tf_op jit(solution)/shard_map/pallas_call | solution.py:486
  30.1 1.6 %collective-permute-start.11 = (bf16[384,128]{1,0:T(8,128)(2,1)S(1)}, bf16[384,128]{1,0:T(8,128)(2,1)S(1)}, u32[]{:S(2)}, u32[]{:S(2)}) collective-permute-start(bf16[384,128]{1,0:T(8,128)(2,1)S(1)} %shard_map.133.refs_1_), channel_id=1, source_target_pairs={{0,2},{1,3},{2,0},{3,1},{4,6},{5,7},{6,4},{7,5},{8,10},{9,11},{10,... | collective-permute-start | bytes 294920 | tf_op jit(solution)/shard_map/ppermute | solution.py:55
  31.6 1.7 %collective-permute-done.16.refs_2_ = bf16[384,128]{1,0:T(8,128)(2,1)S(1)} collective-permute-done((bf16[384,128]{1,0:T(8,128)(2,1)S(1)}, bf16[384,128]{1,0:T(8,128)(2,1)S(1)}, u32[]{:S(2)}, u32[]{:S(2)}) %collective-permute-start.16) | collective-permute-done | bytes 98336 | tf_op jit(solution)/shard_map/ppermute | solution.py:55
  33.3 0.5 %collective-permute-start.12 = (bf16[384,128]{1,0:T(8,128)(2,1)S(1)}, bf16[384,128]{1,0:T(8,128)(2,1)S(1)}, u32[]{:S(2)}, u32[]{:S(2)}) collective-permute-start(bf16[384,128]{1,0:T(8,128)(2,1)S(1)} %shard_map.133.refs_1_), channel_id=1, source_target_pairs={{0,1},{1,0},{2,3},{3,2},{4,5},{5,4},{6,7},{7,6},{8,9},{9,8},{10,11... | collective-permute-start | bytes 294920 | tf_op jit(solution)/shard_map/ppermute | solution.py:55
  33.9 1.2 %collective-permute-done.11.refs_2_ = bf16[384,128]{1,0:T(8,128)(2,1)S(1)} collective-permute-done((bf16[384,128]{1,0:T(8,128)(2,1)S(1)}, bf16[384,128]{1,0:T(8,128)(2,1)S(1)}, u32[]{:S(2)}, u32[]{:S(2)}) %collective-permute-start.11) | collective-permute-done | bytes 98336 | tf_op jit(solution)/shard_map/ppermute | solution.py:55
  35.1 0.4 shard_map.135.refs_5_
  35.5 0.9 %collective-permute-done.13.refs_4_ = bf16[384,128]{1,0:T(8,128)(2,1)S(1)} collective-permute-done((bf16[384,128]{1,0:T(8,128)(2,1)S(1)}, bf16[384,128]{1,0:T(8,128)(2,1)S(1)}, u32[]{:S(2)}, u32[]{:S(2)}) %collective-permute-start.13) | collective-permute-done | bytes 98336 | tf_op jit(solution)/shard_map/ppermute | solution.py:55
  36.4 1.1 %shard_map.136 = bf16[384,512]{1,0:T(8,128)(2,1)} custom-call(bf16[1024,512]{1,0:T(8,128)(2,1)S(1)} %copy-done.1, bf16[384,128]{1,0:T(8,128)(2,1)S(1)} %shard_map.133.refs_1_, bf16[384,128]{1,0:T(8,128)(2,1)S(1)} %collective-permute-done.11.refs_2_, bf16[384,128]{1,0:T(8,128)(2,1)S(1)} %collective-permute-done.12.refs_3_, ...), custom_call_target="tpu_custom_call" | custom-call | tf_op jit(solution)/shard_map/pallas_call | solution.py:498
  (34 shorter events, 0.2 us)
Async XLA Ops:
  0.0 7.6 %copy-start.3 = (f32[4,15,31]{2,0,1:T(4,128)S(1)}, f32[4,15,31]{2,0,1:T(4,128)}, u32[]{:S(2)}) copy-start(f32[4,15,31]{2,0,1:T(4,128)} %param.24) | copy-start | bytes 22324
  0.0 15.4 %copy-start = (bf16[384,2048]{1,0:T(8,128)(2,1)S(1)}, bf16[384,2048]{1,0:T(8,128)(2,1)}, u32[]{:S(2)}) copy-start(bf16[384,2048]{1,0:T(8,128)(2,1)} %latent_ref.1) | copy-start | bytes 4718596
  1.8 7.0 %collective-permute-start = (bf16[32,512]{1,0:T(8,128)(2,1)S(1)}, bf16[32,512]{1,0:T(8,128)(2,1)S(1)}, u32[]{:S(2)}, u32[]{:S(2)}) collective-permute-start(bf16[32,512]{1,0:T(8,128)(2,1)S(1)} %shard_map.128), channel_id=1, source_target_pairs={{0,12},{4,8},{8,4},{12,0},{1,13},{5,9},{9,5},{13,1},{2,14},{6,10},... | collective-permute-start | bytes 98312 | tf_op jit(solution)/shard_map/ppermute | solution.py:55
  7.0 4.8 %collective-permute-start.1 = (bf16[32,512]{1,0:T(8,128)(2,1)S(1)}, bf16[32,512]{1,0:T(8,128)(2,1)S(1)}, u32[]{:S(2)}, u32[]{:S(2)}) collective-permute-start(bf16[32,512]{1,0:T(8,128)(2,1)S(1)} %shard_map.128), channel_id=1, source_target_pairs={{0,8},{4,12},{8,0},{12,4},{1,9},{5,13},{9,1},{13,5},{2,10},{6,14},... | collective-permute-start | bytes 98312 | tf_op jit(solution)/shard_map/ppermute | solution.py:55
  7.0 4.8 %collective-permute-start.2 = (bf16[32,512]{1,0:T(8,128)(2,1)S(1)}, bf16[32,512]{1,0:T(8,128)(2,1)S(1)}, u32[]{:S(2)}, u32[]{:S(2)}) collective-permute-start(bf16[32,512]{1,0:T(8,128)(2,1)S(1)} %shard_map.128), channel_id=1, source_target_pairs={{0,4},{4,0},{8,12},{12,8},{1,5},{5,1},{9,13},{13,9},{2,6},{6,2},{1... | collective-permute-start | bytes 98312 | tf_op jit(solution)/shard_map/ppermute | solution.py:55
  11.8 5.5 %collective-permute-start.3 = (f32[8,512]{1,0:T(8,128)S(1)}, f32[8,512]{1,0:T(8,128)S(1)}, u32[]{:S(2)}, u32[]{:S(2)}) collective-permute-start(f32[8,512]{1,0:T(8,128)S(1)} %add_add_fusion.refs_4_.refs_7_), channel_id=1, source_target_pairs={{0,1},{1,0},{2,3},{3,2},{4,5},{5,4},{6,7},{7,6},{8,9},{9,8},{10,11... | collective-permute-start | bytes 49160 | tf_op jit(solution)/shard_map/ppermute | solution.py:55
  11.9 5.4 %collective-permute-start.4 = (f32[8,512]{1,0:T(8,128)S(1)}, f32[8,512]{1,0:T(8,128)S(1)}, u32[]{:S(2)}, u32[]{:S(2)}) collective-permute-start(f32[8,512]{1,0:T(8,128)S(1)} %add_add_fusion.refs_4_.refs_7_), channel_id=1, source_target_pairs={{0,2},{1,3},{2,0},{3,1},{4,6},{5,7},{6,4},{7,5},{8,10},{9,11},{10,... | collective-permute-start | bytes 49160 | tf_op jit(solution)/shard_map/ppermute | solution.py:55
  13.4 3.9 %collective-permute-start.5 = (f32[8,512]{1,0:T(8,128)S(1)}, f32[8,512]{1,0:T(8,128)S(1)}, u32[]{:S(2)}, u32[]{:S(2)}) collective-permute-start(f32[8,512]{1,0:T(8,128)S(1)} %add_add_fusion.refs_4_.refs_7_), channel_id=1, source_target_pairs={{0,3},{1,2},{2,1},{3,0},{4,7},{5,6},{6,5},{7,4},{8,11},{9,10},{10,... | collective-permute-start | bytes 49160 | tf_op jit(solution)/shard_map/ppermute | solution.py:55
  13.7 10.3 %collective-permute-start.8 = (bf16[64,512]{1,0:T(8,128)(2,1)S(1)}, bf16[64,512]{1,0:T(8,128)(2,1)S(1)}, u32[]{:S(2)}, u32[]{:S(2)}) collective-permute-start(bf16[64,512]{1,0:T(8,128)(2,1)S(1)} %pad_maximum_fusion.refs_2_), channel_id=1, source_target_pairs={{0,2},{1,3},{2,0},{3,1},{4,6},{5,7},{6,4},{7,5},{8,10},{9,11},{10,... | collective-permute-start | bytes 196616 | tf_op jit(solution)/shard_map/ppermute | solution.py:55
  17.2 7.5 %collective-permute-start.9 = (bf16[64,512]{1,0:T(8,128)(2,1)S(1)}, bf16[64,512]{1,0:T(8,128)(2,1)S(1)}, u32[]{:S(2)}, u32[]{:S(2)}) collective-permute-start(bf16[64,512]{1,0:T(8,128)(2,1)S(1)} %pad_maximum_fusion.refs_2_), channel_id=1, source_target_pairs={{0,1},{1,0},{2,3},{3,2},{4,5},{5,4},{6,7},{7,6},{8,9},{9,8},{10,11... | collective-permute-start | bytes 196616 | tf_op jit(solution)/shard_map/ppermute | solution.py:55
  18.6 6.2 %copy-start.2 = (bf16[2048,256]{1,0:T(8,128)(2,1)S(1)}, bf16[2048,256]{1,0:T(8,128)(2,1)}, u32[]{:S(2)}) copy-start(bf16[2048,256]{1,0:T(8,128)(2,1)} %wq_ref.1) | copy-start | bytes 3145732
  18.6 8.0 %collective-permute-start.14 = (bf16[256,256]{1,0:T(8,128)(2,1)S(1)}, bf16[256,256]{1,0:T(8,128)(2,1)S(1)}, u32[]{:S(2)}, u32[]{:S(2)}) collective-permute-start(bf16[256,256]{1,0:T(8,128)(2,1)S(1)} %get-tuple-element.36), channel_id=1, source_target_pairs={{0,4},{4,0},{8,12},{12,8},{1,5},{5,1},{9,13},{13,9},{2,6},{6,2},{1... | collective-permute-start | bytes 393224 | tf_op jit(solution)/shard_map/ppermute | solution.py:99
  18.7 7.9 %collective-permute-start.15 = (bf16[256,256]{1,0:T(8,128)(2,1)S(1)}, bf16[256,256]{1,0:T(8,128)(2,1)S(1)}, u32[]{:S(2)}, u32[]{:S(2)}) collective-permute-start(bf16[256,256]{1,0:T(8,128)(2,1)S(1)} %get-tuple-element.37), channel_id=1, source_target_pairs={{4,8},{8,4},{5,9},{9,5},{6,10},{10,6},{7,11},{11,7},{20,24},{24,20... | collective-permute-start | bytes 393224 | tf_op jit(solution)/shard_map/ppermute | solution.py:99
  20.1 8.5 %collective-permute-start.6 = (bf16[256,256]{1,0:T(8,128)(2,1)S(1)}, bf16[256,256]{1,0:T(8,128)(2,1)S(1)}, u32[]{:S(2)}, u32[]{:S(2)}) collective-permute-start(bf16[256,256]{1,0:T(8,128)(2,1)S(1)} %get-tuple-element.30), channel_id=1, source_target_pairs={{0,4},{4,0},{8,12},{12,8},{1,5},{5,1},{9,13},{13,9},{2,6},{6,2},{1... | collective-permute-start | bytes 393224 | tf_op jit(solution)/shard_map/ppermute | solution.py:99
  24.0 4.6 %collective-permute-start.7 = (bf16[256,256]{1,0:T(8,128)(2,1)S(1)}, bf16[256,256]{1,0:T(8,128)(2,1)S(1)}, u32[]{:S(2)}, u32[]{:S(2)}) collective-permute-start(bf16[256,256]{1,0:T(8,128)(2,1)S(1)} %get-tuple-element.31), channel_id=1, source_target_pairs={{4,8},{8,4},{5,9},{9,5},{6,10},{10,6},{7,11},{11,7},{20,24},{24,20... | collective-permute-start | bytes 393224 | tf_op jit(solution)/shard_map/ppermute | solution.py:99
  24.7 1.3 %collective-permute-start.10 = (bf16[64,512]{1,0:T(8,128)(2,1)S(1)}, bf16[64,512]{1,0:T(8,128)(2,1)S(1)}, u32[]{:S(2)}, u32[]{:S(2)}) collective-permute-start(bf16[64,512]{1,0:T(8,128)(2,1)S(1)} %collective-permute-done.8.refs_3_), channel_id=1, source_target_pairs={{0,1},{1,0},{2,3},{3,2},{4,5},{5,4},{6,7},{7,6},{8,9},{9,8},{10,11... | collective-permute-start | bytes 196616 | tf_op jit(solution)/shard_map/ppermute | solution.py:55
  26.6 8.5 %copy-start.1 = (bf16[1024,512]{1,0:T(8,128)(2,1)S(1)}, bf16[1024,512]{1,0:T(8,128)(2,1)}, u32[]{:S(2)}) copy-start(bf16[1024,512]{1,0:T(8,128)(2,1)} %refs_0_.7) | copy-start | bytes 3145732
  28.0 5.3 %collective-permute-start.16 = (bf16[384,128]{1,0:T(8,128)(2,1)S(1)}, bf16[384,128]{1,0:T(8,128)(2,1)S(1)}, u32[]{:S(2)}, u32[]{:S(2)}) collective-permute-start(bf16[384,128]{1,0:T(8,128)(2,1)S(1)} %shard_map.134.refs_1_), channel_id=1, source_target_pairs={{0,2},{1,3},{2,0},{3,1},{4,6},{5,7},{6,4},{7,5},{8,10},{9,11},{10,... | collective-permute-start | bytes 294920 | tf_op jit(solution)/shard_map/ppermute | solution.py:55
  30.1 5.0 %collective-permute-start.11 = (bf16[384,128]{1,0:T(8,128)(2,1)S(1)}, bf16[384,128]{1,0:T(8,128)(2,1)S(1)}, u32[]{:S(2)}, u32[]{:S(2)}) collective-permute-start(bf16[384,128]{1,0:T(8,128)(2,1)S(1)} %shard_map.133.refs_1_), channel_id=1, source_target_pairs={{0,2},{1,3},{2,0},{3,1},{4,6},{5,7},{6,4},{7,5},{8,10},{9,11},{10,... | collective-permute-start | bytes 294920 | tf_op jit(solution)/shard_map/ppermute | solution.py:55
  31.6 3.5 %collective-permute-start.17 = (bf16[384,128]{1,0:T(8,128)(2,1)S(1)}, bf16[384,128]{1,0:T(8,128)(2,1)S(1)}, u32[]{:S(2)}, u32[]{:S(2)}) collective-permute-start(bf16[384,128]{1,0:T(8,128)(2,1)S(1)} %shard_map.134.refs_1_), channel_id=1, source_target_pairs={{0,1},{1,0},{2,3},{3,2},{4,5},{5,4},{6,7},{7,6},{8,9},{9,8},{10,11... | collective-permute-start | bytes 294920 | tf_op jit(solution)/shard_map/ppermute | solution.py:55
  33.3 1.7 %collective-permute-start.18 = (bf16[384,128]{1,0:T(8,128)(2,1)S(1)}, bf16[384,128]{1,0:T(8,128)(2,1)S(1)}, u32[]{:S(2)}, u32[]{:S(2)}) collective-permute-start(bf16[384,128]{1,0:T(8,128)(2,1)S(1)} %collective-permute-done.16.refs_2_), channel_id=1, source_target_pairs={{0,1},{1,0},{2,3},{3,2},{4,5},{5,4},{6,7},{7,6},{8,9},{9,8},{10,11... | collective-permute-start | bytes 294920 | tf_op jit(solution)/shard_map/ppermute | solution.py:55
  33.3 2.1 %collective-permute-start.12 = (bf16[384,128]{1,0:T(8,128)(2,1)S(1)}, bf16[384,128]{1,0:T(8,128)(2,1)S(1)}, u32[]{:S(2)}, u32[]{:S(2)}) collective-permute-start(bf16[384,128]{1,0:T(8,128)(2,1)S(1)} %shard_map.133.refs_1_), channel_id=1, source_target_pairs={{0,1},{1,0},{2,3},{3,2},{4,5},{5,4},{6,7},{7,6},{8,9},{9,8},{10,11... | collective-permute-start | bytes 294920 | tf_op jit(solution)/shard_map/ppermute | solution.py:55
  35.1 1.3 %collective-permute-start.13 = (bf16[384,128]{1,0:T(8,128)(2,1)S(1)}, bf16[384,128]{1,0:T(8,128)(2,1)S(1)}, u32[]{:S(2)}, u32[]{:S(2)}) collective-permute-start(bf16[384,128]{1,0:T(8,128)(2,1)S(1)} %collective-permute-done.11.refs_2_), channel_id=1, source_target_pairs={{0,1},{1,0},{2,3},{3,2},{4,5},{5,4},{6,7},{7,6},{8,9},{9,8},{10,11... | collective-permute-start | bytes 294920 | tf_op jit(solution)/shard_map/ppermute | solution.py:55

commit v7 on v6

--- a/solution.py
+++ b/solution.py
@@ -15,6 +15,7 @@
 EPSILON = 1e-06
 HALO = WIN_H // 2
 MASKED = -1e30
+LOG2_E = 1.4426950408889634
 SHIFT, CTX_SHIFT, SCALE, CTX_SCALE, GATE, MOD_ROWS = 0, 1, 2, 3, 4, 8
 
 HBM = pl.BlockSpec(memory_space=pltpu.HBM)
@@ -154,19 +155,22 @@
             stride=1,
             stride_axis=0,
         )
-        out_ref[r * GRID_W : (r + 1) * GRID_W, :] = jnp.where(inside, table, MASKED)
+        out_ref[r * GRID_W : (r + 1) * GRID_W, :] = jnp.where(inside, table * LOG2_E, MASKED)
 
 
 def inverse_rms(floats):
     return lax.rsqrt(jnp.mean(floats * floats, axis=-1, keepdims=True) + EPSILON)
 
 
-def send_halo(kv_ref, send_a_ref, send_b_ref):
-    halo = HALO * GRID_W
-    last = kv_ref.shape[0] - halo
-    odd = lax.axis_index("sp") % 2
-    send_a_ref[...] = kv_ref[pl.ds(pl.multiple_of((1 - odd) * last, GRID_W), halo), :]
-    send_b_ref[...] = kv_ref[pl.ds(pl.multiple_of(odd * last, GRID_W), halo), :]
+def send_halo(kv_refs, send_refs, low_side):
+    halo, _ = send_refs[0].shape
+    at = pl.ds(pl.multiple_of(low_side * (kv_refs[0].shape[0] - halo), GRID_W), halo)
+    each = kv_refs[0].shape[1]
+    for c, kv_ref in enumerate(kv_refs):
+        if len(send_refs) > 1:
+            send_refs[c][...] = kv_ref[at, :]
+        else:
+            send_refs[0][:, c * each : (c + 1) * each] = kv_ref[at, :]
 
 
 def prepare_kernel(*refs, chunks):
@@ -201,10 +205,13 @@
         copy.wait()
 
 
-def norm_kernel(*refs):
-    latent_ref, inverse_ref, gain_ref, weight_ref = refs[:4]
-    piece_refs = refs[4:-7]
-    normed_ref, kv_ref, send_a_ref, send_b_ref, mod_ref, factor_ref, offset_ref = refs[-7:]
+def norm_kernel(*refs, chunks, tp_count, evens):
+    latent_ref, inverse_ref, gain_ref = refs[:3]
+    weight_refs, piece_refs = refs[3 : 3 + chunks], refs[3 + chunks : 3 + chunks + tp_count]
+    normed_ref, mod_ref = refs[3 + chunks + tp_count : 5 + chunks + tp_count]
+    kv_refs = refs[5 + chunks + tp_count : 5 + 2 * chunks + tp_count]
+    send_refs = refs[5 + 2 * chunks + tp_count : -2]
+    factor_ref, offset_ref = refs[-2:]
     tokens, model = latent_ref.shape
     cols = piece_refs[0].shape[1]
     tp_index = lax.axis_index("tp")
@@ -226,23 +233,19 @@
         return carry
 
     lax.fori_loop(0, tokens // step, body, 0, unroll=4)
-    kv_ref[...] = jnp.dot(
-        normed_ref[...], weight_ref[...], preferred_element_type=F32
-    ).astype(BF16)
-    send_halo(kv_ref, send_a_ref, send_b_ref)
-
-
-def chunk_kernel(normed_ref, weight_ref, kv_ref, send_a_ref, send_b_ref):
-    kv_ref[...] = jnp.dot(
-        normed_ref[...], weight_ref[...], preferred_element_type=F32
-    ).astype(BF16)
-    send_halo(kv_ref, send_a_ref, send_b_ref)
+    for kv_ref, weight_ref in zip(kv_refs, weight_refs):
+        kv_ref[...] = jnp.dot(
+            normed_ref[...], weight_ref[...], preferred_element_type=F32
+        ).astype(BF16)
+    odd = lax.axis_index("sp") % 2
+    send_halo(kv_refs, send_refs[:evens], 1 - odd)
+    send_halo(kv_refs, send_refs[evens:], odd)
 
 
 def query_kernel(normed_ref, wq_ref, latent_ref, q_ref, resid_ref):
     cols = resid_ref.shape[1]
-    query = jnp.dot(normed_ref[...], wq_ref[...], preferred_element_type=F32).astype(BF16)
-    q_ref[...] = query * BF16(HEAD_DIM**-0.5)
+    query = jnp.dot(normed_ref[...], wq_ref[...], preferred_element_type=F32)
+    q_ref[...] = (query * (LOG2_E * HEAD_DIM**-0.5)).astype(BF16)
     own = pl.ds(pl.multiple_of(lax.axis_index("tp") * cols, 128), cols)
     resid_ref[...] = latent_ref[:, own]
 
@@ -290,10 +293,12 @@
     sp_index = lax.axis_index("sp")
     odd = sp_index % 2
     far = halo + tokens
-    pad_ref[pl.ds(pl.multiple_of((1 - odd) * far, GRID_W), halo), : 2 * width] = recv_a_ref[...]
-    pad_ref[pl.ds(pl.multiple_of(odd * far, GRID_W), halo), : 2 * width] = recv_b_ref[...]
+    for recv_ref, side in ((recv_a_ref, 1 - odd), (recv_b_ref, odd)):
+        lane = chunk * 2 * width if recv_ref.shape[1] > 2 * width else 0
+        pad_ref[pl.ds(pl.multiple_of(side * far, GRID_W), halo), : 2 * width] = recv_ref[
+            :, lane : lane + 2 * width
+        ]
     pad_ref[halo : halo + tokens, : 2 * width] = kv_ref[...]
-    pad_ref[:, 2 * width :] = jnp.ones((tokens + 2 * halo, width), BF16)
     lane_head = lax.broadcasted_iota(jnp.int32, (1, width), 1) // HEAD_DIM
     picks = [(lane_head == h) for h in range(heads)]
     nt = (((1,), (1,)), ((), ()))
@@ -308,66 +313,66 @@
         return pl.ds(pl.multiple_of(start_of(g * group)[0] * GRID_W, GRID_W), span)
 
     def score(g):
-        left = []
-        for l in range(g * group, (g + 1) * group):
+        left, bias = [], []
+        first_start = start_of(g * group)[0]
+        for k in range(group):
+            l = g * group + k
             query = q_ref[l * GRID_W : (l + 1) * GRID_W, chunk * width : (chunk + 1) * width]
             left += [jnp.where(pick, query, BF16(0)) for pick in picks]
-        left = jnp.concatenate(left, axis=0)
-        score_ref[g, :span, :] = lax.dot_general(
-            pad_ref[window_of(g), :width], left, nt, preferred_element_type=F32
-        )
-        score_ref[g, span:, :] = lax.dot_general(
-            ctx_ref[:, :width], left, nt, preferred_element_type=F32
-        )
-
-    def weigh(g):
-        for k in range(group):
-            start, offset = start_of(g * group + k)
-            shift = start - start_of(g * group)[0]
-            lanes = slice(k * width, (k + 1) * width)
-            highest = jnp.max(score_ref[g, span:, lanes], axis=0, keepdims=True)
+            start, offset = start_of(l)
+            shift = start - first_start
             blocks = []
             for u in range(span // GRID_W):
                 row = jnp.clip(u - shift, 0, WIN_H - 1) + offset
                 block = table_ref[pl.ds(pl.multiple_of(row * GRID_W, GRID_W), GRID_W), :]
-                if u < k or u >= WIN_H:
+                if k == 0 and u >= WIN_H:
+                    block = jnp.full_like(block, MASKED)
+                elif u < k or u >= WIN_H:
                     block = jnp.where((u >= shift) & (u < shift + WIN_H), block, MASKED)
-                block = block + score_ref[g, u * GRID_W : (u + 1) * GRID_W, lanes]
                 blocks.append(block)
-                highest = jnp.maximum(highest, jnp.max(block, axis=0, keepdims=True))
-            for u, block in enumerate(blocks):
-                weight_ref[g, u * GRID_W : (u + 1) * GRID_W, lanes] = jnp.exp(
-                    block - highest
-                ).astype(BF16)
-            weight_ref[g, span:, lanes] = jnp.exp(score_ref[g, span:, lanes] - highest).astype(BF16)
-
-    def mix(g):
-        ctx_values = jnp.concatenate(
-            [ctx_ref[:, width:], jnp.ones((ctx_rows, width), BF16)], axis=1
+            bias.append(jnp.concatenate(blocks, axis=0))
+        left = jnp.concatenate(left, axis=0)
+        scores = jnp.concatenate(bias, axis=1) + lax.dot_general(
+            pad_ref[window_of(g), :width], left, nt, preferred_element_type=F32
         )
+        ctx_scores = lax.dot_general(ctx_ref[:, :width], left, nt, preferred_element_type=F32)
+        score_ref[g, :span, :] = scores
+        score_ref[g, span:, :] = ctx_scores
+        return jnp.maximum(
+            jnp.max(scores, axis=0, keepdims=True), jnp.max(ctx_scores, axis=0, keepdims=True)
+        )
+
+    def weigh(g, highest):
+        partial = None
+        for at in range(0, keys, 32):
+            weights = jnp.exp2(score_ref[g, at : at + 32, :] - highest)
+            weight_ref[g, at : at + 32, :] = weights.astype(BF16)
+            folded = jnp.sum(weights.reshape(4, 8, -1), axis=0)
+            partial = folded if partial is None else partial + folded
+        return 1.0 / jnp.sum(partial, axis=0, keepdims=True)
+
+    def mix(g, scale):
         mixed = lax.dot_general(
-            weight_ref[g, :span, :],
-            pad_ref[window_of(g), width:],
-            tn,
-            preferred_element_type=F32,
-        ) + lax.dot_general(weight_ref[g, span:, :], ctx_values, tn, preferred_element_type=F32)
-        mixed = mixed[:, :width] / mixed[:, width:]
+            pad_ref[window_of(g), width:], weight_ref[g, :span, :], tn, preferred_element_type=F32
+        ) + lax.dot_general(
+            ctx_ref[:, width:], weight_ref[g, span:, :], tn, preferred_element_type=F32
+        )
+        mixed = mixed * scale
         for k in range(group):
-            low = k * heads * GRID_W
-            result = mixed[low : low + GRID_W]
+            turned = mixed[:, k * width : (k + 1) * width].T
+            result = turned[:GRID_W]
             for h in range(1, heads):
-                low += GRID_W
-                result = jnp.where(picks[h], mixed[low : low + GRID_W], result)
+                result = jnp.where(picks[h], turned[h * GRID_W : (h + 1) * GRID_W], result)
             l = g * group + k
             out_ref[l * GRID_W : (l + 1) * GRID_W, :] = result.astype(BF16)
 
+    highest = [score(g) for g in range(groups)]
+    scales = []
     for g in range(groups):
-        score(g)
-    for g in range(groups):
-        weigh(g)
+        scales.append(weigh(g, highest[g]))
         if g > 0:
-            mix(g - 1)
-    mix(groups - 1)
+            mix(g - 1, scales[g - 1])
+    mix(groups - 1, scales[-1])
 
 
 def output_kernel(*refs, masks, chunk, chunks):
@@ -414,7 +419,7 @@
     heads = width // HEAD_DIM
     chunks = width // 128 if width % 128 == 0 else 1
     each = width // chunks
-    sp_count = lax.axis_size("sp")
+    sp_count, tp_count = lax.axis_size("sp"), lax.axis_size("tp")
     halo = HALO * GRID_W
 
     own_context = shape_of((context.shape[0], cols), BF16)
@@ -446,24 +451,18 @@
     )(latent, *in_hbm((norm_gain, w_key, w_value)), *vectors)
     weights, tables = prepared[:chunks], prepared[chunks:]
 
-    kv_shapes = (
-        shape_of((tokens, 2 * each), BF16),
-        shape_of((halo, 2 * each), BF16),
-        shape_of((halo, 2 * each), BF16),
-    )
-    normed, kv_0, send_a_0, send_b_0, mod = call(
-        norm_kernel,
-        (shape_of((tokens, model), BF16),) + kv_shapes + (shape_of((MOD_ROWS, model), F32),),
+    evens, odds = 1, chunks
+    normed, mod, *projected = call(
+        functools.partial(norm_kernel, chunks=chunks, tp_count=tp_count, evens=evens),
+        (shape_of((tokens, model), BF16), shape_of((MOD_ROWS, model), F32))
+        + (shape_of((tokens, 2 * each), BF16),) * chunks
+        + (shape_of((halo, 2 * width // evens), BF16),) * evens
+        + (shape_of((halo, 2 * width // odds), BF16),) * odds,
         scratch=[pltpu.VMEM((8, model), F32), pltpu.VMEM((8, model), F32)],
-    )(latent, inverse, gain, weights[0], *mod_pieces)
-
-    keys_values = [(kv_0, send_a_0, send_b_0)]
-    for c in range(1, chunks):
-        keys_values.append(call(chunk_kernel, kv_shapes)(normed, weights[c]))
-    halos = [
-        (pairwise(a, "sp", 0), pairwise(b, "sp", 1))
-        for _, a, b in keys_values
-    ]
+    )(latent, inverse, gain, *weights, *mod_pieces)
+    keys_values, sends = projected[:chunks], projected[chunks:]
+    from_even = [pairwise(s, "sp", 0) for s in sends[:evens]]
+    from_odd = [pairwise(s, "sp", 1) for s in sends[evens:]]
 
     query, resid = call(
         query_kernel, (shape_of((tokens, width), BF16), shape_of((tokens, cols), BF16))
@@ -487,11 +486,18 @@
             functools.partial(attention_kernel, chunk=c, sp_count=sp_count),
             shape_of((tokens, each), BF16),
             scratch=[
-                pltpu.VMEM((tokens + 2 * halo, 3 * each), BF16),
+                pltpu.VMEM((tokens + 2 * halo, 2 * each), BF16),
                 pltpu.VMEM((rows // group, keys, group * each), F32),
                 pltpu.VMEM((rows // group, keys, group * each), BF16),
             ],
-        )(query, keys_values[c][0], *halos[c], tables[c], ctx_all[c])
+        )(
+            query,
+            keys_values[c],
+            from_even[min(c, evens - 1)],
+            from_odd[min(c, odds - 1)],
+            tables[c],
+            ctx_all[c],
+        )
         found = pieces_by_bits(attended, "tp")
         last = c == chunks - 1
         branch = [

time: 37.7 us -> 37.4 us (level)
  waiting for transfers between devices: 8.58 us -> 13.9 us
  starting transfers between devices: 17.6 us -> 12.6 us
  Pallas kernels: 11 us -> 10.2 us
    ppermute x4 -> x3, starting transfers between devices: 5.42 us -> 1.4 us  [pairwise(): return lax.ppermute(block, axis, pairs)]
    ppermute x15, waiting for transfers between devices: 8.57 us -> 11.8 us  [peer(): return lax.ppermute(block, axis, [(i, i ^ mask) for i in range(count)])]
    ppermute x4 -> x3, waiting for transfers between devices: 0.01 us -> 2.1 us  [pairwise(): return lax.ppermute(block, axis, pairs)]
    ppermute x15, starting transfers between devices: 12.1 us -> 11.2 us  [peer(): return lax.ppermute(block, axis, [(i, i ^ mask) for i in range(count)])]
    pallas_call x2, Pallas kernels: 2.8 us -> 2.18 us  [local(): call(functools.partial(attention_kernel, chunk=c, sp_count=sp_count), sha...]
    pallas_call x2 -> x1, Pallas kernels: 1.9 us -> 1.69 us  [local(): call(functools.partial(norm_kernel, chunks=chunks, tp_count=tp_count, eve...]
  transfers between devices with their start and end apart: 19 -> 18, of which waited for: 6 -> 10; matrix products, arithmetic and copies ran while one was open for 0% -> 0% of each run, Pallas kernels for 21% -> 15%
where the time goes in v7:
time: 37.4 us; the launch traced here: 37 us
  waiting for transfers between devices  13.9 us (37%)
  starting transfers between devices  12.6 us (34%)
  Pallas kernels  10.2 us (27%)
    ppermute x15, waiting for transfers between devices, peer(): return lax.ppermute(block, axis, [(i, i ^ mask) for i in range(count)])  11.8 us
    ppermute x15, starting transfers between devices, peer(): return lax.ppermute(block, axis, [(i, i ^ mask) for i in range(count)])  11.2 us
    pallas_call x2, Pallas kernels, local(): call(functools.partial(attention_kernel, chunk=c, sp_count=sp_count), sha...  2.18 us
    ppermute x3, waiting for transfers between devices, pairwise(): return lax.ppermute(block, axis, pairs)  2.1 us
    pallas_call x1, Pallas kernels, local(): call(functools.partial(prepare_kernel, chunks=chunks), (shape_of((tokens,...  1.82 us
    pallas_call x1, Pallas kernels, local(): call(modulation_kernel, shape_of((2 * MOD_ROWS + context.shape[0], cols),...  1.8 us
    pallas_call x1, Pallas kernels, local(): call(functools.partial(norm_kernel, chunks=chunks, tp_count=tp_count, eve...  1.69 us
    pallas_call x2, Pallas kernels, local(): call(functools.partial(output_kernel, masks=[m for m, _ in found], chunk=...  1.5 us
  transfers between devices with their start and end apart: 18, of which 10 were waited for; matrix products, arithmetic and copies ran while one was open for 0% of the time, Pallas kernels for 15%

profile of v7, /device:TPU:0, one launch (start us, length us, event | category | flops | bytes accessed | tf_op | source)
XLA Modules:
  0.0 37.0 jit_solution(349314373180185513)
XLA Ops:
  0.0 1.8 %shard_map.128 = bf16[32,512]{1,0:T(8,128)(2,1)S(1)} custom-call(bf16[512]{0:T(512)(128)(2,1)} %cond_hbm.1, bf16[512]{0:T(512)(128)(2,1)} %ctx_hbm.1, bf16[512,512]{1,0:T(8,128)(2,1)} %w_shift_hbm.1, bf16[512,512]{1,0:T(8,128)(2,1)} %w_scale_hbm.1, bf16[512,512]{1,0:T(8,128)(2,1)} %w_gate_hbm.1, bf16[16,2048]{1,0:T(8,128)(2,1)} %context_hbm.1), custom_call_target="tpu_custom_call" | custom-call | tf_op jit(solution)/shard_map/pallas_call | solution.py:427
  1.8 5.1 %collective-permute-start = (bf16[32,512]{1,0:T(8,128)(2,1)S(1)}, bf16[32,512]{1,0:T(8,128)(2,1)S(1)}, u32[]{:S(2)}, u32[]{:S(2)}) collective-permute-start(bf16[32,512]{1,0:T(8,128)(2,1)S(1)} %shard_map.128), channel_id=1, source_target_pairs={{0,12},{4,8},{8,4},{12,0},{1,13},{5,9},{9,5},{13,1},{2,14},{6,10},... | collective-permute-start | bytes 98312 | tf_op jit(solution)/shard_map/ppermute | solution.py:56
  7.0 0.6 %collective-permute-start.2 = (bf16[32,512]{1,0:T(8,128)(2,1)S(1)}, bf16[32,512]{1,0:T(8,128)(2,1)S(1)}, u32[]{:S(2)}, u32[]{:S(2)}) collective-permute-start(bf16[32,512]{1,0:T(8,128)(2,1)S(1)} %shard_map.128), channel_id=1, source_target_pairs={{0,4},{4,0},{8,12},{12,8},{1,5},{5,1},{9,13},{13,9},{2,6},{6,2},{1... | collective-permute-start | bytes 98312 | tf_op jit(solution)/shard_map/ppermute | solution.py:56
  7.6 0.1 rev.3
  7.7 1.2 %collective-permute-done = bf16[32,512]{1,0:T(8,128)(2,1)S(1)} collective-permute-done((bf16[32,512]{1,0:T(8,128)(2,1)S(1)}, bf16[32,512]{1,0:T(8,128)(2,1)S(1)}, u32[]{:S(2)}, u32[]{:S(2)}) %collective-permute-start) | collective-permute-done | bytes 32800 | tf_op jit(solution)/shard_map/ppermute | solution.py:56
  8.9 2.9 %collective-permute-done.1 = bf16[32,512]{1,0:T(8,128)(2,1)S(1)} collective-permute-done((bf16[32,512]{1,0:T(8,128)(2,1)S(1)}, bf16[32,512]{1,0:T(8,128)(2,1)S(1)}, u32[]{:S(2)}, u32[]{:S(2)}) %collective-permute-start.1) | collective-permute-done | bytes 32800 | tf_op jit(solution)/shard_map/ppermute | solution.py:56
  11.8 0.1 collective-permute-start.3
  11.9 1.6 %collective-permute-start.4 = (f32[8,512]{1,0:T(8,128)S(1)}, f32[8,512]{1,0:T(8,128)S(1)}, u32[]{:S(2)}, u32[]{:S(2)}) collective-permute-start(f32[8,512]{1,0:T(8,128)S(1)} %add_add_fusion.refs_5_.refs_7_), channel_id=1, source_target_pairs={{0,2},{1,3},{2,0},{3,1},{4,6},{5,7},{6,4},{7,5},{8,10},{9,11},{10,... | collective-permute-start | bytes 49160 | tf_op jit(solution)/shard_map/ppermute | solution.py:56
  13.4 0.3 collective-permute-start.5
  13.7 0.1 pad_maximum_fusion.1
  13.8 1.8 %shard_map.127 = (f32[384,128]{1,0:T(8,128)S(1)}, f32[8,2048]{1,0:T(8,128)S(1)}, bf16[2048,256]{1,0:T(8,128)(2,1)S(1)}, bf16[2048,256]{1,0:T(8,128)(2,1)S(1)}, f...) custom-call(bf16[384,2048]{1,0:T(8,128)(2,1)S(1)} %copy-done, bf16[2048]{0:T(1024)(128)(2,1)} %refs_1_.1, ...), custom_call_target="tpu_custom_call" | custom-call | tf_op jit(solution)/shard_map/pallas_call | solution.py:444
  15.7 0.9 %collective-permute-done.5.refs_8_ = f32[8,512]{1,0:T(8,128)S(1)} collective-permute-done((f32[8,512]{1,0:T(8,128)S(1)}, f32[8,512]{1,0:T(8,128)S(1)}, u32[]{:S(2)}, u32[]{:S(2)}) %collective-permute-start.5) | collective-permute-done | bytes 16416 | tf_op jit(solution)/shard_map/ppermute | solution.py:56
  16.6 1.7 %shard_map.129 = (bf16[384,2048]{1,0:T(8,128)(2,1)S(1)}, f32[8,2048]{1,0:T(8,128)S(1)}, bf16[384,256]{1,0:T(8,128)(2,1)S(1)}, bf16[384,256]{1,0:T(8,128)(2,1)S(1...) custom-call(bf16[384,2048]{1,0:T(8,128)(2,1)S(1)} %copy-done, ...), custom_call_target="tpu_custom_call" | custom-call | tf_op jit(solution)/shard_map/pallas_call | solution.py:455
  18.4 0.8 %collective-permute-start.8 = (bf16[64,512]{1,0:T(8,128)(2,1)S(1)}, bf16[64,512]{1,0:T(8,128)(2,1)S(1)}, u32[]{:S(2)}, u32[]{:S(2)}) collective-permute-start(bf16[64,512]{1,0:T(8,128)(2,1)S(1)} %pad_maximum_fusion.refs_2_), channel_id=1, source_target_pairs={{0,2},{1,3},{2,0},{3,1},{4,6},{5,7},{6,4},{7,5},{8,10},{9,11},{10,... | collective-permute-start | bytes 196616 | tf_op jit(solution)/shard_map/ppermute | solution.py:56
  19.2 0.7 %collective-permute-start.14 = (bf16[256,256]{1,0:T(8,128)(2,1)S(1)}, bf16[256,256]{1,0:T(8,128)(2,1)S(1)}, u32[]{:S(2)}, u32[]{:S(2)}) collective-permute-start(bf16[256,256]{1,0:T(8,128)(2,1)S(1)} %get-tuple-element.35), channel_id=1, source_target_pairs={{4,8},{8,4},{5,9},{9,5},{6,10},{10,6},{7,11},{11,7},{20,24},{24,20... | collective-permute-start | bytes 393224 | tf_op jit(solution)/shard_map/ppermute | solution.py:100
  19.9 0.7 %collective-permute-start.7 = (bf16[256,256]{1,0:T(8,128)(2,1)S(1)}, bf16[256,256]{1,0:T(8,128)(2,1)S(1)}, u32[]{:S(2)}, u32[]{:S(2)}) collective-permute-start(bf16[256,256]{1,0:T(8,128)(2,1)S(1)} %get-tuple-element.30), channel_id=1, source_target_pairs={{4,8},{8,4},{5,9},{9,5},{6,10},{10,6},{7,11},{11,7},{20,24},{24,20... | collective-permute-start | bytes 393224 | tf_op jit(solution)/shard_map/ppermute | solution.py:100
  20.6 2.1 %collective-permute-done.8.refs_3_ = bf16[64,512]{1,0:T(8,128)(2,1)S(1)} collective-permute-done((bf16[64,512]{1,0:T(8,128)(2,1)S(1)}, bf16[64,512]{1,0:T(8,128)(2,1)S(1)}, u32[]{:S(2)}, u32[]{:S(2)}) %collective-permute-start.8) | collective-permute-done | bytes 65568 | tf_op jit(solution)/shard_map/ppermute | solution.py:56
  22.8 0.6 %shard_map.130 = (bf16[384,256]{1,0:T(8,128)(2,1)S(1)}, bf16[384,512]{1,0:T(8,128)(2,1)S(1)}) custom-call(bf16[384,2048]{1,0:T(8,128)(2,1)S(1)} %get-tuple-element.26.normed_ref, bf16[2048,256]{1,0:T(8,128)(2,1)S(1)} %copy-done.2, bf16[384,2048]{1,0:T(8,128)(2,1)S(1)} %copy-done), custom_call_target="tpu_custom_call" | custom-call | tf_op jit(solution)/shard_map/pallas_call | solution.py:467
  23.4 0.7 %collective-permute-done.10.refs_5_ = bf16[64,512]{1,0:T(8,128)(2,1)S(1)} collective-permute-done((bf16[64,512]{1,0:T(8,128)(2,1)S(1)}, bf16[64,512]{1,0:T(8,128)(2,1)S(1)}, u32[]{:S(2)}, u32[]{:S(2)}) %collective-permute-start.10) | collective-permute-done | bytes 65568 | tf_op jit(solution)/shard_map/ppermute | solution.py:56
  24.0 0.6 %shard_map.131 = (bf16[64,256]{1,0:T(8,128)(2,1)S(1)}, bf16[64,256]{1,0:T(8,128)(2,1)S(1)}) custom-call(f32[8,2048]{1,0:T(8,128)S(1)} %get-tuple-element.32.refs_0_, f32[8,2048]{1,0:T(8,128)S(1)} %get-tuple-element.23.refs_2_.refs_1_, bf16[64,512]{1,0:T(8,128)(2,1)S(1)} %pad_maximum_fusion.refs_2_, bf16[64,512]{1,0:T(8,128)(2,1)S(1)} %collective-permute-done.8.refs_3_, ...), custom_call_target="tpu_custom_call" | custom-call | tf_op jit(solution)/shard_map/pallas_call | solution.py:478
  24.6 2.1 %collective-permute-done.6.recv_a_ref = bf16[256,512]{1,0:T(8,128)(2,1)S(1)} collective-permute-done((bf16[256,512]{1,0:T(8,128)(2,1)S(1)}, bf16[256,512]{1,0:T(8,128)(2,1)S(1)}, u32[]{:S(2)}, u32[]{:S(2)}) %collective-permute-start.6) | collective-permute-done | bytes 262176 | tf_op jit(solution)/shard_map/ppermute | solution.py:100
  26.7 1.1 %shard_map.133.refs_1_ = bf16[384,128]{1,0:T(8,128)(2,1)S(1)} custom-call(bf16[384,256]{1,0:T(8,128)(2,1)S(1)} %get-tuple-element.27.q_ref, bf16[384,256]{1,0:T(8,128)(2,1)S(1)} %get-tuple-element.34.kv_ref, bf16[256,512]{1,0:T(8,128)(2,1)S(1)} %collective-permute-done.6.recv_a_ref, bf16[256,256]{1,0:T(8,128)(2,1)S(1)} %collective-permute-done.14.recv_b_ref, ...), custom_call_target="tpu_custom_call" | custom-call | tf_op jit(solution)/shard_map/pallas_call | solution.py:485
  27.8 0.9 %collective-permute-start.15 = (bf16[384,128]{1,0:T(8,128)(2,1)S(1)}, bf16[384,128]{1,0:T(8,128)(2,1)S(1)}, u32[]{:S(2)}, u32[]{:S(2)}) collective-permute-start(bf16[384,128]{1,0:T(8,128)(2,1)S(1)} %shard_map.133.refs_1_), channel_id=1, source_target_pairs={{0,2},{1,3},{2,0},{3,1},{4,6},{5,7},{6,4},{7,5},{8,10},{9,11},{10,... | collective-permute-start | bytes 294920 | tf_op jit(solution)/shard_map/ppermute | solution.py:56
  28.7 1.1 %shard_map.132.refs_1_ = bf16[384,128]{1,0:T(8,128)(2,1)S(1)} custom-call(bf16[384,256]{1,0:T(8,128)(2,1)S(1)} %get-tuple-element.27.q_ref, bf16[384,256]{1,0:T(8,128)(2,1)S(1)} %get-tuple-element.28.kv_ref, bf16[256,512]{1,0:T(8,128)(2,1)S(1)} %collective-permute-done.6.recv_a_ref, bf16[256,256]{1,0:T(8,128)(2,1)S(1)} %collective-permute-done.7.recv_b_ref, ...), custom_call_target="tpu_custom_call" | custom-call | tf_op jit(solution)/shard_map/pallas_call | solution.py:485
  29.8 1.3 %collective-permute-start.11 = (bf16[384,128]{1,0:T(8,128)(2,1)S(1)}, bf16[384,128]{1,0:T(8,128)(2,1)S(1)}, u32[]{:S(2)}, u32[]{:S(2)}) collective-permute-start(bf16[384,128]{1,0:T(8,128)(2,1)S(1)} %shard_map.132.refs_1_), channel_id=1, source_target_pairs={{0,2},{1,3},{2,0},{3,1},{4,6},{5,7},{6,4},{7,5},{8,10},{9,11},{10,... | collective-permute-start | bytes 294920 | tf_op jit(solution)/shard_map/ppermute | solution.py:56
  31.1 2.4 %collective-permute-done.15.refs_2_ = bf16[384,128]{1,0:T(8,128)(2,1)S(1)} collective-permute-done((bf16[384,128]{1,0:T(8,128)(2,1)S(1)}, bf16[384,128]{1,0:T(8,128)(2,1)S(1)}, u32[]{:S(2)}, u32[]{:S(2)}) %collective-permute-start.15) | collective-permute-done | bytes 98336 | tf_op jit(solution)/shard_map/ppermute | solution.py:56
  33.5 0.5 %collective-permute-start.12 = (bf16[384,128]{1,0:T(8,128)(2,1)S(1)}, bf16[384,128]{1,0:T(8,128)(2,1)S(1)}, u32[]{:S(2)}, u32[]{:S(2)}) collective-permute-start(bf16[384,128]{1,0:T(8,128)(2,1)S(1)} %shard_map.132.refs_1_), channel_id=1, source_target_pairs={{0,1},{1,0},{2,3},{3,2},{4,5},{5,4},{6,7},{7,6},{8,9},{9,8},{10,11... | collective-permute-start | bytes 294920 | tf_op jit(solution)/shard_map/ppermute | solution.py:56
  34.0 0.6 %collective-permute-done.11.refs_2_ = bf16[384,128]{1,0:T(8,128)(2,1)S(1)} collective-permute-done((bf16[384,128]{1,0:T(8,128)(2,1)S(1)}, bf16[384,128]{1,0:T(8,128)(2,1)S(1)}, u32[]{:S(2)}, u32[]{:S(2)}) %collective-permute-start.11) | collective-permute-done | bytes 98336 | tf_op jit(solution)/shard_map/ppermute | solution.py:56
  34.6 0.2 collective-permute-done.17.refs_4_
  34.8 0.4 shard_map.134.refs_5_
  35.2 0.7 %collective-permute-done.13.refs_4_ = bf16[384,128]{1,0:T(8,128)(2,1)S(1)} collective-permute-done((bf16[384,128]{1,0:T(8,128)(2,1)S(1)}, bf16[384,128]{1,0:T(8,128)(2,1)S(1)}, u32[]{:S(2)}, u32[]{:S(2)}) %collective-permute-start.13) | collective-permute-done | bytes 98336 | tf_op jit(solution)/shard_map/ppermute | solution.py:56
  35.9 1.1 %shard_map.135 = bf16[384,512]{1,0:T(8,128)(2,1)} custom-call(bf16[1024,512]{1,0:T(8,128)(2,1)S(1)} %copy-done.1, bf16[384,128]{1,0:T(8,128)(2,1)S(1)} %shard_map.132.refs_1_, bf16[384,128]{1,0:T(8,128)(2,1)S(1)} %collective-permute-done.11.refs_2_, bf16[384,128]{1,0:T(8,128)(2,1)S(1)} %collective-permute-done.12.refs_3_, ...), custom_call_target="tpu_custom_call" | custom-call | tf_op jit(solution)/shard_map/pallas_call | solution.py:504
  (31 shorter events, 0.3 us)
Async XLA Ops:
  0.0 7.6 %copy-start.3 = (f32[4,15,31]{2,0,1:T(4,128)S(1)}, f32[4,15,31]{2,0,1:T(4,128)}, u32[]{:S(2)}) copy-start(f32[4,15,31]{2,0,1:T(4,128)} %param.24) | copy-start | bytes 22324
  0.0 13.8 %copy-start = (bf16[384,2048]{1,0:T(8,128)(2,1)S(1)}, bf16[384,2048]{1,0:T(8,128)(2,1)}, u32[]{:S(2)}) copy-start(bf16[384,2048]{1,0:T(8,128)(2,1)} %latent_ref.1) | copy-start | bytes 4718596
  1.8 7.0 %collective-permute-start = (bf16[32,512]{1,0:T(8,128)(2,1)S(1)}, bf16[32,512]{1,0:T(8,128)(2,1)S(1)}, u32[]{:S(2)}, u32[]{:S(2)}) collective-permute-start(bf16[32,512]{1,0:T(8,128)(2,1)S(1)} %shard_map.128), channel_id=1, source_target_pairs={{0,12},{4,8},{8,4},{12,0},{1,13},{5,9},{9,5},{13,1},{2,14},{6,10},... | collective-permute-start | bytes 98312 | tf_op jit(solution)/shard_map/ppermute | solution.py:56
  7.0 4.8 %collective-permute-start.1 = (bf16[32,512]{1,0:T(8,128)(2,1)S(1)}, bf16[32,512]{1,0:T(8,128)(2,1)S(1)}, u32[]{:S(2)}, u32[]{:S(2)}) collective-permute-start(bf16[32,512]{1,0:T(8,128)(2,1)S(1)} %shard_map.128), channel_id=1, source_target_pairs={{0,8},{4,12},{8,0},{12,4},{1,9},{5,13},{9,1},{13,5},{2,10},{6,14},... | collective-permute-start | bytes 98312 | tf_op jit(solution)/shard_map/ppermute | solution.py:56
  7.0 4.8 %collective-permute-start.2 = (bf16[32,512]{1,0:T(8,128)(2,1)S(1)}, bf16[32,512]{1,0:T(8,128)(2,1)S(1)}, u32[]{:S(2)}, u32[]{:S(2)}) collective-permute-start(bf16[32,512]{1,0:T(8,128)(2,1)S(1)} %shard_map.128), channel_id=1, source_target_pairs={{0,4},{4,0},{8,12},{12,8},{1,5},{5,1},{9,13},{13,9},{2,6},{6,2},{1... | collective-permute-start | bytes 98312 | tf_op jit(solution)/shard_map/ppermute | solution.py:56
  11.8 3.8 %collective-permute-start.3 = (f32[8,512]{1,0:T(8,128)S(1)}, f32[8,512]{1,0:T(8,128)S(1)}, u32[]{:S(2)}, u32[]{:S(2)}) collective-permute-start(f32[8,512]{1,0:T(8,128)S(1)} %add_add_fusion.refs_5_.refs_7_), channel_id=1, source_target_pairs={{0,1},{1,0},{2,3},{3,2},{4,5},{5,4},{6,7},{7,6},{8,9},{9,8},{10,11... | collective-permute-start | bytes 49160 | tf_op jit(solution)/shard_map/ppermute | solution.py:56
  11.9 3.8 %collective-permute-start.4 = (f32[8,512]{1,0:T(8,128)S(1)}, f32[8,512]{1,0:T(8,128)S(1)}, u32[]{:S(2)}, u32[]{:S(2)}) collective-permute-start(f32[8,512]{1,0:T(8,128)S(1)} %add_add_fusion.refs_5_.refs_7_), channel_id=1, source_target_pairs={{0,2},{1,3},{2,0},{3,1},{4,6},{5,7},{6,4},{7,5},{8,10},{9,11},{10,... | collective-permute-start | bytes 49160 | tf_op jit(solution)/shard_map/ppermute | solution.py:56
  13.4 3.2 %collective-permute-start.5 = (f32[8,512]{1,0:T(8,128)S(1)}, f32[8,512]{1,0:T(8,128)S(1)}, u32[]{:S(2)}, u32[]{:S(2)}) collective-permute-start(f32[8,512]{1,0:T(8,128)S(1)} %add_add_fusion.refs_5_.refs_7_), channel_id=1, source_target_pairs={{0,3},{1,2},{2,1},{3,0},{4,7},{5,6},{6,5},{7,4},{8,11},{9,10},{10,... | collective-permute-start | bytes 49160 | tf_op jit(solution)/shard_map/ppermute | solution.py:56
  16.6 6.2 %copy-start.2 = (bf16[2048,256]{1,0:T(8,128)(2,1)S(1)}, bf16[2048,256]{1,0:T(8,128)(2,1)}, u32[]{:S(2)}) copy-start(bf16[2048,256]{1,0:T(8,128)(2,1)} %wq_ref.1) | copy-start | bytes 3145732
  18.3 8.4 %collective-permute-start.6 = (bf16[256,512]{1,0:T(8,128)(2,1)S(1)}, bf16[256,512]{1,0:T(8,128)(2,1)S(1)}, u32[]{:S(2)}, u32[]{:S(2)}) collective-permute-start(bf16[256,512]{1,0:T(8,128)(2,1)S(1)} %get-tuple-element.29), channel_id=1, source_target_pairs={{0,4},{4,0},{8,12},{12,8},{1,5},{5,1},{9,13},{13,9},{2,6},{6,2},{1... | collective-permute-start | bytes 786440 | tf_op jit(solution)/shard_map/ppermute | solution.py:100
  18.4 4.3 %collective-permute-start.8 = (bf16[64,512]{1,0:T(8,128)(2,1)S(1)}, bf16[64,512]{1,0:T(8,128)(2,1)S(1)}, u32[]{:S(2)}, u32[]{:S(2)}) collective-permute-start(bf16[64,512]{1,0:T(8,128)(2,1)S(1)} %pad_maximum_fusion.refs_2_), channel_id=1, source_target_pairs={{0,2},{1,3},{2,0},{3,1},{4,6},{5,7},{6,4},{7,5},{8,10},{9,11},{10,... | collective-permute-start | bytes 196616 | tf_op jit(solution)/shard_map/ppermute | solution.py:56
  19.2 5.4 %collective-permute-start.14 = (bf16[256,256]{1,0:T(8,128)(2,1)S(1)}, bf16[256,256]{1,0:T(8,128)(2,1)S(1)}, u32[]{:S(2)}, u32[]{:S(2)}) collective-permute-start(bf16[256,256]{1,0:T(8,128)(2,1)S(1)} %get-tuple-element.35), channel_id=1, source_target_pairs={{4,8},{8,4},{5,9},{9,5},{6,10},{10,6},{7,11},{11,7},{20,24},{24,20... | collective-permute-start | bytes 393224 | tf_op jit(solution)/shard_map/ppermute | solution.py:100
  19.9 8.8 %collective-permute-start.7 = (bf16[256,256]{1,0:T(8,128)(2,1)S(1)}, bf16[256,256]{1,0:T(8,128)(2,1)S(1)}, u32[]{:S(2)}, u32[]{:S(2)}) collective-permute-start(bf16[256,256]{1,0:T(8,128)(2,1)S(1)} %get-tuple-element.30), channel_id=1, source_target_pairs={{4,8},{8,4},{5,9},{9,5},{6,10},{10,6},{7,11},{11,7},{20,24},{24,20... | collective-permute-start | bytes 393224 | tf_op jit(solution)/shard_map/ppermute | solution.py:100
  20.5 2.8 %collective-permute-start.9 = (bf16[64,512]{1,0:T(8,128)(2,1)S(1)}, bf16[64,512]{1,0:T(8,128)(2,1)S(1)}, u32[]{:S(2)}, u32[]{:S(2)}) collective-permute-start(bf16[64,512]{1,0:T(8,128)(2,1)S(1)} %pad_maximum_fusion.refs_2_), channel_id=1, source_target_pairs={{0,1},{1,0},{2,3},{3,2},{4,5},{5,4},{6,7},{7,6},{8,9},{9,8},{10,11... | collective-permute-start | bytes 196616 | tf_op jit(solution)/shard_map/ppermute | solution.py:56
  22.8 1.3 %collective-permute-start.10 = (bf16[64,512]{1,0:T(8,128)(2,1)S(1)}, bf16[64,512]{1,0:T(8,128)(2,1)S(1)}, u32[]{:S(2)}, u32[]{:S(2)}) collective-permute-start(bf16[64,512]{1,0:T(8,128)(2,1)S(1)} %collective-permute-done.8.refs_3_), channel_id=1, source_target_pairs={{0,1},{1,0},{2,3},{3,2},{4,5},{5,4},{6,7},{7,6},{8,9},{9,8},{10,11... | collective-permute-start | bytes 196616 | tf_op jit(solution)/shard_map/ppermute | solution.py:56
  24.6 10.2 %copy-start.1 = (bf16[1024,512]{1,0:T(8,128)(2,1)S(1)}, bf16[1024,512]{1,0:T(8,128)(2,1)}, u32[]{:S(2)}) copy-start(bf16[1024,512]{1,0:T(8,128)(2,1)} %refs_0_.7) | copy-start | bytes 3145732
  27.8 5.7 %collective-permute-start.15 = (bf16[384,128]{1,0:T(8,128)(2,1)S(1)}, bf16[384,128]{1,0:T(8,128)(2,1)S(1)}, u32[]{:S(2)}, u32[]{:S(2)}) collective-permute-start(bf16[384,128]{1,0:T(8,128)(2,1)S(1)} %shard_map.133.refs_1_), channel_id=1, source_target_pairs={{0,2},{1,3},{2,0},{3,1},{4,6},{5,7},{6,4},{7,5},{8,10},{9,11},{10,... | collective-permute-start | bytes 294920 | tf_op jit(solution)/shard_map/ppermute | solution.py:56
  29.8 4.8 %collective-permute-start.11 = (bf16[384,128]{1,0:T(8,128)(2,1)S(1)}, bf16[384,128]{1,0:T(8,128)(2,1)S(1)}, u32[]{:S(2)}, u32[]{:S(2)}) collective-permute-start(bf16[384,128]{1,0:T(8,128)(2,1)S(1)} %shard_map.132.refs_1_), channel_id=1, source_target_pairs={{0,2},{1,3},{2,0},{3,1},{4,6},{5,7},{6,4},{7,5},{8,10},{9,11},{10,... | collective-permute-start | bytes 294920 | tf_op jit(solution)/shard_map/ppermute | solution.py:56
  31.1 3.5 %collective-permute-start.16 = (bf16[384,128]{1,0:T(8,128)(2,1)S(1)}, bf16[384,128]{1,0:T(8,128)(2,1)S(1)}, u32[]{:S(2)}, u32[]{:S(2)}) collective-permute-start(bf16[384,128]{1,0:T(8,128)(2,1)S(1)} %shard_map.133.refs_1_), channel_id=1, source_target_pairs={{0,1},{1,0},{2,3},{3,2},{4,5},{5,4},{6,7},{7,6},{8,9},{9,8},{10,11... | collective-permute-start | bytes 294920 | tf_op jit(solution)/shard_map/ppermute | solution.py:56
  33.5 1.3 %collective-permute-start.17 = (bf16[384,128]{1,0:T(8,128)(2,1)S(1)}, bf16[384,128]{1,0:T(8,128)(2,1)S(1)}, u32[]{:S(2)}, u32[]{:S(2)}) collective-permute-start(bf16[384,128]{1,0:T(8,128)(2,1)S(1)} %collective-permute-done.15.refs_2_), channel_id=1, source_target_pairs={{0,1},{1,0},{2,3},{3,2},{4,5},{5,4},{6,7},{7,6},{8,9},{9,8},{10,11... | collective-permute-start | bytes 294920 | tf_op jit(solution)/shard_map/ppermute | solution.py:56
  33.5 1.7 %collective-permute-start.12 = (bf16[384,128]{1,0:T(8,128)(2,1)S(1)}, bf16[384,128]{1,0:T(8,128)(2,1)S(1)}, u32[]{:S(2)}, u32[]{:S(2)}) collective-permute-start(bf16[384,128]{1,0:T(8,128)(2,1)S(1)} %shard_map.132.refs_1_), channel_id=1, source_target_pairs={{0,1},{1,0},{2,3},{3,2},{4,5},{5,4},{6,7},{7,6},{8,9},{9,8},{10,11... | collective-permute-start | bytes 294920 | tf_op jit(solution)/shard_map/ppermute | solution.py:56
  34.6 1.3 %collective-permute-start.13 = (bf16[384,128]{1,0:T(8,128)(2,1)S(1)}, bf16[384,128]{1,0:T(8,128)(2,1)S(1)}, u32[]{:S(2)}, u32[]{:S(2)}) collective-permute-start(bf16[384,128]{1,0:T(8,128)(2,1)S(1)} %collective-permute-done.11.refs_2_), channel_id=1, source_target_pairs={{0,1},{1,0},{2,3},{3,2},{4,5},{5,4},{6,7},{7,6},{8,9},{9,8},{10,11... | collective-permute-start | bytes 294920 | tf_op jit(solution)/shard_map/ppermute | solution.py:56

commit v8 on v7

--- a/solution.py
+++ b/solution.py
@@ -15,6 +15,8 @@
 EPSILON = 1e-06
 HALO = WIN_H // 2
 MASKED = -1e30
+OUT_BLOCKS = 3
+PARTS = 1
 LOG2_E = 1.4426950408889634
 SHIFT, CTX_SHIFT, SCALE, CTX_SCALE, GATE, MOD_ROWS = 0, 1, 2, 3, 4, 8
 
@@ -113,31 +115,46 @@
     return copies
 
 
+def in_parts(source, target):
+    step = target.shape[0] // PARTS
+    parts = [pl.ds(i * step, step) for i in range(PARTS)]
+    return [(source.at[at, :], target.at[at, :]) for at in parts]
+
+
 def modulation_kernel(
     cond_hbm, ctx_hbm, w_shift_hbm, w_scale_hbm, w_gate_hbm, context_hbm, out_ref, *scratch
 ):
     cond_ref, ctx_ref, w_shift_ref, w_scale_ref, w_gate_ref, context_ref, sems = scratch
     cols = w_shift_ref.shape[1]
     own = pl.ds(pl.multiple_of(lax.axis_index("tp") * cols, 128), cols)
-    sources = (cond_hbm, ctx_hbm, w_shift_hbm, w_scale_hbm, w_gate_hbm, context_hbm.at[:, own])
-    copies = fetch(list(zip(sources, scratch[:-1])), sems)
+    pairs = [(cond_hbm, cond_ref), (ctx_hbm, ctx_ref)]
+    for source, target in (
+        (w_shift_hbm, w_shift_ref),
+        (w_scale_hbm, w_scale_ref),
+        (w_gate_hbm, w_gate_ref),
+    ):
+        pairs += in_parts(source, target)
+    copies = fetch(pairs + [(context_hbm.at[:, own], context_ref)], sems)
     copies[0].wait()
     copies[1].wait()
+
+    def product(weight_ref, at):
+        for copy in copies[2 + at * PARTS : 2 + (at + 1) * PARTS]:
+            copy.wait()
+        return jnp.dot(acts, weight_ref[...], preferred_element_type=F32)
+
     cond = silu(cond_ref[...].astype(F32)).reshape(1, -1)
     ctx = silu(ctx_ref[...].astype(F32)).reshape(1, -1)
     row = lax.broadcasted_iota(jnp.int32, (MOD_ROWS, cond.shape[1]), 0)
     acts = jnp.where(row % 2 == 0, cond, ctx).astype(BF16)
-    copies[2].wait()
-    shifts = jnp.dot(acts, w_shift_ref[...], preferred_element_type=F32)
-    copies[3].wait()
-    scales = jnp.dot(acts, w_scale_ref[...], preferred_element_type=F32)
-    copies[4].wait()
-    gates = jnp.dot(acts, w_gate_ref[...], preferred_element_type=F32)
+    shifts = product(w_shift_ref, 0)
+    scales = product(w_scale_ref, 1)
+    gates = product(w_gate_ref, 2)
     out_row = lax.broadcasted_iota(jnp.int32, shifts.shape, 0)
     sums = jnp.where(out_row < SCALE, shifts, jnp.where(out_row < GATE, scales, gates))
     high = sums.astype(BF16).astype(F32)
     out_ref[: 2 * MOD_ROWS, :] = jnp.concatenate([high, sums - high], axis=0).astype(BF16)
-    copies[5].wait()
+    copies[-1].wait()
     out_ref[2 * MOD_ROWS :, :] = context_ref[...]
 
 
@@ -375,27 +392,35 @@
     mix(groups - 1, scales[-1])
 
 
-def output_kernel(*refs, masks, chunk, chunks):
-    count = len(masks)
-    w_out_ref, piece_refs = refs[0], refs[1 : 1 + count]
-    more, out_ref = list(refs[1 + count : -1]), refs[-1]
+def output_kernel(*refs, places, blocks):
+    w_out_ref, mod_ref, before_ref = refs[:3]
+    piece_refs, more = refs[3 : 3 + len(places)], refs[3 + len(places) :]
     tp_index = lax.axis_index("tp")
     each = piece_refs[0].shape[1]
     rows = [
-        w_out_ref[pl.ds(pl.multiple_of(((tp_index ^ m) * chunks + chunk) * each, 128), each), :]
-        for m in masks
+        w_out_ref[pl.ds(pl.multiple_of(((tp_index ^ mask) * of + chunk) * each, 128), each), :]
+        for mask, chunk, of in places
     ]
-    branch = jnp.dot(
-        jnp.concatenate([piece[...] for piece in piece_refs], axis=1),
-        jnp.concatenate(rows, axis=0),
-        preferred_element_type=F32,
-    )
-    if chunk > 0:
-        branch = branch + more.pop(0)[...]
-    if chunk == chunks - 1:
-        resid_ref, mod_ref = more
-        branch = resid_ref[...].astype(F32) + mod_ref[GATE : GATE + 1, :] * branch
-    out_ref[...] = branch.astype(out_ref.dtype)
+    weight = jnp.concatenate(rows, axis=0)
+    gate = mod_ref[GATE : GATE + 1, :]
+
+    def updated(at):
+        pieces = jnp.concatenate([piece[at, :] for piece in piece_refs], axis=1)
+        product = jnp.dot(pieces, weight, preferred_element_type=F32)
+        return before_ref[at, :].astype(F32) + gate * product
+
+    if not blocks:
+        more[0][...] = updated(slice(None))
+        return
+    out_hbm, out_ref, sems = more
+    step = out_ref.shape[0] // blocks
+    copies = []
+    for i in range(blocks):
+        at = pl.ds(i * step, step)
+        out_ref[at, :] = updated(at).astype(BF16)
+        copies += fetch([(out_ref.at[at, :], out_hbm.at[at, :])], sems.at[pl.ds(i, 1)])
+    for copy in copies:
+        copy.wait()
 
 
 def local(
@@ -428,7 +453,7 @@
         modulation_kernel,
         shape_of((2 * MOD_ROWS + context.shape[0], cols), BF16),
         scratch=[pltpu.VMEM(a.shape, a.dtype) for a in mod_inputs + (own_context,)]
-        + [pltpu.SemaphoreType.DMA((6,))],
+        + [pltpu.SemaphoreType.DMA((3 + 3 * PARTS,))],
         in_specs=[HBM] * 6,
     )(*in_hbm(mod_inputs + (context,)))
     mod_own, ctx_own = total_and_context(partial, "sp")
@@ -480,7 +505,7 @@
     rows = tokens // GRID_W
     group = 2 if rows % 2 == 0 else 1
     keys = (WIN_H + group - 1) * GRID_W + ctx_rows
-    branch = []
+    arrived = []
     for c in range(chunks):
         attended = call(
             functools.partial(attention_kernel, chunk=c, sp_count=sp_count),
@@ -499,16 +524,32 @@
             ctx_all[c],
         )
         found = pieces_by_bits(attended, "tp")
-        last = c == chunks - 1
-        branch = [
-            call(
-                functools.partial(
-                    output_kernel, masks=[m for m, _ in found], chunk=c, chunks=chunks
-                ),
-                shape_of((tokens, cols), BF16 if last else F32),
-            )(w_out, *[p for _, p in found], *branch, *([resid, mod_own] if last else []))
-        ]
-    return branch[0]
+        arrived += [((mask, c, chunks), piece) for mask, piece in found]
+
+    stages = [[], [], []]
+    for place, piece in arrived:
+        late = place[1] == chunks - 1 and place[0] > 1
+        stages[1 + place[0] % 2 if late else 0].append((place, piece))
+    stages = [stage for stage in stages if stage]
+    result = resid
+    for s, stage in enumerate(stages):
+        last = s == len(stages) - 1
+        result = call(
+            functools.partial(
+                output_kernel,
+                places=[place for place, _ in stage],
+                blocks=OUT_BLOCKS if last else 0,
+            ),
+            shape_of((tokens, cols), BF16 if last else F32),
+            scratch=[
+                pltpu.VMEM((tokens, cols), BF16),
+                pltpu.SemaphoreType.DMA((OUT_BLOCKS,)),
+            ]
+            if last
+            else [],
+            **(dict(out_specs=HBM) if last else {}),
+        )(w_out, mod_own, result, *[piece for _, piece in stage])
+    return result
 
 
 def solution(mesh):

time: 37.4 us -> 37.2 us (level)
  waiting for transfers between devices: 13.9 us -> 13.5 us
    pallas_call x2 -> x3, Pallas kernels: 1.5 us -> 1.68 us  [local(): call(functools.partial(output_kernel, places=[place for place, _ in stage...]
  transfers between devices with their start and end apart: 18 -> 18, of which waited for: 10 -> 10; matrix products, arithmetic and copies ran while one was open for 0% -> 0% of each run, Pallas kernels for 15% -> 16%
where the time goes in v8:
time: 37.2 us; the launch traced here: 36.9 us
  waiting for transfers between devices  13.5 us (36%)
  starting transfers between devices  12.6 us (34%)
  Pallas kernels  10.3 us (28%)
    ppermute x15, waiting for transfers between devices, peer(): return lax.ppermute(block, axis, [(i, i ^ mask) for i in range(count)])  11.4 us
    ppermute x15, starting transfers between devices, peer(): return lax.ppermute(block, axis, [(i, i ^ mask) for i in range(count)])  11.2 us
    pallas_call x2, Pallas kernels, local(): call(functools.partial(attention_kernel, chunk=c, sp_count=sp_count), sha...  2.18 us
    ppermute x3, waiting for transfers between devices, pairwise(): return lax.ppermute(block, axis, pairs)  2.1 us
    pallas_call x1, Pallas kernels, local(): call(functools.partial(prepare_kernel, chunks=chunks), (shape_of((tokens,...  1.82 us
    pallas_call x1, Pallas kernels, local(): call(modulation_kernel, shape_of((2 * MOD_ROWS + context.shape[0], cols),...  1.8 us
    pallas_call x1, Pallas kernels, local(): call(functools.partial(norm_kernel, chunks=chunks, tp_count=tp_count, eve...  1.69 us
    pallas_call x3, Pallas kernels, local(): call(functools.partial(output_kernel, places=[place for place, _ in stage...  1.68 us
  transfers between devices with their start and end apart: 18, of which 10 were waited for; matrix products, arithmetic and copies ran while one was open for 0% of the time, Pallas kernels for 16%

profile of v8, /device:TPU:0, one launch (start us, length us, event | category | flops | bytes accessed | tf_op | source)
XLA Modules:
  0.0 36.9 jit_solution(15899217941746627477)
XLA Ops:
  0.0 1.8 %shard_map.127 = bf16[32,512]{1,0:T(8,128)(2,1)S(1)} custom-call(bf16[512]{0:T(512)(128)(2,1)} %cond_hbm.1, bf16[512]{0:T(512)(128)(2,1)} %ctx_hbm.1, bf16[512,512]{1,0:T(8,128)(2,1)} %w_shift_hbm.1, bf16[512,512]{1,0:T(8,128)(2,1)} %w_scale_hbm.1, bf16[512,512]{1,0:T(8,128)(2,1)} %w_gate_hbm.1, bf16[16,2048]{1,0:T(8,128)(2,1)} %context_hbm.1), custom_call_target="tpu_custom_call" | custom-call | tf_op jit(solution)/shard_map/pallas_call | solution.py:452
  1.8 5.1 %collective-permute-start = (bf16[32,512]{1,0:T(8,128)(2,1)S(1)}, bf16[32,512]{1,0:T(8,128)(2,1)S(1)}, u32[]{:S(2)}, u32[]{:S(2)}) collective-permute-start(bf16[32,512]{1,0:T(8,128)(2,1)S(1)} %shard_map.127), channel_id=1, source_target_pairs={{0,12},{4,8},{8,4},{12,0},{1,13},{5,9},{9,5},{13,1},{2,14},{6,10},... | collective-permute-start | bytes 98312 | tf_op jit(solution)/shard_map/ppermute | solution.py:58
  7.0 0.6 %collective-permute-start.2 = (bf16[32,512]{1,0:T(8,128)(2,1)S(1)}, bf16[32,512]{1,0:T(8,128)(2,1)S(1)}, u32[]{:S(2)}, u32[]{:S(2)}) collective-permute-start(bf16[32,512]{1,0:T(8,128)(2,1)S(1)} %shard_map.127), channel_id=1, source_target_pairs={{0,4},{4,0},{8,12},{12,8},{1,5},{5,1},{9,13},{13,9},{2,6},{6,2},{1... | collective-permute-start | bytes 98312 | tf_op jit(solution)/shard_map/ppermute | solution.py:58
  7.6 0.1 rev.3
  7.7 1.2 %collective-permute-done = bf16[32,512]{1,0:T(8,128)(2,1)S(1)} collective-permute-done((bf16[32,512]{1,0:T(8,128)(2,1)S(1)}, bf16[32,512]{1,0:T(8,128)(2,1)S(1)}, u32[]{:S(2)}, u32[]{:S(2)}) %collective-permute-start) | collective-permute-done | bytes 32800 | tf_op jit(solution)/shard_map/ppermute | solution.py:58
  8.9 2.9 %collective-permute-done.1 = bf16[32,512]{1,0:T(8,128)(2,1)S(1)} collective-permute-done((bf16[32,512]{1,0:T(8,128)(2,1)S(1)}, bf16[32,512]{1,0:T(8,128)(2,1)S(1)}, u32[]{:S(2)}, u32[]{:S(2)}) %collective-permute-start.1) | collective-permute-done | bytes 32800 | tf_op jit(solution)/shard_map/ppermute | solution.py:58
  11.9 1.6 %collective-permute-start.4 = (f32[8,512]{1,0:T(8,128)S(1)}, f32[8,512]{1,0:T(8,128)S(1)}, u32[]{:S(2)}, u32[]{:S(2)}) collective-permute-start(f32[8,512]{1,0:T(8,128)S(1)} %add_add_fusion.refs_5_.refs_1_), channel_id=1, source_target_pairs={{0,2},{1,3},{2,0},{3,1},{4,6},{5,7},{6,4},{7,5},{8,10},{9,11},{10,... | collective-permute-start | bytes 49160 | tf_op jit(solution)/shard_map/ppermute | solution.py:58
  13.4 0.3 collective-permute-start.5
  13.7 0.1 pad_maximum_fusion.1
  13.8 1.8 %shard_map.128 = (f32[384,128]{1,0:T(8,128)S(1)}, f32[8,2048]{1,0:T(8,128)S(1)}, bf16[2048,256]{1,0:T(8,128)(2,1)S(1)}, bf16[2048,256]{1,0:T(8,128)(2,1)S(1)}, f...) custom-call(bf16[384,2048]{1,0:T(8,128)(2,1)S(1)} %copy-done, bf16[2048]{0:T(1024)(128)(2,1)} %refs_1_.1, ...), custom_call_target="tpu_custom_call" | custom-call | tf_op jit(solution)/shard_map/pallas_call | solution.py:469
  15.7 0.9 %collective-permute-done.5.refs_8_ = f32[8,512]{1,0:T(8,128)S(1)} collective-permute-done((f32[8,512]{1,0:T(8,128)S(1)}, f32[8,512]{1,0:T(8,128)S(1)}, u32[]{:S(2)}, u32[]{:S(2)}) %collective-permute-start.5) | collective-permute-done | bytes 16416 | tf_op jit(solution)/shard_map/ppermute | solution.py:58
  16.6 1.7 %shard_map.129 = (bf16[384,2048]{1,0:T(8,128)(2,1)S(1)}, f32[8,2048]{1,0:T(8,128)S(1)}, bf16[384,256]{1,0:T(8,128)(2,1)S(1)}, bf16[384,256]{1,0:T(8,128)(2,1)S(1...) custom-call(bf16[384,2048]{1,0:T(8,128)(2,1)S(1)} %copy-done, ...), custom_call_target="tpu_custom_call" | custom-call | tf_op jit(solution)/shard_map/pallas_call | solution.py:480
  18.4 0.8 %collective-permute-start.8 = (bf16[64,512]{1,0:T(8,128)(2,1)S(1)}, bf16[64,512]{1,0:T(8,128)(2,1)S(1)}, u32[]{:S(2)}, u32[]{:S(2)}) collective-permute-start(bf16[64,512]{1,0:T(8,128)(2,1)S(1)} %pad_maximum_fusion.refs_2_), channel_id=1, source_target_pairs={{0,2},{1,3},{2,0},{3,1},{4,6},{5,7},{6,4},{7,5},{8,10},{9,11},{10,... | collective-permute-start | bytes 196616 | tf_op jit(solution)/shard_map/ppermute | solution.py:58
  19.2 0.7 %collective-permute-start.7 = (bf16[256,256]{1,0:T(8,128)(2,1)S(1)}, bf16[256,256]{1,0:T(8,128)(2,1)S(1)}, u32[]{:S(2)}, u32[]{:S(2)}) collective-permute-start(bf16[256,256]{1,0:T(8,128)(2,1)S(1)} %get-tuple-element.31), channel_id=1, source_target_pairs={{4,8},{8,4},{5,9},{9,5},{6,10},{10,6},{7,11},{11,7},{20,24},{24,20... | collective-permute-start | bytes 393224 | tf_op jit(solution)/shard_map/ppermute | solution.py:102
  19.9 0.7 %collective-permute-start.14 = (bf16[256,256]{1,0:T(8,128)(2,1)S(1)}, bf16[256,256]{1,0:T(8,128)(2,1)S(1)}, u32[]{:S(2)}, u32[]{:S(2)}) collective-permute-start(bf16[256,256]{1,0:T(8,128)(2,1)S(1)} %get-tuple-element.36), channel_id=1, source_target_pairs={{4,8},{8,4},{5,9},{9,5},{6,10},{10,6},{7,11},{11,7},{20,24},{24,20... | collective-permute-start | bytes 393224 | tf_op jit(solution)/shard_map/ppermute | solution.py:102
  20.6 2.1 %collective-permute-done.8.refs_3_ = bf16[64,512]{1,0:T(8,128)(2,1)S(1)} collective-permute-done((bf16[64,512]{1,0:T(8,128)(2,1)S(1)}, bf16[64,512]{1,0:T(8,128)(2,1)S(1)}, u32[]{:S(2)}, u32[]{:S(2)}) %collective-permute-start.8) | collective-permute-done | bytes 65568 | tf_op jit(solution)/shard_map/ppermute | solution.py:58
  22.8 0.6 %shard_map.130 = (bf16[384,256]{1,0:T(8,128)(2,1)S(1)}, bf16[384,512]{1,0:T(8,128)(2,1)S(1)}) custom-call(bf16[384,2048]{1,0:T(8,128)(2,1)S(1)} %get-tuple-element.26.normed_ref, bf16[2048,256]{1,0:T(8,128)(2,1)S(1)} %copy-done.2, bf16[384,2048]{1,0:T(8,128)(2,1)S(1)} %copy-done), custom_call_target="tpu_custom_call" | custom-call | tf_op jit(solution)/shard_map/pallas_call | solution.py:492
  23.4 0.7 %collective-permute-done.10.refs_5_ = bf16[64,512]{1,0:T(8,128)(2,1)S(1)} collective-permute-done((bf16[64,512]{1,0:T(8,128)(2,1)S(1)}, bf16[64,512]{1,0:T(8,128)(2,1)S(1)}, u32[]{:S(2)}, u32[]{:S(2)}) %collective-permute-start.10) | collective-permute-done | bytes 65568 | tf_op jit(solution)/shard_map/ppermute | solution.py:58
  24.0 0.6 %shard_map.131 = (bf16[64,256]{1,0:T(8,128)(2,1)S(1)}, bf16[64,256]{1,0:T(8,128)(2,1)S(1)}) custom-call(f32[8,2048]{1,0:T(8,128)S(1)} %get-tuple-element.33.refs_0_, f32[8,2048]{1,0:T(8,128)S(1)} %get-tuple-element.23.refs_2_.refs_1_, bf16[64,512]{1,0:T(8,128)(2,1)S(1)} %pad_maximum_fusion.refs_2_, bf16[64,512]{1,0:T(8,128)(2,1)S(1)} %collective-permute-done.8.refs_3_, ...), custom_call_target="tpu_custom_call" | custom-call | tf_op jit(solution)/shard_map/pallas_call | solution.py:503
  24.6 2.1 %collective-permute-done.6.recv_a_ref = bf16[256,512]{1,0:T(8,128)(2,1)S(1)} collective-permute-done((bf16[256,512]{1,0:T(8,128)(2,1)S(1)}, bf16[256,512]{1,0:T(8,128)(2,1)S(1)}, u32[]{:S(2)}, u32[]{:S(2)}) %collective-permute-start.6) | collective-permute-done | bytes 262176 | tf_op jit(solution)/shard_map/ppermute | solution.py:102
  26.7 1.1 %shard_map.132.refs_3_ = bf16[384,128]{1,0:T(8,128)(2,1)S(1)} custom-call(bf16[384,256]{1,0:T(8,128)(2,1)S(1)} %get-tuple-element.28.q_ref, bf16[384,256]{1,0:T(8,128)(2,1)S(1)} %get-tuple-element.29.kv_ref, bf16[256,512]{1,0:T(8,128)(2,1)S(1)} %collective-permute-done.6.recv_a_ref, bf16[256,256]{1,0:T(8,128)(2,1)S(1)} %collective-permute-done.7.recv_b_ref, ...), custom_call_target="tpu_custom_call" | custom-call | tf_op jit(solution)/shard_map/pallas_call | solution.py:510
  27.8 0.9 %collective-permute-start.11 = (bf16[384,128]{1,0:T(8,128)(2,1)S(1)}, bf16[384,128]{1,0:T(8,128)(2,1)S(1)}, u32[]{:S(2)}, u32[]{:S(2)}) collective-permute-start(bf16[384,128]{1,0:T(8,128)(2,1)S(1)} %shard_map.132.refs_3_), channel_id=1, source_target_pairs={{0,2},{1,3},{2,0},{3,1},{4,6},{5,7},{6,4},{7,5},{8,10},{9,11},{10,... | collective-permute-start | bytes 294920 | tf_op jit(solution)/shard_map/ppermute | solution.py:58
  28.7 1.1 %shard_map.133.refs_7_ = bf16[384,128]{1,0:T(8,128)(2,1)S(1)} custom-call(bf16[384,256]{1,0:T(8,128)(2,1)S(1)} %get-tuple-element.28.q_ref, bf16[384,256]{1,0:T(8,128)(2,1)S(1)} %get-tuple-element.35.kv_ref, bf16[256,512]{1,0:T(8,128)(2,1)S(1)} %collective-permute-done.6.recv_a_ref, bf16[256,256]{1,0:T(8,128)(2,1)S(1)} %collective-permute-done.14.recv_b_ref, ...), custom_call_target="tpu_custom_call" | custom-call | tf_op jit(solution)/shard_map/pallas_call | solution.py:510
  29.8 1.3 %collective-permute-start.16 = (bf16[384,128]{1,0:T(8,128)(2,1)S(1)}, bf16[384,128]{1,0:T(8,128)(2,1)S(1)}, u32[]{:S(2)}, u32[]{:S(2)}) collective-permute-start(bf16[384,128]{1,0:T(8,128)(2,1)S(1)} %shard_map.133.refs_7_), channel_id=1, source_target_pairs={{0,2},{1,3},{2,0},{3,1},{4,6},{5,7},{6,4},{7,5},{8,10},{9,11},{10,... | collective-permute-start | bytes 294920 | tf_op jit(solution)/shard_map/ppermute | solution.py:58
  31.1 0.5 %collective-permute-start.12 = (bf16[384,128]{1,0:T(8,128)(2,1)S(1)}, bf16[384,128]{1,0:T(8,128)(2,1)S(1)}, u32[]{:S(2)}, u32[]{:S(2)}) collective-permute-start(bf16[384,128]{1,0:T(8,128)(2,1)S(1)} %shard_map.132.refs_3_), channel_id=1, source_target_pairs={{0,1},{1,0},{2,3},{3,2},{4,5},{5,4},{6,7},{7,6},{8,9},{9,8},{10,11... | collective-permute-start | bytes 294920 | tf_op jit(solution)/shard_map/ppermute | solution.py:58
  31.6 1.9 %collective-permute-done.11.refs_4_ = bf16[384,128]{1,0:T(8,128)(2,1)S(1)} collective-permute-done((bf16[384,128]{1,0:T(8,128)(2,1)S(1)}, bf16[384,128]{1,0:T(8,128)(2,1)S(1)}, u32[]{:S(2)}, u32[]{:S(2)}) %collective-permute-start.11) | collective-permute-done | bytes 98336 | tf_op jit(solution)/shard_map/ppermute | solution.py:58
  33.5 1.1 %collective-permute-done.16.refs_3_ = bf16[384,128]{1,0:T(8,128)(2,1)S(1)} collective-permute-done((bf16[384,128]{1,0:T(8,128)(2,1)S(1)}, bf16[384,128]{1,0:T(8,128)(2,1)S(1)}, u32[]{:S(2)}, u32[]{:S(2)}) %collective-permute-start.16) | collective-permute-done | bytes 98336 | tf_op jit(solution)/shard_map/ppermute | solution.py:58
  34.6 0.2 collective-permute-done.13.refs_6_
  34.8 0.5 %shard_map.134.refs_2_ = f32[384,512]{1,0:T(8,128)S(1)} custom-call(bf16[1024,512]{1,0:T(8,128)(2,1)S(1)} %copy-done.1, f32[8,512]{1,0:T(8,128)S(1)} %add_add_fusion.refs_5_.refs_1_, bf16[384,512]{1,0:T(8,128)(2,1)S(1)} %get-tuple-element.27.refs_2_, bf16[384,128]{1,0:T(8,128)(2,1)S(1)} %shard_map.132.refs_3_, ...), custom_call_target="tpu_custom_call" | custom-call | tf_op jit(solution)/shard_map/pallas_call | solution.py:537
  35.3 0.3 shard_map.135.refs_2_
  35.5 0.4 %collective-permute-done.17.refs_3_ = bf16[384,128]{1,0:T(8,128)(2,1)S(1)} collective-permute-done((bf16[384,128]{1,0:T(8,128)(2,1)S(1)}, bf16[384,128]{1,0:T(8,128)(2,1)S(1)}, u32[]{:S(2)}, u32[]{:S(2)}) %collective-permute-start.17) | collective-permute-done | bytes 98336 | tf_op jit(solution)/shard_map/ppermute | solution.py:58
  35.9 1.0 %shard_map.136 = bf16[384,512]{1,0:T(8,128)(2,1)} custom-call(bf16[1024,512]{1,0:T(8,128)(2,1)S(1)} %copy-done.1, f32[8,512]{1,0:T(8,128)S(1)} %add_add_fusion.refs_5_.refs_1_, f32[384,512]{1,0:T(8,128)S(1)} %shard_map.135.refs_2_, bf16[384,128]{1,0:T(8,128)(2,1)S(1)} %collective-permute-done.17.refs_3_), custom_call_target="tpu_custom_call" | custom-call | tf_op jit(solution)/shard_map/pallas_call | solution.py:537
  (32 shorter events, 0.3 us)
Async XLA Ops:
  0.0 7.6 %copy-start.3 = (f32[4,15,31]{2,0,1:T(4,128)S(1)}, f32[4,15,31]{2,0,1:T(4,128)}, u32[]{:S(2)}) copy-start(f32[4,15,31]{2,0,1:T(4,128)} %param.24) | copy-start | bytes 22324
  0.0 13.8 %copy-start = (bf16[384,2048]{1,0:T(8,128)(2,1)S(1)}, bf16[384,2048]{1,0:T(8,128)(2,1)}, u32[]{:S(2)}) copy-start(bf16[384,2048]{1,0:T(8,128)(2,1)} %latent_ref.1) | copy-start | bytes 4718596
  1.8 7.0 %collective-permute-start = (bf16[32,512]{1,0:T(8,128)(2,1)S(1)}, bf16[32,512]{1,0:T(8,128)(2,1)S(1)}, u32[]{:S(2)}, u32[]{:S(2)}) collective-permute-start(bf16[32,512]{1,0:T(8,128)(2,1)S(1)} %shard_map.127), channel_id=1, source_target_pairs={{0,12},{4,8},{8,4},{12,0},{1,13},{5,9},{9,5},{13,1},{2,14},{6,10},... | collective-permute-start | bytes 98312 | tf_op jit(solution)/shard_map/ppermute | solution.py:58
  7.0 4.8 %collective-permute-start.1 = (bf16[32,512]{1,0:T(8,128)(2,1)S(1)}, bf16[32,512]{1,0:T(8,128)(2,1)S(1)}, u32[]{:S(2)}, u32[]{:S(2)}) collective-permute-start(bf16[32,512]{1,0:T(8,128)(2,1)S(1)} %shard_map.127), channel_id=1, source_target_pairs={{0,8},{4,12},{8,0},{12,4},{1,9},{5,13},{9,1},{13,5},{2,10},{6,14},... | collective-permute-start | bytes 98312 | tf_op jit(solution)/shard_map/ppermute | solution.py:58
  7.0 4.8 %collective-permute-start.2 = (bf16[32,512]{1,0:T(8,128)(2,1)S(1)}, bf16[32,512]{1,0:T(8,128)(2,1)S(1)}, u32[]{:S(2)}, u32[]{:S(2)}) collective-permute-start(bf16[32,512]{1,0:T(8,128)(2,1)S(1)} %shard_map.127), channel_id=1, source_target_pairs={{0,4},{4,0},{8,12},{12,8},{1,5},{5,1},{9,13},{13,9},{2,6},{6,2},{1... | collective-permute-start | bytes 98312 | tf_op jit(solution)/shard_map/ppermute | solution.py:58
  11.8 3.8 %collective-permute-start.3 = (f32[8,512]{1,0:T(8,128)S(1)}, f32[8,512]{1,0:T(8,128)S(1)}, u32[]{:S(2)}, u32[]{:S(2)}) collective-permute-start(f32[8,512]{1,0:T(8,128)S(1)} %add_add_fusion.refs_5_.refs_1_), channel_id=1, source_target_pairs={{0,1},{1,0},{2,3},{3,2},{4,5},{5,4},{6,7},{7,6},{8,9},{9,8},{10,11... | collective-permute-start | bytes 49160 | tf_op jit(solution)/shard_map/ppermute | solution.py:58
  11.9 3.8 %collective-permute-start.4 = (f32[8,512]{1,0:T(8,128)S(1)}, f32[8,512]{1,0:T(8,128)S(1)}, u32[]{:S(2)}, u32[]{:S(2)}) collective-permute-start(f32[8,512]{1,0:T(8,128)S(1)} %add_add_fusion.refs_5_.refs_1_), channel_id=1, source_target_pairs={{0,2},{1,3},{2,0},{3,1},{4,6},{5,7},{6,4},{7,5},{8,10},{9,11},{10,... | collective-permute-start | bytes 49160 | tf_op jit(solution)/shard_map/ppermute | solution.py:58
  13.4 3.2 %collective-permute-start.5 = (f32[8,512]{1,0:T(8,128)S(1)}, f32[8,512]{1,0:T(8,128)S(1)}, u32[]{:S(2)}, u32[]{:S(2)}) collective-permute-start(f32[8,512]{1,0:T(8,128)S(1)} %add_add_fusion.refs_5_.refs_1_), channel_id=1, source_target_pairs={{0,3},{1,2},{2,1},{3,0},{4,7},{5,6},{6,5},{7,4},{8,11},{9,10},{10,... | collective-permute-start | bytes 49160 | tf_op jit(solution)/shard_map/ppermute | solution.py:58
  16.6 6.2 %copy-start.2 = (bf16[2048,256]{1,0:T(8,128)(2,1)S(1)}, bf16[2048,256]{1,0:T(8,128)(2,1)}, u32[]{:S(2)}) copy-start(bf16[2048,256]{1,0:T(8,128)(2,1)} %wq_ref.1) | copy-start | bytes 3145732
  18.3 8.4 %collective-permute-start.6 = (bf16[256,512]{1,0:T(8,128)(2,1)S(1)}, bf16[256,512]{1,0:T(8,128)(2,1)S(1)}, u32[]{:S(2)}, u32[]{:S(2)}) collective-permute-start(bf16[256,512]{1,0:T(8,128)(2,1)S(1)} %get-tuple-element.30), channel_id=1, source_target_pairs={{0,4},{4,0},{8,12},{12,8},{1,5},{5,1},{9,13},{13,9},{2,6},{6,2},{1... | collective-permute-start | bytes 786440 | tf_op jit(solution)/shard_map/ppermute | solution.py:102
  18.4 4.3 %collective-permute-start.8 = (bf16[64,512]{1,0:T(8,128)(2,1)S(1)}, bf16[64,512]{1,0:T(8,128)(2,1)S(1)}, u32[]{:S(2)}, u32[]{:S(2)}) collective-permute-start(bf16[64,512]{1,0:T(8,128)(2,1)S(1)} %pad_maximum_fusion.refs_2_), channel_id=1, source_target_pairs={{0,2},{1,3},{2,0},{3,1},{4,6},{5,7},{6,4},{7,5},{8,10},{9,11},{10,... | collective-permute-start | bytes 196616 | tf_op jit(solution)/shard_map/ppermute | solution.py:58
  19.2 5.4 %collective-permute-start.7 = (bf16[256,256]{1,0:T(8,128)(2,1)S(1)}, bf16[256,256]{1,0:T(8,128)(2,1)S(1)}, u32[]{:S(2)}, u32[]{:S(2)}) collective-permute-start(bf16[256,256]{1,0:T(8,128)(2,1)S(1)} %get-tuple-element.31), channel_id=1, source_target_pairs={{4,8},{8,4},{5,9},{9,5},{6,10},{10,6},{7,11},{11,7},{20,24},{24,20... | collective-permute-start | bytes 393224 | tf_op jit(solution)/shard_map/ppermute | solution.py:102
  19.9 8.8 %collective-permute-start.14 = (bf16[256,256]{1,0:T(8,128)(2,1)S(1)}, bf16[256,256]{1,0:T(8,128)(2,1)S(1)}, u32[]{:S(2)}, u32[]{:S(2)}) collective-permute-start(bf16[256,256]{1,0:T(8,128)(2,1)S(1)} %get-tuple-element.36), channel_id=1, source_target_pairs={{4,8},{8,4},{5,9},{9,5},{6,10},{10,6},{7,11},{11,7},{20,24},{24,20... | collective-permute-start | bytes 393224 | tf_op jit(solution)/shard_map/ppermute | solution.py:102
  20.5 2.8 %collective-permute-start.9 = (bf16[64,512]{1,0:T(8,128)(2,1)S(1)}, bf16[64,512]{1,0:T(8,128)(2,1)S(1)}, u32[]{:S(2)}, u32[]{:S(2)}) collective-permute-start(bf16[64,512]{1,0:T(8,128)(2,1)S(1)} %pad_maximum_fusion.refs_2_), channel_id=1, source_target_pairs={{0,1},{1,0},{2,3},{3,2},{4,5},{5,4},{6,7},{7,6},{8,9},{9,8},{10,11... | collective-permute-start | bytes 196616 | tf_op jit(solution)/shard_map/ppermute | solution.py:58
  22.8 1.3 %collective-permute-start.10 = (bf16[64,512]{1,0:T(8,128)(2,1)S(1)}, bf16[64,512]{1,0:T(8,128)(2,1)S(1)}, u32[]{:S(2)}, u32[]{:S(2)}) collective-permute-start(bf16[64,512]{1,0:T(8,128)(2,1)S(1)} %collective-permute-done.8.refs_3_), channel_id=1, source_target_pairs={{0,1},{1,0},{2,3},{3,2},{4,5},{5,4},{6,7},{7,6},{8,9},{9,8},{10,11... | collective-permute-start | bytes 196616 | tf_op jit(solution)/shard_map/ppermute | solution.py:58
  24.6 10.2 %copy-start.1 = (bf16[1024,512]{1,0:T(8,128)(2,1)S(1)}, bf16[1024,512]{1,0:T(8,128)(2,1)}, u32[]{:S(2)}) copy-start(bf16[1024,512]{1,0:T(8,128)(2,1)} %refs_0_.9) | copy-start | bytes 3145732
  27.8 5.7 %collective-permute-start.11 = (bf16[384,128]{1,0:T(8,128)(2,1)S(1)}, bf16[384,128]{1,0:T(8,128)(2,1)S(1)}, u32[]{:S(2)}, u32[]{:S(2)}) collective-permute-start(bf16[384,128]{1,0:T(8,128)(2,1)S(1)} %shard_map.132.refs_3_), channel_id=1, source_target_pairs={{0,2},{1,3},{2,0},{3,1},{4,6},{5,7},{6,4},{7,5},{8,10},{9,11},{10,... | collective-permute-start | bytes 294920 | tf_op jit(solution)/shard_map/ppermute | solution.py:58
  29.8 4.8 %collective-permute-start.16 = (bf16[384,128]{1,0:T(8,128)(2,1)S(1)}, bf16[384,128]{1,0:T(8,128)(2,1)S(1)}, u32[]{:S(2)}, u32[]{:S(2)}) collective-permute-start(bf16[384,128]{1,0:T(8,128)(2,1)S(1)} %shard_map.133.refs_7_), channel_id=1, source_target_pairs={{0,2},{1,3},{2,0},{3,1},{4,6},{5,7},{6,4},{7,5},{8,10},{9,11},{10,... | collective-permute-start | bytes 294920 | tf_op jit(solution)/shard_map/ppermute | solution.py:58
  31.1 3.5 %collective-permute-start.15 = (bf16[384,128]{1,0:T(8,128)(2,1)S(1)}, bf16[384,128]{1,0:T(8,128)(2,1)S(1)}, u32[]{:S(2)}, u32[]{:S(2)}) collective-permute-start(bf16[384,128]{1,0:T(8,128)(2,1)S(1)} %shard_map.133.refs_7_), channel_id=1, source_target_pairs={{0,1},{1,0},{2,3},{3,2},{4,5},{5,4},{6,7},{7,6},{8,9},{9,8},{10,11... | collective-permute-start | bytes 294920 | tf_op jit(solution)/shard_map/ppermute | solution.py:58
  31.1 3.5 %collective-permute-start.12 = (bf16[384,128]{1,0:T(8,128)(2,1)S(1)}, bf16[384,128]{1,0:T(8,128)(2,1)S(1)}, u32[]{:S(2)}, u32[]{:S(2)}) collective-permute-start(bf16[384,128]{1,0:T(8,128)(2,1)S(1)} %shard_map.132.refs_3_), channel_id=1, source_target_pairs={{0,1},{1,0},{2,3},{3,2},{4,5},{5,4},{6,7},{7,6},{8,9},{9,8},{10,11... | collective-permute-start | bytes 294920 | tf_op jit(solution)/shard_map/ppermute | solution.py:58
  33.5 1.3 %collective-permute-start.13 = (bf16[384,128]{1,0:T(8,128)(2,1)S(1)}, bf16[384,128]{1,0:T(8,128)(2,1)S(1)}, u32[]{:S(2)}, u32[]{:S(2)}) collective-permute-start(bf16[384,128]{1,0:T(8,128)(2,1)S(1)} %collective-permute-done.11.refs_4_), channel_id=1, source_target_pairs={{0,1},{1,0},{2,3},{3,2},{4,5},{5,4},{6,7},{7,6},{8,9},{9,8},{10,11... | collective-permute-start | bytes 294920 | tf_op jit(solution)/shard_map/ppermute | solution.py:58
  34.6 1.3 %collective-permute-start.17 = (bf16[384,128]{1,0:T(8,128)(2,1)S(1)}, bf16[384,128]{1,0:T(8,128)(2,1)S(1)}, u32[]{:S(2)}, u32[]{:S(2)}) collective-permute-start(bf16[384,128]{1,0:T(8,128)(2,1)S(1)} %collective-permute-done.16.refs_3_), channel_id=1, source_target_pairs={{0,1},{1,0},{2,3},{3,2},{4,5},{5,4},{6,7},{7,6},{8,9},{9,8},{10,11... | collective-permute-start | bytes 294920 | tf_op jit(solution)/shard_map/ppermute | solution.py:58
